TPU v7x, 512 devices: a whole 4x4x16 slice. The times are simulated.
512 devices in a mesh: ep: 128 (over z, x, core), tp: 4 (over y).
Axes of the slice: x: 4, y: 4, z: 16, core: 2. Of those that a mesh axis runs over, the one named last changes fastest.
Arguments:
- tokens: bfloat16 [1024, 1024], P('ep'), may hold values from -6 to 6
- lengths: int32 [1024], P('ep'), may hold values from 1 to 512, as said below
- cache_keys: bfloat16 [1024, 512, 4, 128], P('ep', None, 'tp'), may hold values from -2.5 to 2.5
- cache_values: bfloat16 [1024, 512, 4, 128], P('ep', None, 'tp'), may hold values from -6 to 6
- cache_cum: float32 [1024, 4, 512], P('ep', 'tp'), may hold values from -1536 to 0, as said below
- norm_gain: bfloat16 [1024], replicated, may hold values from 0.099609375 to 1.8984375
- query_weight: bfloat16 [1024, 1024], P(None, 'tp'), may hold values from -0.1875 to 0.1875
- key_weight: bfloat16 [1024, 512], P(None, 'tp'), may hold values from -0.1875 to 0.1875
- value_weight: bfloat16 [1024, 512], P(None, 'tp'), may hold values from -0.1875 to 0.1875
- forget_weight: bfloat16 [1024, 4], P(None, 'tp'), may hold values from -0.1875 to 0.1875
- forget_bias: float32 [4], P('tp'), may hold values from -1 to 2
- query_gain: bfloat16 [128], replicated, may hold values from 0.29882812 to 2.5
- key_gain: bfloat16 [128], replicated, may hold values from 0.099609375 to 1.8984375
- out_weight: bfloat16 [1024, 1024], P('tp'), may hold values from -0.1875 to 0.1875
- ffn_gain: bfloat16 [1024], replicated, may hold values from 0.099609375 to 1.8984375
- mix_weight: bfloat16 [1024], replicated, may hold values from -0.1875 to 0.1875
- shared_gate: bfloat16 [1024, 4096], P(None, 'ep'), may hold values from -0.1875 to 0.1875
- shared_up: bfloat16 [1024, 4096], P(None, 'ep'), may hold values from -0.1875 to 0.1875
- shared_down: bfloat16 [4096, 1024], P('ep', 'tp'), may hold values from -0.09375 to 0.09375
- routes: int32 [1024, 2], P('ep'), may hold values from 0 to 127, all different within a row; in each aligned block of 8 rows (0 to 7, 8 to 15, ...) at most 4 rows name the same one
- route_weights: float32 [1024, 2], P('ep'), may hold values from 0.1 to 1
- expert_gate: bfloat16 [128, 1024, 512], P('ep', None, 'tp'), may hold values from -0.1875 to 0.1875
- expert_up: bfloat16 [128, 1024, 512], P('ep', None, 'tp'), may hold values from -0.1875 to 0.1875
- expert_down: bfloat16 [128, 512, 1024], P('ep', 'tp'), may hold values from -0.25 to 0.25
Outputs:
- layer_out: bfloat16 [1024, 1024], P('ep', 'tp')
Inputs may be any that keep to these rules, and one draw needn't show every extreme that they name: `lengths`: at least one sequence has exactly 512 cached positions. `cache_cum`: along the positions each row never rises. `routes`: the 2 experts of a token differ; among the 8 rows of one device no expert is named by more than 4 rows, a bound that some block reaches.
All inputs are finite; a program needn't handle non-finite values.
Results may differ from a plain program's by a relative error of at most 0.013.
Values may be sent and summed in bfloat16 or wider, within the bound.
No kernel may reach another device: no remote copies, remote signals or barrier semaphores. Data moves between devices by JAX's collectives and lax.ppermute only.
A program may use at most 64 MiB of HBM per device.

v0:
```python
import jax
import jax.numpy as jnp
from jax import lax
from jax.sharding import Mesh
from jax.sharding import PartitionSpec as P

CAP = 4
EP = ("ep_0", "ep_1", "ep_2")


epsilon = 1e-06


def copy_for_each(shard, axis):
    peers = lax.axis_size(axis)
    return lax.all_to_all(
        jnp.broadcast_to(shard[None], (peers, *shard.shape)), axis, 0, 0, tiled=True
    )


def of_everyone(shard, axis):
    return copy_for_each(shard, axis).astype(jnp.float32).sum(axis=0)


def cut_along(shard, dim, peers):
    before, after = (shard.shape[:dim], shard.shape[dim + 1 :])
    return jnp.moveaxis(shard.reshape(*before, peers, -1, *after), dim, 0)


def summed_on_arrival(shard, axis, dim):
    peers = lax.axis_size(axis)
    tiles = lax.all_to_all(cut_along(shard, dim, peers), axis, 0, 0, tiled=True)
    return jnp.sum(tiles.astype(jnp.float32), axis=0)


def sum_in_order(tiles, axes, sequence):
    shape = [lax.axis_size(a) for a in axes]
    tiles = tiles.reshape(*shape, *tiles.shape[1:])
    tiles = tiles.transpose(*sequence, *range(len(axes), tiles.ndim))
    tiles = tiles.reshape(-1, *tiles.shape[len(axes) :])
    for k in sequence:
        tiles = lax.psum_scatter(tiles, axes[k], scatter_dimension=0, tiled=True)
    return tiles[0]


def summed_rows(shard, axes, sequence, dim):
    peers = lax.axis_size(axes)
    return sum_in_order(cut_along(shard, dim, peers), axes, sequence)


def rms_norm(values, gain):
    values = values.astype(jnp.float32)
    return (
        values
        * lax.rsqrt(jnp.mean(values * values, axis=-1, keepdims=True) + epsilon)
        * gain.astype(jnp.float32)
    )


def per_device(
    tokens,
    lengths,
    cache_keys,
    cache_values,
    cache_cum,
    norm_gain,
    query_weight,
    key_weight,
    value_weight,
    forget_weight,
    forget_bias,
    query_gain,
    key_gain,
    out_weight,
    ffn_gain,
    mix_weight,
    shared_gate,
    shared_up,
    shared_down,
    routes,
    route_weights,
    expert_gate,
    expert_up,
    expert_down,
):
    seq_rows = tokens.shape[0]
    cache_len = cache_keys.shape[1]
    kv_local = cache_keys.shape[2]
    head_size = cache_keys.shape[3]
    normed = rms_norm(tokens, norm_gain).astype(jnp.bfloat16)
    query = jnp.dot(normed, query_weight, preferred_element_type=jnp.float32)
    query = rms_norm(query.reshape(seq_rows, kv_local, -1, head_size), query_gain).astype(
        jnp.bfloat16
    )
    new_key = jnp.dot(normed, key_weight, preferred_element_type=jnp.float32)
    new_key = rms_norm(new_key.reshape(seq_rows, kv_local, head_size), key_gain).astype(
        jnp.bfloat16
    )
    new_value = jnp.dot(normed, value_weight, preferred_element_type=jnp.float32).astype(
        jnp.bfloat16
    )
    new_value = new_value.reshape(seq_rows, kv_local, head_size)
    new_log = jax.nn.log_sigmoid(
        jnp.dot(normed, forget_weight, preferred_element_type=jnp.float32) + forget_bias
    )
    position = jnp.arange(cache_len, dtype=jnp.int32)
    live = position[None, :] < lengths[:, None]
    at_last = (position[None, :] == lengths[:, None] - 1)[:, None, :]
    last_cum = jnp.sum(jnp.where(at_last, cache_cum, 0.0), axis=-1)
    gate_bias = last_cum[:, :, None] - cache_cum + new_log[:, :, None]
    score_scale = head_size ** (-0.5)
    past = (
        jnp.einsum("skgd,spkd->skgp", query, cache_keys, preferred_element_type=jnp.float32)
        * score_scale
    )
    past = past + gate_bias[:, :, None, :]
    past = jnp.where(live[:, None, None, :], past, -jnp.inf)
    own = (
        jnp.sum(query.astype(jnp.float32) * new_key.astype(jnp.float32)[:, :, None, :], axis=-1)
        * score_scale
    )
    past_exp = jnp.exp(past)
    own_exp = jnp.exp(own)
    denominator = jnp.sum(past_exp, axis=-1) + own_exp
    past_prob = (past_exp / denominator[..., None]).astype(jnp.bfloat16)
    own_prob = (own_exp / denominator).astype(jnp.bfloat16)
    mixed = jnp.einsum(
        "skgp,spkd->skgd", past_prob, cache_values, preferred_element_type=jnp.float32
    )
    mixed = (
        mixed
        + own_prob.astype(jnp.float32)[..., None] * new_value.astype(jnp.float32)[:, :, None, :]
    )
    heads_out = mixed.astype(jnp.bfloat16).reshape(seq_rows, -1)
    partial_value = jnp.dot(heads_out, out_weight, preferred_element_type=jnp.float32)
    attended = of_everyone(partial_value.astype(jnp.bfloat16), "tp").astype(jnp.float32)
    residual = tokens.astype(jnp.float32) + attended
    ffn_in = rms_norm(residual, ffn_gain).astype(jnp.bfloat16)
    mix_gate = jax.nn.sigmoid(jnp.dot(ffn_in, mix_weight, preferred_element_type=jnp.float32))
    slice_width = ffn_in.shape[1] // lax.axis_size("tp")
    slice_start = lax.axis_index("tp") * slice_width
    ep_count = lax.axis_size(EP)
    local_experts = expert_gate.shape[0]
    num_experts = ep_count * local_experts
    topk = routes.shape[1]
    n_assign = seq_rows * topk
    order = jnp.arange(n_assign, dtype=jnp.int32)
    earlier = order[None, :] < order[:, None]
    slot_ids = jnp.arange(num_experts * CAP, dtype=jnp.int32)
    flat_route = routes.reshape(-1)
    same_expert = flat_route[:, None] == flat_route[None, :]
    slot_rank = jnp.sum(jnp.logical_and(same_expert, earlier), axis=1)
    slot_index = flat_route * CAP + slot_rank
    gathered_rows, gathered_routes = (
        lax.all_gather(ffn_in, EP, axis=0, tiled=True),
        lax.all_gather(routes, EP, axis=0, tiled=True),
    )
    pre_gate = jnp.dot(gathered_rows, shared_gate, preferred_element_type=jnp.float32)
    pre_up = jnp.dot(gathered_rows, shared_up, preferred_element_type=jnp.float32)
    shared_hidden = (jax.nn.silu(pre_gate) * pre_up).astype(jnp.bfloat16)
    terms = jnp.dot(shared_hidden, shared_down, preferred_element_type=jnp.float32)
    block_routes = gathered_routes.reshape(ep_count, n_assign)
    local_id = block_routes - lax.axis_index(EP) * local_experts
    mine = jnp.logical_and(local_id >= 0, local_id < local_experts)
    same_block = block_routes[:, :, None] == block_routes[:, None, :]
    block_rank = jnp.sum(jnp.logical_and(same_block, earlier[None, :, :]), axis=2)
    source = jnp.arange(ep_count, dtype=jnp.int32)[:, None]
    own_slot = source * (local_experts * CAP) + local_id * CAP + block_rank
    own_slot = jnp.where(mine, own_slot, -1).reshape(-1)
    pick_table = (own_slot[None, :] == slot_ids[:, None]).astype(jnp.bfloat16)
    repeated_all = jnp.repeat(gathered_rows, topk, axis=0)
    received = jnp.dot(pick_table, repeated_all, preferred_element_type=jnp.float32).astype(
        jnp.bfloat16
    )
    received = received.reshape(ep_count, local_experts, CAP, ffn_in.shape[1])
    pre_gate = jnp.einsum(
        "nekd,edf->nekf", received, expert_gate, preferred_element_type=jnp.float32
    )
    pre_up = jnp.einsum("nekd,edf->nekf", received, expert_up, preferred_element_type=jnp.float32)
    hidden = (jax.nn.silu(pre_gate) * pre_up).astype(jnp.bfloat16)
    part_out = jnp.einsum("nekf,efd->nekd", hidden, expert_down, preferred_element_type=jnp.float32)
    summed = summed_on_arrival(part_out.astype(jnp.bfloat16), "tp", 3)
    results = summed.astype(jnp.bfloat16)
    dense = summed_rows(terms, EP, (2, 0, 1), 0)
    returned = lax.all_to_all(results, EP, split_axis=0, concat_axis=0, tiled=True)
    returned = returned.reshape(num_experts * CAP, -1).astype(jnp.float32)
    norm_weights = route_weights / jnp.sum(route_weights, axis=1, keepdims=True)
    slot_table = slot_index.reshape(seq_rows, topk)
    combine = jnp.sum(
        (slot_table[:, :, None] == slot_ids[None, None, :]) * norm_weights[:, :, None], axis=1
    )
    routed = jnp.dot(combine, returned, precision=lax.Precision.HIGHEST)
    residual_slice = lax.dynamic_slice_in_dim(residual, slice_start, slice_width, 1)
    return (residual_slice + mix_gate[:, None] * dense + routed).astype(jnp.bfloat16)


def solution(mesh):
    finer = Mesh(mesh.devices.reshape(16, 4, 2, mesh.shape["tp"]), ("ep_0", "ep_1", "ep_2", "tp"))
    placed = (
        P(EP, None),
        P(EP),
        P(EP, None, "tp", None),
        P(EP, None, "tp", None),
        P(EP, "tp", None),
        P(),
        P(None, "tp"),
        P(None, "tp"),
        P(None, "tp"),
        P(None, "tp"),
        P("tp"),
        P(),
        P(),
        P("tp", None),
        P(),
        P(),
        P(None, EP),
        P(None, EP),
        P(EP, "tp"),
        P(EP, None),
        P(EP, None),
        P(EP, None, "tp"),
        P(EP, None, "tp"),
        P(EP, "tp", None),
    )
    return jax.shard_map(
        per_device, mesh=finer, in_specs=placed, out_specs=P(EP, "tp"), check_vma=False
    )
```

profile of v0, /device:TPU:1, one launch (start us, length us, event | category | flops | bytes accessed | tf_op | source)
XLA Modules:
  0.0 318.6 jit_solution(15933887718298431837)
XLA Ops:
  6.5 0.8 broadcast_add_fusion
  7.3 0.7 iota_compare_fusion.5
  8.7 0.7 convert_element_type.133
  9.4 0.7 convert_element_type.137
  10.0 0.8 fusion.43
  10.9 0.7 convert_element_type.131
  11.6 1.2 fusion.14
  12.7 1.3 multiply_reduce_fusion.2
  14.1 1.3 fusion.49
  15.5 0.1 copy.97
  15.5 0.1 fusion.60
  15.6 0.2 multiply_reduce_fusion.1
  15.8 0.1 copy.99
  15.8 0.9 fusion.47
  16.8 0.9 fusion.62
  17.7 0.8 subtract_add_fusion
  18.6 0.5 fusion.71
  19.1 0.3 fusion.13
  19.4 0.2 convolution_convert_fusion.1
  19.6 0.6 broadcast_in_dim.26
  20.2 5.0 %all-to-all-start = ((bf16[4,8,1024]{2,1,0:T(8,128)(2,1)}), bf16[4,8,1024]{2,1,0:T(8,128)(2,1)S(1)}, u32[]{:S(2)}, u32[]{:S(2)}) async-start(bf16[4,8,1024]{2,1,0:T(8,128)(2,1)} %broadcast_in_dim.26), calls=%async_computation | async-start | bytes 131072 | tf_op jit(solution)/shard_map/all_to_all | solution.py:16
  25.2 4.5 %all-to-all-done = bf16[4,8,1024]{2,1,0:T(8,128)(2,1)S(1)} async-done(((bf16[4,8,1024]{2,1,0:T(8,128)(2,1)}), bf16[4,8,1024]{2,1,0:T(8,128)(2,1)S(1)}, u32[]{:S(2)}, u32[]{:S(2)}) %all-to-all-start) | async-done | bytes 65568 | tf_op jit(solution)/shard_map/all_to_all | solution.py:16
  29.7 0.1 multiply_reduce_fusion
  29.9 0.7 multiply_convert_fusion
  30.6 91.3 %all-gather = s32[128,8,2]{1,2,0:T(2,128)S(1)} all-gather(s32[1,8,2]{1,2,0:T(2,128)S(1)} %bitcast.132), channel_id=1, replica_groups=mesh['ep_0'=16,'ep_1'=4,'ep_2'=2,'tp'=4] {'ep_0','ep_1','ep_2'}, dimensions={0}, use_global_device_ids=true | all-gather | bytes 8256 | tf_op jit(solution)/shard_map/all_gather | solution.py:156
  121.9 0.1 copy.104
  122.0 0.1 copy.107
  122.1 0.1 convert_reduce_fusion
  122.2 53.6 %all-gather.3.cloned.1.call-done = bf16[1024,1024]{1,0:T(8,128)(2,1)} async-done(((bf16[8,1024]{1,0:T(8,128)(2,1)}), bf16[1024,1024]{1,0:T(8,128)(2,1)}) %all-gather.3.cloned.1.call-update) | async-done | bytes 2097168 | tf_op jit(solution)/shard_map/all_gather | solution.py:155
  175.8 2.5 fusion.72
  178.3 2.0 fusion.7
  180.3 2.4 copy.100
  182.8 0.1 add.171
  182.9 0.1 add.172
  183.0 0.1 copy.108
  183.1 0.1 reduce_sum.139
  183.2 0.3 copy.105
  183.4 0.3 and.27
  183.8 1.0 copy.106
  184.8 1.3 mul.279
  186.1 3.6 %broadcast_in_dim.28 = bf16[1024,2,1024]{2,1,0:T(2,128)(2,1)} broadcast(bf16[1024,1024]{1,0:T(8,128)(2,1)S(1)} %copy-done.1), dimensions={0,2} | broadcast | bytes 6291456 | tf_op jit(solution)/shard_map/broadcast_in_dim | solution.py:171
  189.7 7.3 %reshape.353 = bf16[2048,1024]{1,0:T(8,128)(2,1)} reshape(bf16[1024,2,1024]{2,1,0:T(2,128)(2,1)} %broadcast_in_dim.28) | data formatting | bytes 8388608 | tf_op jit(solution)/shard_map/reshape | solution.py:171
  197.1 4.7 %fusion.2 = bf16[512,1024]{1,0:T(8,128)(2,1)S(1)} fusion(bf16[2048,1024]{1,0:T(8,128)(2,1)} %reshape.353, s32[2048]{0:T(1024)S(1)} %add_select_fusion), kind=kOutput, calls=%fused_computation.3 | convolution fusion | flops 2149056512 | bytes 5251072 | tf_op jit(solution)/shard_map/dot_general | solution.py:172
  201.7 0.4 reshape.354
  202.2 2.3 convolution_bitcast_fusion.1
  204.5 2.3 convolution_convert_fusion
  206.8 1.1 copy.138
  207.9 4.2 %all-to-all-start.1 = ((bf16[4,128,1,4,256]{4,1,3,2,0:T(8,128)(2,1)}), bf16[4,128,1,4,256]{4,1,3,2,0:T(8,128)(2,1)S(1)}, u32[]{:S(2)}, u32[]{:S(2)}) async-start(bf16[4,128,1,4,256]{4,1,3,2,0:T(8,128)(2,1)} %bitcast.122), calls=%async_computation.4 | async-start | bytes 2097152 | tf_op jit(solution)/shard_map/all_to_all | solution.py:32
  212.1 0.7 reduce-scatter.6.cloned.1.call-update
  212.8 13.9 %all-to-all-done.1 = bf16[4,128,1,4,256]{4,1,3,2,0:T(8,128)(2,1)S(1)} async-done(((bf16[4,128,1,4,256]{4,1,3,2,0:T(8,128)(2,1)}), bf16[4,128,1,4,256]{4,1,3,2,0:T(8,128)(2,1)S(1)}, u32[]{:S(2)}, u32[]{:S(2)}) %all-to-all-start.1) | async-done | bytes 1048608 | tf_op jit(solution)/shard_map/all_to_all | solution.py:32
  226.7 0.2 reduce_sum.140
  226.9 0.9 copy.113
  227.8 12.0 %all-to-all-start.2 = ((bf16[128,1,4,256]{3,2,1,0:T(4,128)(2,1)}), bf16[128,1,4,256]{3,2,1,0:T(4,128)(2,1)S(1)}, u32[]{:S(2)}, u32[]{:S(2)}) async-start(bf16[128,1,4,256]{3,2,1,0:T(4,128)(2,1)} %copy.113), calls=%async_computation.5 | async-start | bytes 524288 | tf_op jit(solution)/shard_map/all_to_all | solution.py:185
  239.9 0.1 copy.101
  240.0 0.1 eq.76
  240.0 0.2 convert_reduce_fusion.2
  240.2 0.1 reduce_sum.135
  240.3 0.1 copy.103
  240.5 0.1 select_reduce_fusion
  240.5 33.8 %reduce-scatter.6.cloned.1.call-done = f32[4,8,256]{2,1,0:T(8,128)} async-done(((f32[64,8,256]{2,1,0:T(8,128)}), f32[4,8,256]{2,1,0:T(8,128)}) %reduce-scatter.6.cloned.1.call-update) | async-done | bytes 32784 | tf_op jit(solution)/shard_map/reduce_scatter | solution.py:42
  274.4 0.1 fusion.18
  274.5 0.1 reshape.360
  274.6 36.0 %reduce-scatter.8.cloned.1.call-done = f32[1,8,256]{2,1,0:T(8,128)} async-done(((f32[4,8,256]{2,1,0:T(8,128)}), f32[1,8,256]{2,1,0:T(8,128)}) %reduce-scatter.8.cloned.1.call-update) | async-done | bytes 8208 | tf_op jit(solution)/shard_map/reduce_scatter | solution.py:42
  310.6 1.5 fusion.12
  (52 shorter events, 0.3 us)
Async XLA Ops:
  6.5 12.0 %copy-start = (bf16[8,512,1,128]{3,1,2,0:T(8,128)(2,1)S(1)}, bf16[8,512,1,128]{3,1,2,0:T(8,128)(2,1)}, u32[]{:S(2)}) copy-start(bf16[8,512,1,128]{3,1,2,0:T(8,128)(2,1)} %param.26) | copy-start | bytes 3145732
  6.5 12.5 %copy-start.12 = (bf16[8,512,1,128]{3,1,2,0:T(8,128)(2,1)S(1)}, bf16[8,512,1,128]{3,1,2,0:T(8,128)(2,1)}, u32[]{:S(2)}) copy-start(bf16[8,512,1,128]{3,1,2,0:T(8,128)(2,1)} %param.27) | copy-start | bytes 3145732
  6.5 12.8 %copy-start.2 = (bf16[256,1024]{1,0:T(8,128)(2,1)S(1)}, bf16[256,1024]{1,0:T(8,128)(2,1)}, u32[]{:S(2)}) copy-start(bf16[256,1024]{1,0:T(8,128)(2,1)} %param.37) | copy-start | bytes 1572868
  12.7 12.5 %copy-start.10 = (bf16[1024]{0:T(1024)(128)(2,1)S(1)}, bf16[1024]{0:T(1024)(128)(2,1)}, u32[]{:S(2)}) copy-start(bf16[1024]{0:T(1024)(128)(2,1)} %param.38) | copy-start | bytes 6148
  12.7 17.0 %copy-start.3 = (bf16[8,1024]{1,0:T(8,128)(2,1)S(1)}, bf16[8,1024]{1,0:T(8,128)(2,1)}, u32[]{:S(2)}) copy-start(bf16[8,1024]{1,0:T(8,128)(2,1)} %param.24) | copy-start | bytes 49156
  14.1 16.6 %copy-start.8 = (s32[8,2]{0,1:T(2,128)S(1)}, s32[8,2]{0,1:T(2,128)}, u32[]{:S(2)}) copy-start(s32[8,2]{0,1:T(2,128)} %param.43) | copy-start | bytes 196
  15.4 160.4 %copy-start.4 = (bf16[1024,32]{0,1:T(8,128)(2,1)S(1)}, bf16[1024,32]{0,1:T(8,128)(2,1)}, u32[]{:S(2)}) copy-start(bf16[1024,32]{0,1:T(8,128)(2,1)} %param.40) | copy-start | bytes 196612
  19.4 158.9 %copy-start.5 = (bf16[1024,32]{0,1:T(8,128)(2,1)S(1)}, bf16[1024,32]{0,1:T(8,128)(2,1)}, u32[]{:S(2)}) copy-start(bf16[1024,32]{0,1:T(8,128)(2,1)} %param.41) | copy-start | bytes 196612
  19.4 158.9 %copy-start.7 = (bf16[32,256]{1,0:T(8,128)(2,1)S(1)}, bf16[32,256]{1,0:T(8,128)(2,1)}, u32[]{:S(2)}) copy-start(bf16[32,256]{1,0:T(8,128)(2,1)} %param.42) | copy-start | bytes 49156
  20.2 9.5 %all-to-all-start = ((bf16[4,8,1024]{2,1,0:T(8,128)(2,1)}), bf16[4,8,1024]{2,1,0:T(8,128)(2,1)S(1)}, u32[]{:S(2)}, u32[]{:S(2)}) async-start(bf16[4,8,1024]{2,1,0:T(8,128)(2,1)} %broadcast_in_dim.26), calls=%async_computation | async-start | bytes 131072 | tf_op jit(solution)/shard_map/all_to_all | solution.py:16
  25.2 150.6 %all-gather.3.cloned.1.call-start = ((), (), s32[]{:S(2)}) async-start(), calls=%async_computation.6 | async-start | bytes 2113536 | tf_op jit(solution)/shard_map/all_gather | solution.py:155
  30.6 181.5 %reduce-scatter.4.cloned.1.call-start = ((), (), s32[]{:S(2)}) async-start(), calls=%async_computation.7 | async-start | bytes 1572864 | tf_op jit(solution)/shard_map/reduce_scatter | solution.py:42
  175.8 2.5 copy-start.1
  207.9 32.5 %copy-start.11 = (bf16[1024]{0:T(1024)(128)(2,1)S(1)}, bf16[1024]{0:T(1024)(128)(2,1)}, u32[]{:S(2)}) copy-start(bf16[1024]{0:T(1024)(128)(2,1)} %param.39) | copy-start | bytes 6148
  207.9 32.5 %copy-start.9 = (f32[8,2]{0,1:T(2,128)S(1)}, f32[8,2]{0,1:T(2,128)}, u32[]{:S(2)}) copy-start(f32[8,2]{0,1:T(2,128)} %param.44) | copy-start | bytes 196
  207.9 66.5 %copy-start.6 = (bf16[8,1024]{1,0:T(8,128)(2,1)S(1)}, bf16[8,1024]{1,0:T(8,128)(2,1)}, u32[]{:S(2)}) copy-start(bf16[8,1024]{1,0:T(8,128)(2,1)} %multiply_convert_fusion) | copy-start | bytes 49156
  207.9 18.8 %all-to-all-start.1 = ((bf16[4,128,1,4,256]{4,1,3,2,0:T(8,128)(2,1)}), bf16[4,128,1,4,256]{4,1,3,2,0:T(8,128)(2,1)S(1)}, u32[]{:S(2)}, u32[]{:S(2)}) async-start(bf16[4,128,1,4,256]{4,1,3,2,0:T(8,128)(2,1)} %bitcast.122), calls=%async_computation.4 | async-start | bytes 2097152 | tf_op jit(solution)/shard_map/all_to_all | solution.py:32
  212.1 62.3 %reduce-scatter.6.cloned.1.call-start = ((), (), s32[]{:S(2)}) async-start(), calls=%async_computation.8 | async-start | bytes 557056 | tf_op jit(solution)/shard_map/reduce_scatter | solution.py:42
  227.8 46.7 %all-to-all-start.2 = ((bf16[128,1,4,256]{3,2,1,0:T(4,128)(2,1)}), bf16[128,1,4,256]{3,2,1,0:T(4,128)(2,1)S(1)}, u32[]{:S(2)}, u32[]{:S(2)}) async-start(bf16[128,1,4,256]{3,2,1,0:T(4,128)(2,1)} %copy.113), calls=%async_computation.5 | async-start | bytes 524288 | tf_op jit(solution)/shard_map/all_to_all | solution.py:185
  239.8 70.8 %reduce-scatter.8.cloned.1.call-start = ((), (), s32[]{:S(2)}) async-start(), calls=%async_computation.9 | async-start | bytes 40960 | tf_op jit(solution)/shard_map/reduce_scatter | solution.py:42
Sparse Core Ops, SparseCore 0:
  30.7 145.0 all-gather.2
  182.9 16.1 reduce-scatter.3
  215.7 58.6 reduce-scatter.5
  277.0 33.5 reduce-scatter.7
where the time goes:
time: 321 us; the launch traced here: 319 us
  waiting for transfers between devices  143 us (45%)
  blocking collectives  91.3 us (28%)
  matrix products  21.2 us (7%)
  starting transfers between devices  21.2 us (7%)
  local copies, waits for them, and re-layouts  20.5 us (6%)
  between operations  14 us (4%)
  other arithmetic  7.9 us (2%)
    all_gather x1, blocking collectives, per_device(): lax.all_gather(routes, EP, axis=0, tiled=True)  91.3 us
    reduce_scatter x3, waiting for transfers between devices, sum_in_order(): tiles = lax.psum_scatter(tiles, axes[k], scatter_dimension=0, tiled=True)  69.8 us
    all_gather x1, waiting for transfers between devices, per_device(): lax.all_gather(ffn_in, EP, axis=0, tiled=True)  53.6 us
    all_to_all x1, waiting for transfers between devices, summed_on_arrival(): tiles = lax.all_to_all(cut_along(shard, dim, peers), axis, 0, 0, tiled=True)  13.9 us
    all_to_all x1, starting transfers between devices, per_device(): lax.all_to_all(results, EP, split_axis=0, concat_axis=0, tiled=True)  12 us
    reshape x1, local copies, waits for them, and re-layouts, per_device(): repeated_all = jnp.repeat(gathered_rows, topk, axis=0)  7.34 us
  transfers between devices with their start and end apart: 7, of which 5 were waited for; matrix products, arithmetic and copies ran while one was open for 9% of the time, Pallas kernels for 0%

commit v1 on v0

v1 whole, which is shorter than its diff:
```python
import jax
import jax.numpy as jnp
from jax import lax
from jax.sharding import Mesh
from jax.sharding import PartitionSpec as P

EP = ("ep_0", "ep_1", "ep_2")
PAIR = "ep_2"
LANES = 128


epsilon = 1e-06


def copy_for_each(shard, axis):
    peers = lax.axis_size(axis)
    return lax.all_to_all(
        jnp.broadcast_to(shard[None], (peers, *shard.shape)), axis, 0, 0, tiled=True
    )


def swap(shard):
    return lax.ppermute(shard, PAIR, [(0, 1), (1, 0)])


def lane_blocks(weight):
    rows, columns = weight.shape
    return jnp.concatenate(jnp.split(weight, columns // LANES, axis=1), axis=0)


def wide_rows(blocks, rows):
    peers = blocks.shape[0]
    blocks = blocks.reshape(peers, -1, rows, LANES)
    return jnp.moveaxis(blocks, 2, 1).reshape(peers, rows, -1)


def pair_of(values, member):
    split = values.reshape(2, -1, values.shape[-1])
    return lax.dynamic_index_in_dim(split, member, 1, keepdims=False)


def rms_norm(values, gain):
    values = values.astype(jnp.float32)
    return (
        values
        * lax.rsqrt(jnp.mean(values * values, axis=-1, keepdims=True) + epsilon)
        * gain.astype(jnp.float32)
    )


def per_device(
    tokens,
    lengths,
    cache_keys,
    cache_values,
    cache_cum,
    norm_gain,
    query_weight,
    key_weight,
    value_weight,
    forget_weight,
    forget_bias,
    query_gain,
    key_gain,
    out_weight,
    ffn_gain,
    mix_weight,
    shared_gate,
    shared_up,
    shared_down,
    routes,
    route_weights,
    expert_gate,
    expert_up,
    expert_down,
):
    seq_rows = tokens.shape[0]
    cache_len = cache_keys.shape[1]
    kv_local = cache_keys.shape[2]
    head_size = cache_keys.shape[3]
    normed = rms_norm(tokens, norm_gain).astype(jnp.bfloat16)
    query = jnp.dot(normed, query_weight, preferred_element_type=jnp.float32)
    query = rms_norm(query.reshape(seq_rows, kv_local, -1, head_size), query_gain).astype(
        jnp.bfloat16
    )
    new_key = jnp.dot(normed, key_weight, preferred_element_type=jnp.float32)
    new_key = rms_norm(new_key.reshape(seq_rows, kv_local, head_size), key_gain).astype(
        jnp.bfloat16
    )
    new_value = jnp.dot(normed, value_weight, preferred_element_type=jnp.float32).astype(
        jnp.bfloat16
    )
    new_value = new_value.reshape(seq_rows, kv_local, head_size)
    new_log = jax.nn.log_sigmoid(
        jnp.dot(normed, forget_weight, preferred_element_type=jnp.float32) + forget_bias
    )
    position = jnp.arange(cache_len, dtype=jnp.int32)
    live = position[None, :] < lengths[:, None]
    at_last = (position[None, :] == lengths[:, None] - 1)[:, None, :]
    last_cum = jnp.sum(jnp.where(at_last, cache_cum, 0.0), axis=-1)
    gate_bias = last_cum[:, :, None] - cache_cum + new_log[:, :, None]
    score_scale = head_size ** (-0.5)
    past = (
        jnp.einsum("skgd,spkd->skgp", query, cache_keys, preferred_element_type=jnp.float32)
        * score_scale
    )
    past = past + gate_bias[:, :, None, :]
    past = jnp.where(live[:, None, None, :], past, -jnp.inf)
    own = (
        jnp.sum(query.astype(jnp.float32) * new_key.astype(jnp.float32)[:, :, None, :], axis=-1)
        * score_scale
    )
    past_exp = jnp.exp(past)
    own_exp = jnp.exp(own)
    denominator = jnp.sum(past_exp, axis=-1) + own_exp
    past_prob = (past_exp / denominator[..., None]).astype(jnp.bfloat16)
    own_prob = (own_exp / denominator).astype(jnp.bfloat16)
    mixed = jnp.einsum(
        "skgp,spkd->skgd", past_prob, cache_values, preferred_element_type=jnp.float32
    )
    mixed = (
        mixed
        + own_prob.astype(jnp.float32)[..., None] * new_value.astype(jnp.float32)[:, :, None, :]
    )
    heads_out = mixed.astype(jnp.bfloat16).reshape(seq_rows, -1)
    partial_value = jnp.dot(heads_out, out_weight, preferred_element_type=jnp.float32)
    attended = copy_for_each(partial_value.astype(jnp.bfloat16), "tp")
    attended = jnp.sum(attended.astype(jnp.float32), axis=0)
    residual = tokens.astype(jnp.float32) + attended
    ffn_in = rms_norm(residual, ffn_gain).astype(jnp.bfloat16)

    member = lax.axis_index("tp")
    width = ffn_in.shape[1]
    hidden_local = expert_gate.shape[2]
    units = shared_gate.shape[1]
    pack = jnp.concatenate(
        [
            expert_gate[0],
            expert_up[0],
            lane_blocks(expert_down[0]),
            lane_blocks(shared_down),
        ],
        axis=0,
    )
    packs = copy_for_each(pack, "tp")
    packs = packs.reshape(-1, *pack.shape)
    gate_all = packs[:, :width]
    up_all = packs[:, width : 2 * width]
    down_end = 2 * width + hidden_local * width // LANES
    down_all = wide_rows(packs[:, 2 * width : down_end], hidden_local)
    shared_cols = wide_rows(packs[:, down_end:], units)
    shared_down_all = jnp.moveaxis(shared_cols, 0, 1).reshape(units, width)
    front = jnp.concatenate([shared_gate, shared_up, mix_weight[:, None]], axis=1)

    norm_weights = route_weights / jnp.sum(route_weights, axis=1, keepdims=True)
    high = norm_weights.astype(jnp.bfloat16)
    low = (norm_weights - high.astype(jnp.float32)).astype(jnp.bfloat16)
    notes = jnp.concatenate([routes.astype(jnp.bfloat16), high, low], axis=1)
    notes = jnp.pad(notes, ((0, 0), (0, LANES - notes.shape[1])))
    outgoing = pair_of(jnp.concatenate([ffn_in, notes], axis=1), member)
    peers = lax.axis_size(EP)
    outgoing = jnp.broadcast_to(outgoing[None], (peers // 2, *outgoing.shape))
    own_rows = lax.all_to_all(outgoing.reshape(peers, -1), EP, 0, 0, tiled=True)
    expert = lax.axis_index(EP).astype(jnp.float32)

    def share(rows):
        values = rows[:, :width]
        marks = rows[:, width:].astype(jnp.float32)
        picked = marks[:, 0:2] == expert
        weight = jnp.sum(jnp.where(picked, marks[:, 2:4] + marks[:, 4:6], 0.0), axis=1)
        pre = jnp.dot(values, front, preferred_element_type=jnp.float32)
        mix_gate = jax.nn.sigmoid(pre[:, 2 * units])
        shared = (jax.nn.silu(pre[:, :units]) * pre[:, units : 2 * units]).astype(jnp.bfloat16)
        dense = jnp.dot(shared, shared_down_all, preferred_element_type=jnp.float32)
        gate = jnp.einsum("nd,tdf->tnf", values, gate_all, preferred_element_type=jnp.float32)
        up = jnp.einsum("nd,tdf->tnf", values, up_all, preferred_element_type=jnp.float32)
        hidden = (jax.nn.silu(gate) * up).astype(jnp.bfloat16)
        routed = jnp.einsum("tnf,tfd->nd", hidden, down_all, preferred_element_type=jnp.float32)
        return mix_gate[:, None] * dense + weight[:, None] * routed

    pair_rows = swap(own_rows)
    pair_share = swap(share(pair_rows).astype(jnp.bfloat16))
    total = share(own_rows) + pair_share.astype(jnp.float32)
    total = total.astype(jnp.bfloat16).reshape(peers * lax.axis_size("tp"), -1)
    returned = lax.all_to_all(total, (*EP, "tp"), 0, 0, tiled=True)
    returned = returned.reshape(peers // 2, seq_rows, -1).astype(jnp.float32)
    slice_width = returned.shape[2]
    residual_slice = lax.dynamic_slice_in_dim(residual, member * slice_width, slice_width, 1)
    return (residual_slice + jnp.sum(returned, axis=0)).astype(jnp.bfloat16)


def solution(mesh):
    finer = Mesh(mesh.devices.reshape(16, 4, 2, mesh.shape["tp"]), ("ep_0", "ep_1", "ep_2", "tp"))
    placed = (
        P(EP, None),
        P(EP),
        P(EP, None, "tp", None),
        P(EP, None, "tp", None),
        P(EP, "tp", None),
        P(),
        P(None, "tp"),
        P(None, "tp"),
        P(None, "tp"),
        P(None, "tp"),
        P("tp"),
        P(),
        P(),
        P("tp", None),
        P(),
        P(),
        P(None, EP),
        P(None, EP),
        P(EP, "tp"),
        P(EP, None),
        P(EP, None),
        P(EP, None, "tp"),
        P(EP, None, "tp"),
        P(EP, "tp", None),
    )
    return jax.shard_map(
        per_device, mesh=finer, in_specs=placed, out_specs=P(EP, "tp"), check_vma=False
    )
```

time: 321 us -> 176 us (0.55)
  blocking collectives: 91.3 us -> 0 us
  waiting for transfers between devices: 143 us -> 83.3 us
  starting transfers between devices: 21.2 us -> 47.7 us
  between operations: 14 us -> 1.2 us
  local copies, waits for them, and re-layouts: 20.5 us -> 10.4 us
  other arithmetic: 7.9 us -> 13.6 us
    all_gather x1 -> x0, blocking collectives: 91.3 us -> none  [per_device(): lax.all_gather(routes, EP, axis=0, tiled=True)]
    reduce_scatter x3 -> x0, waiting for transfers between devices: 69.8 us -> none  [sum_in_order(): tiles = lax.psum_scatter(tiles, axes[k], scatter_dimension=0, tiled=True)]
    all_gather x1 -> x0, waiting for transfers between devices: 53.6 us -> none  [per_device(): lax.all_gather(ffn_in, EP, axis=0, tiled=True)]
    all_to_all x2, waiting for transfers between devices: 13.9 us -> 47.6 us  [the longest x1 25 us: per_device(): returned = lax.all_to_all(total, (*EP, 'tp'), 0, 0, tiled=True)]
    all_to_all x1 -> x2, waiting for transfers between devices: 4.46 us -> 35 us  [copy_for_each(): lax.all_to_all(jnp.broadcast_to(shard[None], (peers, *shard.shape)), axis...]
    all_to_all x2, starting transfers between devices: 16.1 us -> 31 us  [the longest x1 21 us: per_device(): own_rows = lax.all_to_all(outgoing.reshape(peers, -1), EP, 0, 0, tiled=True)]
    reshape x3 -> x5, local copies, waits for them, and re-layouts: 8.51 us -> 1.21 us  [the longest x1 0.68 us: wide_rows(): blocks = blocks.reshape(peers, -1, rows, LANES)]
    ppermute x0 -> x2, starting transfers between devices: none -> 6.9 us  [swap(): return lax.ppermute(shard, PAIR, [(0, 1), (1, 0)])]
  transfers between devices with their start and end apart: 7 -> 6, of which waited for: 5 -> 5; matrix products, arithmetic and copies ran while one was open for 9% -> 4% of each run, Pallas kernels for 0% -> 0%
where the time goes in v1:
time: 176 us; the launch traced here: 175 us
  waiting for transfers between devices  83.3 us (47%)
  starting transfers between devices  47.7 us (27%)
  matrix products  18.5 us (11%)
  other arithmetic  13.6 us (8%)
  local copies, waits for them, and re-layouts  10.4 us (6%)
    all_to_all x2, waiting for transfers between devices, copy_for_each(): lax.all_to_all(jnp.broadcast_to(shard[None], (peers, *shard.shape)), axis...  35 us
    all_to_all x1, waiting for transfers between devices, per_device(): returned = lax.all_to_all(total, (*EP, 'tp'), 0, 0, tiled=True)  25 us
    all_to_all x1, waiting for transfers between devices, per_device(): own_rows = lax.all_to_all(outgoing.reshape(peers, -1), EP, 0, 0, tiled=True)  22.6 us
    all_to_all x1, starting transfers between devices, per_device(): own_rows = lax.all_to_all(outgoing.reshape(peers, -1), EP, 0, 0, tiled=True)  21 us
    all_to_all x1, starting transfers between devices, per_device(): returned = lax.all_to_all(total, (*EP, 'tp'), 0, 0, tiled=True)  10.1 us
    all_to_all x2, starting transfers between devices, copy_for_each(): lax.all_to_all(jnp.broadcast_to(shard[None], (peers, *shard.shape)), axis...  9.79 us
    ppermute x2, starting transfers between devices, swap(): return lax.ppermute(shard, PAIR, [(0, 1), (1, 0)])  6.9 us
    dot_general x2, matrix products, share(): jnp.einsum('tnf,tfd->nd', hidden, down_all, preferred_element_type=jnp.fl...  4.42 us
  transfers between devices with their start and end apart: 6, of which 5 were waited for; matrix products, arithmetic and copies ran while one was open for 4% of the time, Pallas kernels for 0%

profile of v1, /device:TPU:1, one launch (start us, length us, event | category | flops | bytes accessed | tf_op | source)
XLA Modules:
  0.0 174.7 jit_solution(75435213628078322)
XLA Ops:
  0.1 0.8 broadcast_add_fusion
  0.9 0.7 iota_compare_fusion.1
  2.3 0.7 convert_element_type.152
  2.9 0.8 fusion.60
  3.8 0.9 fusion.67
  4.7 0.9 fusion.85
  5.7 0.8 subtract_add_fusion
  6.5 1.3 fusion.70
  7.8 0.7 convert_element_type.154
  8.5 0.1 copy.106
  8.6 1.3 multiply_reduce_fusion.2
  9.9 0.7 convert_element_type.158
  10.5 0.1 fusion.83
  10.6 0.2 multiply_reduce_fusion.1
  10.8 0.1 copy.108
  10.9 1.2 fusion.12
  12.0 0.5 fusion.104
  12.6 1.5 fusion.11
  14.1 0.0 copy-done.1
  14.1 0.2 convolution_convert_fusion
  14.3 0.6 broadcast_in_dim.33
  14.9 5.0 %all-to-all-start = ((bf16[4,8,1024]{2,1,0:T(8,128)(2,1)}), bf16[4,8,1024]{2,1,0:T(8,128)(2,1)S(1)}, u32[]{:S(2)}, u32[]{:S(2)}) async-start(bf16[4,8,1024]{2,1,0:T(8,128)(2,1)} %broadcast_in_dim.33), calls=%async_computation | async-start | bytes 131072 | tf_op jit(solution)/shard_map/all_to_all | solution.py:17
  20.2 0.1 copy.128
  20.3 4.1 %all-to-all-done = bf16[4,8,1024]{2,1,0:T(8,128)(2,1)S(1)} async-done(((bf16[4,8,1024]{2,1,0:T(8,128)(2,1)}), bf16[4,8,1024]{2,1,0:T(8,128)(2,1)S(1)}, u32[]{:S(2)}, u32[]{:S(2)}) %all-to-all-start) | async-done | bytes 65568 | tf_op jit(solution)/shard_map/all_to_all | solution.py:17
  24.4 0.1 multiply_reduce_fusion
  24.6 0.1 multiply_convert_fusion.1
  24.7 0.2 broadcast_in_dim.35
  24.9 0.3 all_to_all.27
  25.2 0.5 broadcast.214
  25.7 2.4 %reduce.7 = bf16[128,1152]{1,0:T(8,128)(2,1)S(1)} reduce(bf16[128,1,1152]{2,1,0:T(2,128)(2,1)S(1)} %all_to_all.27, bf16[]{:T(256)} %broadcast.214), dimensions={1}, to_apply=%all_to_all.27.reduce_sub_computation | reduce | bytes 589826 | tf_op jit(solution)/shard_map/all_to_all | solution.py:163
  28.1 1.0 reshape.303
  29.1 21.0 %all-to-all-start.1 = ((bf16[128,2,576]{2,1,0:T(2,128)(2,1)}), bf16[128,2,576]{2,1,0:T(2,128)(2,1)S(1)}, u32[]{:S(2)}, u32[]{:S(2)}) async-start(bf16[128,2,576]{2,1,0:T(2,128)(2,1)} %reshape.303), calls=%async_computation.1 | async-start | bytes 655360 | tf_op jit(solution)/shard_map/all_to_all | solution.py:163
  50.2 22.6 %all-to-all-done.1 = bf16[128,2,576]{2,1,0:T(2,128)(2,1)S(1)} async-done(((bf16[128,2,576]{2,1,0:T(2,128)(2,1)}), bf16[128,2,576]{2,1,0:T(2,128)(2,1)S(1)}, u32[]{:S(2)}, u32[]{:S(2)}) %all-to-all-start.1) | async-done | bytes 294944 | tf_op jit(solution)/shard_map/all_to_all | solution.py:163
  72.8 2.1 %broadcast_in_dim.37 = bf16[4,3136,128]{2,1,0:T(8,128)(2,1)} broadcast(bf16[3136,128]{1,0:T(8,128)(2,1)S(1)} %constant_dynamic-update-slice_fusion.3), dimensions={1,2} | broadcast | bytes 4014080 | tf_op jit(solution)/shard_map/broadcast_in_dim | solution.py:18
  74.9 4.8 %all-to-all-start.2 = ((bf16[4,3136,128]{2,1,0:T(8,128)(2,1)}), bf16[4,3136,128]{2,1,0:T(8,128)(2,1)}, u32[]{:S(2)}, u32[]{:S(2)}) async-start(bf16[4,3136,128]{2,1,0:T(8,128)(2,1)} %broadcast_in_dim.37), calls=%async_computation.2 | async-start | bytes 6422528 | tf_op jit(solution)/shard_map/all_to_all | solution.py:17
  79.8 0.5 reshape.304
  80.4 2.9 %collective-permute-start = (bf16[128,1152]{1,0:T(8,128)(2,1)S(1)}, bf16[128,1152]{1,0:T(8,128)(2,1)S(1)}, u32[]{:S(2)}, u32[]{:S(2)}) collective-permute-start(bf16[128,1152]{1,0:T(8,128)(2,1)S(1)} %bitcast.139), channel_id=1, source_target_pairs={{0,4},{4,0},{1,5},{5,1},{2,6},{6,2},{3,7},{7,3},{8,12},{12,8},{9,1... | collective-permute-start | bytes 884744 | tf_op jit(solution)/shard_map/ppermute | solution.py:23
  83.3 0.2 fusion.51
  83.6 0.2 fusion.58
  83.7 0.8 collective-permute-done
  84.5 0.2 fusion.56
  84.7 0.8 fusion.38
  85.5 0.7 fusion.89
  86.2 30.9 %all-to-all-done.2 = bf16[4,3136,128]{2,1,0:T(8,128)(2,1)} async-done(((bf16[4,3136,128]{2,1,0:T(8,128)(2,1)}), bf16[4,3136,128]{2,1,0:T(8,128)(2,1)}, u32[]{:S(2)}, u32[]{:S(2)}) %all-to-all-start.2) | async-done | bytes 3211296 | tf_op jit(solution)/shard_map/all_to_all | solution.py:17
  117.1 0.8 slice.84
  118.0 1.3 slice.91
  119.3 0.7 copy.150
  120.0 0.5 reshape.294
  120.5 1.0 convolution_multiply_fusion
  121.5 1.7 convolution_bitcast_fusion.3
  123.3 2.2 %fusion.4 = bf16[128,1024]{1,0:T(8,128)(2,1)S(1)} fusion(f32[128,1024]{1,0:T(8,128)S(1)} %convolution_multiply_fusion, bf16[4,128,1024]{2,1,0:T(8,128)(2,1)S(1)} %reshape.294, f32[128]{0:T(128)S(1)} %fusion.56, f32[4,128,128]{1,2,0:T(8,128)S(1)} %convolution_bitcast_fusion.3, bf16[128,1152]{1,0:T(8,128)(2,1)} %copy-done.2, ...), kind=kOutput, calls=%fused_computation.8 | convolution fusion | flops 269221888 | bytes 3408384 | tf_op jit(solution)/shard_map/tnf,tfd->nd/dot_general | solution.py:178
  125.5 4.0 %collective-permute-start.1 = (bf16[128,1024]{1,0:T(8,128)(2,1)S(1)}, bf16[128,1024]{1,0:T(8,128)(2,1)S(1)}, u32[]{:S(2)}, u32[]{:S(2)}) collective-permute-start(bf16[128,1024]{1,0:T(8,128)(2,1)S(1)} %fusion.4), channel_id=1, source_target_pairs={{0,4},{4,0},{1,5},{5,1},{2,6},{6,2},{3,7},{7,3},{8,12},{12,8},{9,1... | collective-permute-start | bytes 786440 | tf_op jit(solution)/shard_map/ppermute | solution.py:23
  129.5 1.0 convolution_multiply_fusion.1
  130.5 2.4 %convolution_bitcast_fusion.5 = f32[4,128,128]{1,2,0:T(8,128)} fusion(bf16[4,3136,128]{2,1,0:T(8,128)(2,1)} %all-to-all-done.2, bf16[128,1152]{1,0:T(8,128)(2,1)S(1)} %bitcast.142), kind=kOutput, calls=%fused_computation.12 | convolution fusion | flops 134217728 | bytes 1572864 | tf_op jit(solution)/shard_map/nd,tdf->tnf/dot_general | solution.py:175
  132.9 2.2 %add_convert_fusion = bf16[128,1024]{1,0:T(8,128)(2,1)S(1)} fusion(bf16[128,1024]{1,0:T(8,128)(2,1)S(1)} %collective-permute-done.1, f32[128,1024]{1,0:T(8,128)S(1)} %convolution_multiply_fusion.1, bf16[4,128,1024]{2,1,0:T(8,128)(2,1)S(1)} %reshape.294, bf16[4,3136,128]{2,1,0:T(8,128)(2,1)} %all-to-all-done.2, ...), kind=kOutput, calls=%fused_computation.36 | convolution fusion | flops 269484032 | bytes 3670528 | tf_op jit(solution)/shard_map/tnf,tfd->nd/dot_general | solution.py:178
  135.1 0.2 all_to_all.28
  135.3 2.2 %reduce.8 = bf16[512,256]{1,0:T(8,128)(2,1)S(1)} reduce(bf16[512,1,256]{2,1,0:T(2,128)(2,1)S(1)} %all_to_all.28, bf16[]{:T(256)} %broadcast.214), dimensions={1}, to_apply=%all_to_all.28.reduce_sub_computation | reduce | bytes 524290 | tf_op jit(solution)/shard_map/all_to_all | solution.py:185
  137.6 0.8 reshape.305
  138.3 10.1 %all-to-all-start.3 = ((bf16[512,2,128]{2,1,0:T(2,128)(2,1)}), bf16[512,2,128]{2,1,0:T(2,128)(2,1)S(1)}, u32[]{:S(2)}, u32[]{:S(2)}) async-start(bf16[512,2,128]{2,1,0:T(2,128)(2,1)} %reshape.305), calls=%async_computation.3 | async-start | bytes 524288 | tf_op jit(solution)/shard_map/all_to_all | solution.py:185
  148.4 25.0 %all-to-all-done.3 = bf16[512,2,128]{2,1,0:T(2,128)(2,1)S(1)} async-done(((bf16[512,2,128]{2,1,0:T(2,128)(2,1)}), bf16[512,2,128]{2,1,0:T(2,128)(2,1)S(1)}, u32[]{:S(2)}, u32[]{:S(2)}) %all-to-all-start.3) | async-done | bytes 262176 | tf_op jit(solution)/shard_map/all_to_all | solution.py:185
  173.4 0.1 reshape.306
  173.5 0.5 convert_element_type.188
  174.0 0.1 bitcast_reduce_fusion
  174.1 0.6 add_convert_fusion.1
  (67 shorter events, 0.5 us)
Async XLA Ops:
  0.0 12.0 %copy-start = (bf16[8,512,1,128]{3,1,2,0:T(8,128)(2,1)S(1)}, bf16[8,512,1,128]{3,1,2,0:T(8,128)(2,1)}, u32[]{:S(2)}) copy-start(bf16[8,512,1,128]{3,1,2,0:T(8,128)(2,1)} %param.26) | copy-start | bytes 3145732
  0.0 24.4 %copy-start.6 = (bf16[8,1024]{1,0:T(8,128)(2,1)S(1)}, bf16[8,1024]{1,0:T(8,128)(2,1)}, u32[]{:S(2)}) copy-start(bf16[8,1024]{1,0:T(8,128)(2,1)} %param.24) | copy-start | bytes 49156
  0.0 14.1 %copy-start.1 = (bf16[256,1024]{1,0:T(8,128)(2,1)S(1)}, bf16[256,1024]{1,0:T(8,128)(2,1)}, u32[]{:S(2)}) copy-start(bf16[256,1024]{1,0:T(8,128)(2,1)} %param.37) | copy-start | bytes 1572868
  0.0 19.9 %copy-start.4 = (bf16[1,1024,128]{2,1,0:T(8,128)(2,1)S(1)}, bf16[1,1024,128]{2,1,0:T(8,128)(2,1)}, u32[]{:S(2)}) copy-start(bf16[1,1024,128]{2,1,0:T(8,128)(2,1)} %param.45) | copy-start | bytes 786436
  0.0 19.9 %copy-start.5 = (bf16[1,1024,128]{2,1,0:T(8,128)(2,1)S(1)}, bf16[1,1024,128]{2,1,0:T(8,128)(2,1)}, u32[]{:S(2)}) copy-start(bf16[1,1024,128]{2,1,0:T(8,128)(2,1)} %param.46) | copy-start | bytes 786436
  0.0 20.0 %copy-start.3 = (bf16[1,128,1024]{2,1,0:T(8,128)(2,1)S(1)}, bf16[1,128,1024]{2,1,0:T(8,128)(2,1)}, u32[]{:S(2)}) copy-start(bf16[1,128,1024]{2,1,0:T(8,128)(2,1)} %param.47) | copy-start | bytes 786436
  0.0 20.1 %copy-start.11 = (f32[8,2]{0,1:T(2,128)S(1)}, f32[8,2]{0,1:T(2,128)}, u32[]{:S(2)}) copy-start(f32[8,2]{0,1:T(2,128)} %param.44) | copy-start | bytes 196
  0.1 20.1 %copy-start.14 = (s32[8,2]{0,1:T(2,128)S(1)}, s32[8,2]{0,1:T(2,128)}, u32[]{:S(2)}) copy-start(s32[8,2]{0,1:T(2,128)} %param.43) | copy-start | bytes 196
  0.1 20.2 %copy-start.12 = (bf16[1024]{0:T(1024)(128)(2,1)S(1)}, bf16[1024]{0:T(1024)(128)(2,1)}, u32[]{:S(2)}) copy-start(bf16[1024]{0:T(1024)(128)(2,1)} %param.38) | copy-start | bytes 6148
  14.1 36.1 %copy-start.10 = (bf16[32,256]{1,0:T(8,128)(2,1)S(1)}, bf16[32,256]{1,0:T(8,128)(2,1)}, u32[]{:S(2)}) copy-start(bf16[32,256]{1,0:T(8,128)(2,1)} %param.42) | copy-start | bytes 49156
  14.9 9.5 %all-to-all-start = ((bf16[4,8,1024]{2,1,0:T(8,128)(2,1)}), bf16[4,8,1024]{2,1,0:T(8,128)(2,1)S(1)}, u32[]{:S(2)}, u32[]{:S(2)}) async-start(bf16[4,8,1024]{2,1,0:T(8,128)(2,1)} %broadcast_in_dim.33), calls=%async_computation | async-start | bytes 131072 | tf_op jit(solution)/shard_map/all_to_all | solution.py:17
  29.1 43.7 %all-to-all-start.1 = ((bf16[128,2,576]{2,1,0:T(2,128)(2,1)}), bf16[128,2,576]{2,1,0:T(2,128)(2,1)S(1)}, u32[]{:S(2)}, u32[]{:S(2)}) async-start(bf16[128,2,576]{2,1,0:T(2,128)(2,1)} %reshape.303), calls=%async_computation.1 | async-start | bytes 655360 | tf_op jit(solution)/shard_map/all_to_all | solution.py:163
  74.9 4.8 %copy-start.8 = (bf16[1024,32]{0,1:T(8,128)(2,1)S(1)}, bf16[1024,32]{0,1:T(8,128)(2,1)}, u32[]{:S(2)}) copy-start(bf16[1024,32]{0,1:T(8,128)(2,1)} %param.40) | copy-start | bytes 196612
  74.9 4.8 %copy-start.9 = (bf16[1024,32]{0,1:T(8,128)(2,1)S(1)}, bf16[1024,32]{0,1:T(8,128)(2,1)}, u32[]{:S(2)}) copy-start(bf16[1024,32]{0,1:T(8,128)(2,1)} %param.41) | copy-start | bytes 196612
  74.9 4.9 %copy-start.13 = (bf16[1024]{0:T(1024)(128)(2,1)S(1)}, bf16[1024]{0:T(1024)(128)(2,1)}, u32[]{:S(2)}) copy-start(bf16[1024]{0:T(1024)(128)(2,1)} %param.39) | copy-start | bytes 6148
  74.9 42.2 %all-to-all-start.2 = ((bf16[4,3136,128]{2,1,0:T(8,128)(2,1)}), bf16[4,3136,128]{2,1,0:T(8,128)(2,1)}, u32[]{:S(2)}, u32[]{:S(2)}) async-start(bf16[4,3136,128]{2,1,0:T(8,128)(2,1)} %broadcast_in_dim.37), calls=%async_computation.2 | async-start | bytes 6422528 | tf_op jit(solution)/shard_map/all_to_all | solution.py:17
  80.4 4.1 %collective-permute-start = (bf16[128,1152]{1,0:T(8,128)(2,1)S(1)}, bf16[128,1152]{1,0:T(8,128)(2,1)S(1)}, u32[]{:S(2)}, u32[]{:S(2)}) collective-permute-start(bf16[128,1152]{1,0:T(8,128)(2,1)S(1)} %bitcast.139), channel_id=1, source_target_pairs={{0,4},{4,0},{1,5},{5,1},{2,6},{6,2},{3,7},{7,3},{8,12},{12,8},{9,1... | collective-permute-start | bytes 884744 | tf_op jit(solution)/shard_map/ppermute | solution.py:23
  83.5 34.5 %copy-start.7 = (f32[128,65]{0,1:T(8,128)}, f32[128,65]{0,1:T(8,128)S(1)}, u32[]{:S(2)}) copy-start(f32[128,65]{0,1:T(8,128)S(1)} %fusion.51) | copy-start | bytes 99844
  84.5 1.0 copy-start.2
  125.5 7.4 %collective-permute-start.1 = (bf16[128,1024]{1,0:T(8,128)(2,1)S(1)}, bf16[128,1024]{1,0:T(8,128)(2,1)S(1)}, u32[]{:S(2)}, u32[]{:S(2)}) collective-permute-start(bf16[128,1024]{1,0:T(8,128)(2,1)S(1)} %fusion.4), channel_id=1, source_target_pairs={{0,4},{4,0},{1,5},{5,1},{2,6},{6,2},{3,7},{7,3},{8,12},{12,8},{9,1... | collective-permute-start | bytes 786440 | tf_op jit(solution)/shard_map/ppermute | solution.py:23
  138.3 35.0 %all-to-all-start.3 = ((bf16[512,2,128]{2,1,0:T(2,128)(2,1)}), bf16[512,2,128]{2,1,0:T(2,128)(2,1)S(1)}, u32[]{:S(2)}, u32[]{:S(2)}) async-start(bf16[512,2,128]{2,1,0:T(2,128)(2,1)} %reshape.305), calls=%async_computation.3 | async-start | bytes 524288 | tf_op jit(solution)/shard_map/all_to_all | solution.py:185

commit v2 on v1

v2 whole, which is shorter than its diff:
```python
import jax
import jax.numpy as jnp
from jax import lax
from jax.experimental import pallas as pl
from jax.experimental.pallas import tpu as pltpu
from jax.sharding import Mesh
from jax.sharding import PartitionSpec as P

EP = ("ep_0", "ep_1", "ep_2")
PAIR = "ep_2"
LANES = 128
NOTE_ROWS = 2

epsilon = 1e-06

VMEM = pl.BlockSpec(memory_space=pltpu.VMEM)
SMEM = pl.BlockSpec(memory_space=pltpu.SMEM)
ANY = pl.BlockSpec(memory_space=pl.ANY)


def swap(shard):
    return lax.ppermute(shard, PAIR, [(0, 1), (1, 0)])


def scaled(values, gain):
    mean = jnp.mean(values * values, axis=-1, keepdims=True)
    return values * lax.rsqrt(mean + epsilon) * gain


def silu(values):
    return values / (1.0 + jnp.exp(-values))


def wide_dot(left, right):
    return jnp.dot(left, right, preferred_element_type=jnp.float32)


def attend_kernel(
    lengths,
    forget_bias,
    tokens,
    keys,
    values,
    cum,
    norm_gain,
    query_weight,
    key_weight,
    value_weight,
    forget_weight,
    query_gain,
    key_gain,
    out_weight,
    expert_gate,
    expert_up,
    expert_down,
    shared_down,
    partial,
    packed,
    sems,
):
    width = expert_gate.shape[0]
    copies = []

    def send(source, first):
        target = packed.at[pl.ds(first, source.shape[0]), :]
        copy = pltpu.make_async_copy(source, target, sems.at[len(copies)])
        copy.start()
        copies.append(copy)
        return first + source.shape[0]

    row = send(expert_gate, 0)
    row = send(expert_up, row)
    for block in range(width // LANES):
        row = send(expert_down.at[:, pl.ds(block * LANES, LANES)], row)
    for block in range(shared_down.shape[1] // LANES):
        row = send(shared_down.at[:, pl.ds(block * LANES, LANES)], row)

    seqs, cache_len, head = keys.shape
    groups = query_weight.shape[1] // head
    normed = scaled(tokens[...].astype(jnp.float32), norm_gain[...].astype(jnp.float32))
    normed = normed.astype(jnp.bfloat16)
    wide = wide_dot(normed, query_weight[...])
    gain = query_gain[...].astype(jnp.float32)
    query = [scaled(wide[:, g * head : (g + 1) * head], gain) for g in range(groups)]
    query = jnp.concatenate(query, axis=0).astype(jnp.bfloat16)
    new_key = scaled(wide_dot(normed, key_weight[...]), key_gain[...].astype(jnp.float32))
    new_key = new_key.astype(jnp.bfloat16).astype(jnp.float32)
    new_value = wide_dot(normed, value_weight[...]).astype(jnp.bfloat16).astype(jnp.float32)
    products = normed.astype(jnp.float32) * forget_weight[...].astype(jnp.float32)
    forget = jnp.sum(products, axis=-1, keepdims=True) + forget_bias[0]
    new_log = jnp.minimum(forget, 0.0) - jnp.log1p(jnp.exp(-jnp.abs(forget)))

    rows = groups * seqs
    owner = lax.broadcasted_iota(jnp.int32, (rows, cache_len), 0) % seqs
    position = lax.broadcasted_iota(jnp.int32, (rows, cache_len), 1)
    scores = jnp.zeros((rows, cache_len), jnp.float32)
    decay = jnp.zeros((rows, cache_len), jnp.float32)
    length = jnp.zeros((rows, cache_len), jnp.int32)
    for b in range(seqs):
        mine = owner == b
        one = lax.dot_general(
            query, keys[b], (((1,), (1,)), ((), ())), preferred_element_type=jnp.float32
        )
        scores = jnp.where(mine, one, scores)
        decay = jnp.where(mine, cum[b], decay)
        length = jnp.where(mine, lengths[b], length)
    last = jnp.where(position == length - 1, decay, 0.0)
    last = jnp.sum(last, axis=-1, keepdims=True)
    bias = last - decay + jnp.concatenate([new_log] * groups, axis=0)
    score_scale = head ** (-0.5)
    past = jnp.where(position < length, scores * score_scale + bias, -jnp.inf)
    own = query.astype(jnp.float32) * jnp.concatenate([new_key] * groups, axis=0)
    own = jnp.sum(own, axis=-1, keepdims=True) * score_scale
    past_exp = jnp.exp(past)
    own_exp = jnp.exp(own)
    denominator = jnp.sum(past_exp, axis=-1, keepdims=True) + own_exp
    past_prob = (past_exp / denominator).astype(jnp.bfloat16)
    own_prob = (own_exp / denominator).astype(jnp.bfloat16).astype(jnp.float32)
    head_owner = owner[:, :head]
    mixed = jnp.zeros((rows, head), jnp.float32)
    for b in range(seqs):
        mixed = jnp.where(head_owner == b, wide_dot(past_prob, values[b]), mixed)
    mixed = mixed + own_prob * jnp.concatenate([new_value] * groups, axis=0)
    heads_out = [mixed[g * seqs : (g + 1) * seqs] for g in range(groups)]
    heads_out = jnp.concatenate(heads_out, axis=1).astype(jnp.bfloat16)
    product = wide_dot(heads_out, out_weight[...]).astype(jnp.bfloat16)
    for peer in range(partial.shape[0]):
        partial[peer] = product
    for copy in copies:
        copy.wait()


def rows_kernel(member, partial, tokens, ffn_gain, notes, residual, outgoing):
    attended = jnp.sum(partial[...].astype(jnp.float32), axis=0)
    full = tokens[...].astype(jnp.float32) + attended
    residual[...] = full
    normed = scaled(full, ffn_gain[...].astype(jnp.float32))
    normed = normed.astype(jnp.bfloat16).astype(jnp.float32)
    marks = notes[...]
    members = full.shape[0] // 2
    here = lax.broadcasted_iota(jnp.int32, (members, 1), 0) == member[0]
    pieces = []
    for half in range(2):
        rows = slice(half * members, (half + 1) * members)
        row = jnp.sum(jnp.where(here, normed[rows], 0.0), axis=0, keepdims=True)
        mark = jnp.sum(jnp.where(here, marks[rows], 0.0), axis=0, keepdims=True)
        pieces += [row[:, k : k + LANES] for k in range(0, full.shape[1], LANES)]
        pieces += [mark, jnp.zeros_like(mark)]
    pattern = jnp.concatenate(pieces * 4, axis=0).astype(jnp.bfloat16)
    step = pattern.shape[0]
    for i in range(outgoing.shape[0] // step):
        outgoing[i * step : (i + 1) * step, :] = pattern


def share_kernel(place, rows, front, pair_front, *refs):
    packs, (out, wide, narrow, columns) = refs[:-4], refs[-4:]
    members = len(packs) // 2
    width = front.shape[1]
    count = narrow.shape[0]
    blocks = width // LANES
    stride = blocks + NOTE_ROWS
    wide[...] = rows[...].astype(jnp.float32)
    for k in range(blocks):
        piece = wide[pl.ds(k, count, stride=stride), :]
        narrow[:, k * LANES : (k + 1) * LANES] = piece.astype(jnp.bfloat16)
    marks = wide[pl.ds(blocks, count, stride=stride), :]
    values = narrow[...]
    down_start = 2 * width
    shared_start = down_start + blocks * LANES
    per_member = blocks // members
    units = (packs[0].shape[0] - shared_start) // per_member

    fronts = [
        lax.dot_general(
            values, each[...], (((1,), (1,)), ((), ())), preferred_element_type=jnp.float32
        )
        for each in (front, pair_front)
    ]
    mix_gate = 1.0 / (1.0 + jnp.exp(-fronts[0][:, 2 * units : 2 * units + 1]))
    shared = [silu(pre[:, :units]) * pre[:, units : 2 * units] for pre in fronts]
    shared = [each.astype(jnp.bfloat16) for each in shared]
    for s in range(members):
        for k in range(per_member):
            rows_of = pl.ds(shared_start + k * units, units)
            dense = wide_dot(shared[0], packs[s][rows_of, :])
            dense = dense + wide_dot(shared[1], packs[members + s][rows_of, :])
            columns[place[2 + s] + k] = mix_gate * dense

    hidden = []
    for side in range(2):
        me = place[side].astype(jnp.float32)
        weight = jnp.zeros((count, 1), jnp.float32)
        for j in range(2):
            chosen = marks[:, j : j + 1] == me
            norm_weight = marks[:, 2 + j : 3 + j] + marks[:, 4 + j : 5 + j]
            weight = weight + jnp.where(chosen, norm_weight, 0.0)
        for s in range(members):
            pack = packs[side * members + s]
            gate = wide_dot(values, pack[:width, :])
            up = wide_dot(values, pack[width : 2 * width, :])
            hidden.append((weight, (silu(gate) * up).astype(jnp.bfloat16)))
    for k in range(blocks):
        total = columns[k]
        for side in range(2):
            first = down_start + k * LANES
            routed = jnp.zeros((count, LANES), jnp.float32)
            for s in range(members):
                weight, each = hidden[side * members + s]
                pack = packs[side * members + s]
                routed = routed + wide_dot(each, pack[first : first + LANES, :])
            total = total + weight * routed
        wide[pl.ds(k, count, stride=blocks), :] = total
    out[...] = wide[: count * blocks, :].astype(jnp.bfloat16)


def per_device(
    tokens,
    lengths,
    cache_keys,
    cache_values,
    cache_cum,
    norm_gain,
    query_weight,
    key_weight,
    value_weight,
    forget_weight,
    forget_bias,
    query_gain,
    key_gain,
    out_weight,
    ffn_gain,
    mix_weight,
    shared_gate,
    shared_up,
    shared_down,
    routes,
    route_weights,
    expert_gate,
    expert_up,
    expert_down,
):
    seqs, width = tokens.shape
    cache_len, head = cache_keys.shape[1], cache_keys.shape[3]
    peers = lax.axis_size(EP)
    members = lax.axis_size("tp")
    member = lax.axis_index("tp")
    blocks = width // LANES
    units = shared_gate.shape[1]
    hidden = expert_gate.shape[2]
    pack_rows = 2 * width + hidden * blocks + units * shared_down.shape[1] // LANES
    copies = 2 + blocks + shared_down.shape[1] // LANES

    partial, packed = pl.pallas_call(
        attend_kernel,
        in_specs=[SMEM, SMEM] + [VMEM] * 12 + [ANY] * 4,
        out_specs=[VMEM, ANY],
        out_shape=[
            jax.ShapeDtypeStruct((members, seqs, width), jnp.bfloat16),
            jax.ShapeDtypeStruct((pack_rows, LANES), jnp.bfloat16),
        ],
        scratch_shapes=[pltpu.SemaphoreType.DMA((copies,))],
        name="attend",
    )(
        lengths,
        forget_bias,
        tokens,
        cache_keys.reshape(seqs, cache_len, head),
        cache_values.reshape(seqs, cache_len, head),
        cache_cum,
        norm_gain[None],
        query_weight,
        key_weight,
        value_weight,
        forget_weight.reshape(1, width),
        query_gain[None],
        key_gain[None],
        out_weight,
        expert_gate[0],
        expert_up[0],
        expert_down[0],
        shared_down,
    )
    partial = lax.all_to_all(partial, "tp", 0, 0, tiled=True)
    packs = [packed]
    for step in (1, members - 1, *range(2, members - 1)):
        ring = [(i, (i + step) % members) for i in range(members)]
        packs.append(lax.ppermute(packed, "tp", ring))

    norm_weights = route_weights / jnp.sum(route_weights, axis=1, keepdims=True)
    high = norm_weights.astype(jnp.bfloat16).astype(jnp.float32)
    low = norm_weights - high
    notes = jnp.concatenate([routes.astype(jnp.float32), high, low], axis=1)
    notes = jnp.pad(notes, ((0, 0), (0, LANES - notes.shape[1])))
    front = [shared_gate.T, shared_up.T, mix_weight[None]]
    front = jnp.concatenate(front, axis=0)
    front = jnp.pad(front, ((0, LANES - front.shape[0]), (0, 0)))
    chip = (lax.axis_index(EP) // 2).astype(jnp.int32)
    core = lax.axis_index(PAIR).astype(jnp.int32)
    steps = jnp.array([0, 1, members - 1, *range(2, members - 1)], jnp.int32)
    origins = (member.astype(jnp.int32) - steps) % members
    place = [2 * chip + core, 2 * chip + 1 - core]
    place += [origins[i] * (blocks // members) for i in range(members)]
    place = jnp.stack(place)

    sub_rows = peers * (blocks + NOTE_ROWS)
    residual, outgoing = pl.pallas_call(
        rows_kernel,
        in_specs=[SMEM] + [VMEM] * 4,
        out_specs=[VMEM, VMEM],
        out_shape=[
            jax.ShapeDtypeStruct((seqs, width), jnp.float32),
            jax.ShapeDtypeStruct((sub_rows, LANES), jnp.bfloat16),
        ],
        name="rows",
    )(member.astype(jnp.int32).reshape(1), partial, tokens, ffn_gain[None], notes)
    own_rows = lax.all_to_all(outgoing.reshape(-1, 2, LANES), EP, 0, 0, tiled=True)

    pair_front = swap(front)
    pair_packs = []
    for pack in packs:
        pair_packs.append(swap(pack))
    total = pl.pallas_call(
        share_kernel,
        in_specs=[SMEM] + [VMEM] * (3 + 2 * members),
        out_specs=VMEM,
        out_shape=jax.ShapeDtypeStruct((peers * blocks, LANES), jnp.bfloat16),
        scratch_shapes=[
            pltpu.VMEM((sub_rows, LANES), jnp.float32),
            pltpu.VMEM((peers, width), jnp.bfloat16),
            pltpu.VMEM((blocks, peers, LANES), jnp.float32),
        ],
        name="share",
    )(place, own_rows.reshape(sub_rows, LANES), front, pair_front, *packs, *pair_packs)
    returned = lax.all_to_all(total.reshape(-1, 2, LANES), (*EP, "tp"), 0, 0, tiled=True)
    returned = returned.reshape(peers // 2, seqs, -1, LANES).astype(jnp.float32)
    returned = jnp.sum(returned, axis=0).reshape(seqs, -1)
    slice_width = returned.shape[1]
    residual_slice = lax.dynamic_slice_in_dim(residual, member * slice_width, slice_width, 1)
    return (residual_slice + returned).astype(jnp.bfloat16)


def solution(mesh):
    finer = Mesh(mesh.devices.reshape(16, 4, 2, mesh.shape["tp"]), ("ep_0", "ep_1", "ep_2", "tp"))
    placed = (
        P(EP, None),
        P(EP),
        P(EP, None, "tp", None),
        P(EP, None, "tp", None),
        P(EP, "tp", None),
        P(),
        P(None, "tp"),
        P(None, "tp"),
        P(None, "tp"),
        P(None, "tp"),
        P("tp"),
        P(),
        P(),
        P("tp", None),
        P(),
        P(),
        P(None, EP),
        P(None, EP),
        P(EP, "tp"),
        P(EP, None),
        P(EP, None),
        P(EP, None, "tp"),
        P(EP, None, "tp"),
        P(EP, "tp", None),
    )

    return jax.shard_map(
        per_device, mesh=finer, in_specs=placed, out_specs=P(EP, "tp"), check_vma=False
    )
```

time: 176 us -> 164 us (0.932)
  Pallas kernels: 0 us -> 36.2 us
  waiting for transfers between devices: 83.3 us -> 57.7 us
  matrix products: 18.5 us -> 0 us
  other arithmetic: 13.6 us -> 2.34 us
  starting transfers between devices: 47.7 us -> 58.4 us
  local copies, waits for them, and re-layouts: 10.4 us -> 5.31 us
  between operations: 1.2 us -> 3.49 us
    pallas_call x0 -> x3, Pallas kernels: none -> 36.2 us  [the longest x1 28.2 us: per_device(): pl.pallas_call(attend_kernel, in_specs=[SMEM, SMEM] + [VMEM] * 12 + [ANY]...]
    all_to_all x4 -> x3, waiting for transfers between devices: 82.6 us -> 57.7 us  [the longest x1 26.1 us: per_device(): partial = lax.all_to_all(partial, 'tp', 0, 0, tiled=True)]
    dot_general x15 -> x0, matrix products: 18.5 us -> none  [the longest x2 4.42 us: share(): jnp.einsum('tnf,tfd->nd', hidden, down_all, preferred_element_type=jnp.fl...]
    ppermute x0 -> x3, starting transfers between devices: none -> 11.1 us  [per_device(): packs.append(lax.ppermute(packed, 'tp', ring))]
    all_to_all x4 -> x3, starting transfers between devices: 40.8 us -> 35.9 us  [the longest x1 20 us: per_device(): lax.all_to_all(outgoing.reshape(-1, 2, LANES), EP, 0, 0, tiled=True)]
    all_to_all x2 -> x0, other arithmetic: 4.61 us -> none  [the longest x1 2.39 us: per_device(): own_rows = lax.all_to_all(outgoing.reshape(peers, -1), EP, 0, 0, tiled=True)]
    ppermute x2 -> x5, starting transfers between devices: 6.9 us -> 11.5 us  [swap(): return lax.ppermute(shard, PAIR, [(0, 1), (1, 0)])]
    reduce_sum x8 -> x1, other arithmetic: 2.5 us -> 0.24 us  [per_device(): returned = jnp.sum(returned, axis=0).reshape(seqs, -1)]
  transfers between devices with their start and end apart: 6 -> 11, of which waited for: 5 -> 3; matrix products, arithmetic and copies ran while one was open for 4% -> 2% of each run, Pallas kernels for 0% -> 1%
where the time goes in v2:
time: 164 us; the launch traced here: 163 us
  starting transfers between devices  58.4 us (36%)
  waiting for transfers between devices  57.7 us (35%)
  Pallas kernels  36.2 us (22%)
  local copies, waits for them, and re-layouts  5.31 us (3%)
  between operations  3.49 us (2%)
  other arithmetic  2.34 us (1%)
    pallas_call x1, Pallas kernels, per_device(): pl.pallas_call(attend_kernel, in_specs=[SMEM, SMEM] + [VMEM] * 12 + [ANY]...  28.2 us
    all_to_all x1, waiting for transfers between devices, per_device(): partial = lax.all_to_all(partial, 'tp', 0, 0, tiled=True)  26.1 us
    all_to_all x1, waiting for transfers between devices, per_device(): lax.all_to_all(total.reshape(-1, 2, LANES), (*EP, 'tp'), 0, 0, tiled=True)  25 us
    all_to_all x1, starting transfers between devices, per_device(): lax.all_to_all(outgoing.reshape(-1, 2, LANES), EP, 0, 0, tiled=True)  20 us
    all_to_all x1, starting transfers between devices, per_device(): lax.all_to_all(total.reshape(-1, 2, LANES), (*EP, 'tp'), 0, 0, tiled=True)  12.7 us
    ppermute x5, starting transfers between devices, swap(): return lax.ppermute(shard, PAIR, [(0, 1), (1, 0)])  11.5 us
    ppermute x3, starting transfers between devices, per_device(): packs.append(lax.ppermute(packed, 'tp', ring))  11.1 us
    all_to_all x1, waiting for transfers between devices, per_device(): lax.all_to_all(outgoing.reshape(-1, 2, LANES), EP, 0, 0, tiled=True)  6.53 us
  transfers between devices with their start and end apart: 11, of which 3 were waited for; matrix products, arithmetic and copies ran while one was open for 2% of the time, Pallas kernels for 1%

profile of v2, /device:TPU:1, one launch (start us, length us, event | category | flops | bytes accessed | tf_op | source)
XLA Modules:
  0.0 163.4 jit_solution(1786261720039252376)
XLA Ops:
  0.7 1.3 broadcast_in_dim.16.norm_gain
  1.9 0.0 copy-start.9
  1.9 0.0 copy-start.12
  1.9 0.0 copy-start.10
  1.9 28.2 %attend.1 = (bf16[4,8,1024]{2,1,0:T(8,128)(2,1)}, bf16[3136,128]{1,0:T(8,128)(2,1)}) custom-call(s32[8]{0:T(128)} %lengths.1, f32[1]{0:T(128)S(6)} %copy.32.forget_bias, bf16[8,1024]{1,0:T(8,128)(2,1)} %tokens.3, bf16[8,512,128]{2,1,0:T(8,128)(2,1)} %bitcast.25, bf16[8,512,128]{2,1,0:T(8,128)(2,1)} %bitcast.26, f32[8,1,512]{2,1,0:T(1,128)} %cum.1, ...), custom_call_target="tpu_custom_call" | custom-call | tf_op jit(solution)/shard_map/attend/pallas_call | solution.py:253
  30.2 0.0 copy-start.2
  30.2 5.8 %collective-permute-start.3 = (bf16[3136,128]{1,0:T(8,128)(2,1)}, bf16[3136,128]{1,0:T(8,128)(2,1)S(1)}, u32[]{:S(2)}, u32[]{:S(2)}) collective-permute-start(bf16[3136,128]{1,0:T(8,128)(2,1)} %get-tuple-element.12.refs_0_), channel_id=1, source_target_pairs={{0,2},{1,3},{2,0},{3,1},{4,6},{5,7},{6,4},{7,5},{8,10},{9,11},{10,... | collective-permute-start | bytes 2408456 | tf_op jit(solution)/shard_map/ppermute | solution.py:287
  36.0 2.7 %collective-permute-start.2 = (bf16[3136,128]{1,0:T(8,128)(2,1)}, bf16[3136,128]{1,0:T(8,128)(2,1)S(1)}, u32[]{:S(2)}, u32[]{:S(2)}) collective-permute-start(bf16[3136,128]{1,0:T(8,128)(2,1)} %get-tuple-element.12.refs_0_), channel_id=1, source_target_pairs={{0,3},{1,0},{2,1},{3,2},{4,7},{5,4},{6,5},{7,6},{8,11},{9,8},{10,9... | collective-permute-start | bytes 2408456 | tf_op jit(solution)/shard_map/ppermute | solution.py:287
  38.6 2.6 %collective-permute-start.1 = (bf16[3136,128]{1,0:T(8,128)(2,1)}, bf16[3136,128]{1,0:T(8,128)(2,1)}, u32[]{:S(2)}, u32[]{:S(2)}) collective-permute-start(bf16[3136,128]{1,0:T(8,128)(2,1)} %get-tuple-element.12.refs_0_), channel_id=1, source_target_pairs={{0,1},{1,2},{2,3},{3,0},{4,5},{5,6},{6,7},{7,4},{8,9},{9,10},{10,1... | collective-permute-start | bytes 2408456 | tf_op jit(solution)/shard_map/ppermute | solution.py:287
  41.3 3.3 %all-to-all-start = ((bf16[4,8,1024]{2,1,0:T(8,128)(2,1)}), bf16[4,8,1024]{2,1,0:T(8,128)(2,1)S(1)}, u32[]{:S(2)}, u32[]{:S(2)}) async-start(bf16[4,8,1024]{2,1,0:T(8,128)(2,1)} %get-tuple-element.9), calls=%async_computation | async-start | bytes 131072 | tf_op jit(solution)/shard_map/all_to_all | solution.py:283
  44.6 0.0 copy-done.9
  44.6 0.1 copy.29
  44.7 0.0 copy-done.12
  44.7 0.1 copy.28
  44.8 0.1 convert_convert_fusion
  44.8 0.7 select_maximum_fusion.notes
  45.5 0.0 copy-done.10
  45.5 0.6 broadcast_in_dim.19.ffn_gain
  46.1 26.1 %all-to-all-done.partial = bf16[4,8,1024]{2,1,0:T(8,128)(2,1)S(1)} async-done(((bf16[4,8,1024]{2,1,0:T(8,128)(2,1)}), bf16[4,8,1024]{2,1,0:T(8,128)(2,1)S(1)}, u32[]{:S(2)}, u32[]{:S(2)}) %all-to-all-start) | async-done | bytes 65568 | tf_op jit(solution)/shard_map/all_to_all | solution.py:283
  72.2 0.0 copy-start.5
  72.2 0.6 copy-done.5
  72.9 1.7 %rows.1 = (f32[8,1024]{1,0:T(8,128)}, bf16[1280,128]{1,0:T(8,128)(2,1)}) custom-call(s32[1]{0:T(128)} %bitcast.member, bf16[4,8,1024]{2,1,0:T(8,128)(2,1)} %copy-done.5, bf16[8,1024]{1,0:T(8,128)(2,1)} %tokens.3, bf16[1,1024]{1,0:T(2,128)(2,1)} %broadcast_in_dim.19.ffn_gain, f32[8,128]{1,0:T(8,128)} %select_maximum_fusion.notes), custom_call_target="tpu_custom_call" | custom-call | tf_op jit(solution)/shard_map/rows/pallas_call | solution.py:306
  74.6 0.0 copy-start.11
  74.6 0.0 copy-start.7
  74.6 0.0 copy-start.8
  74.6 20.0 %all-to-all-start.1 = ((bf16[640,2,128]{2,1,0:T(2,128)(2,1)}), bf16[640,2,128]{2,1,0:T(2,128)(2,1)S(1)}, u32[]{:S(2)}, u32[]{:S(2)}) async-start(bf16[640,2,128]{2,1,0:T(2,128)(2,1)} %bitcast.28), calls=%async_computation.1 | async-start | bytes 655360 | tf_op jit(solution)/shard_map/all_to_all | solution.py:316
  94.6 0.0 copy-done.2
  94.6 2.8 %collective-permute-start.4 = (bf16[3136,128]{1,0:T(8,128)(2,1)S(1)}, bf16[3136,128]{1,0:T(8,128)(2,1)}, u32[]{:S(2)}, u32[]{:S(2)}) collective-permute-start(bf16[3136,128]{1,0:T(8,128)(2,1)S(1)} %copy-done.2), channel_id=1, source_target_pairs={{0,4},{4,0},{1,5},{5,1},{2,6},{6,2},{3,7},{7,3},{8,12},{12,8},{9,1... | collective-permute-start | bytes 2408456 | tf_op jit(solution)/shard_map/ppermute | solution.py:22
  97.4 0.0 collective-permute-done.3.refs_3_
  97.4 0.0 copy-start.3
  97.4 1.9 %collective-permute-start.7 = (bf16[3136,128]{1,0:T(8,128)(2,1)S(1)}, bf16[3136,128]{1,0:T(8,128)(2,1)}, u32[]{:S(2)}, u32[]{:S(2)}) collective-permute-start(bf16[3136,128]{1,0:T(8,128)(2,1)S(1)} %collective-permute-done.3.refs_3_), channel_id=1, source_target_pairs={{0,4},{4,0},{1,5},{5,1},{2,6},{6,2},{3,7},{7,3},{8,12},{12,8},{9,1... | collective-permute-start | bytes 2408456 | tf_op jit(solution)/shard_map/ppermute | solution.py:22
  99.3 0.0 collective-permute-done.2.refs_2_
  99.3 0.0 copy-start.4
  99.4 2.4 %collective-permute-start.6 = (bf16[3136,128]{1,0:T(8,128)(2,1)S(1)}, bf16[3136,128]{1,0:T(8,128)(2,1)}, u32[]{:S(2)}, u32[]{:S(2)}) collective-permute-start(bf16[3136,128]{1,0:T(8,128)(2,1)S(1)} %collective-permute-done.2.refs_2_), channel_id=1, source_target_pairs={{0,4},{4,0},{1,5},{5,1},{2,6},{6,2},{3,7},{7,3},{8,12},{12,8},{9,1... | collective-permute-start | bytes 2408456 | tf_op jit(solution)/shard_map/ppermute | solution.py:22
  101.8 0.0 collective-permute-done.1.refs_1_
  101.8 1.9 %collective-permute-start.5 = (bf16[3136,128]{1,0:T(8,128)(2,1)}, bf16[3136,128]{1,0:T(8,128)(2,1)}, u32[]{:S(2)}, u32[]{:S(2)}) collective-permute-start(bf16[3136,128]{1,0:T(8,128)(2,1)} %collective-permute-done.1.refs_1_), channel_id=1, source_target_pairs={{0,4},{4,0},{1,5},{5,1},{2,6},{6,2},{3,7},{7,3},{8,12},{12,8},{9,1... | collective-permute-start | bytes 2408456 | tf_op jit(solution)/shard_map/ppermute | solution.py:22
  103.7 0.0 copy-done.11
  103.7 0.0 copy-done.7
  103.7 0.0 copy-done.8
  103.8 0.0 copy-start.1
  103.8 2.4 %collective-permute-start = (bf16[128,1024]{1,0:T(8,128)(2,1)S(1)}, bf16[128,1024]{1,0:T(8,128)(2,1)S(1)}, u32[]{:S(2)}, u32[]{:S(2)}) collective-permute-start(bf16[128,1024]{1,0:T(8,128)(2,1)S(1)} %fusion.4.front), channel_id=1, source_target_pairs={{0,4},{4,0},{1,5},{5,1},{2,6},{6,2},{3,7},{7,3},{8,12},{12,8},{9,1... | collective-permute-start | bytes 786440 | tf_op jit(solution)/shard_map/ppermute | solution.py:22
  106.2 0.0 copy-start.13
  106.2 0.6 copy-done.13
  106.9 0.7 fusion.8
  110.1 0.6 stack.15.place
  110.7 0.0 collective-permute-done.pair_front
  110.7 0.0 copy-start.6
  110.7 0.0 collective-permute-done.4.refs_4_
  110.7 6.5 %all-to-all-done.1 = bf16[640,2,128]{2,1,0:T(2,128)(2,1)S(1)} async-done(((bf16[640,2,128]{2,1,0:T(2,128)(2,1)}), bf16[640,2,128]{2,1,0:T(2,128)(2,1)S(1)}, u32[]{:S(2)}, u32[]{:S(2)}) %all-to-all-start.1) | async-done | bytes 327712 | tf_op jit(solution)/shard_map/all_to_all | solution.py:316
  117.3 0.0 copy-start
  117.3 0.0 collective-permute-done.7.refs_7_
  117.3 0.0 collective-permute-done.6.refs_6_
  117.3 0.0 collective-permute-done.5.refs_5_
  117.3 0.0 copy-done.3
  117.3 0.0 copy-done.4
  117.3 0.0 copy-done.1
  117.3 0.0 copy-done.6
  117.3 0.7 copy-done
  118.0 6.2 %share.1 = bf16[1024,128]{1,0:T(8,128)(2,1)} custom-call(s32[6]{0:T(128)} %stack.15.place, bf16[1280,128]{1,0:T(8,128)(2,1)} %bitcast.23, bf16[128,1024]{1,0:T(8,128)(2,1)} %copy-done.1, bf16[128,1024]{1,0:T(8,128)(2,1)} %copy-done.6, bf16[3136,128]{1,0:T(8,128)(2,1)} %get-tuple-element.12.refs_0_, bf16[3136,128]{1,0:T(8,128)(2,1)} %collective-permute-done.1.refs_1_, ...), custom_call_target="tpu_custom_call" | custom-call | tf_op jit(solution)/shard_map/share/pallas_call | solution.py:322
  124.2 12.7 %all-to-all-start.2 = ((bf16[512,2,128]{2,1,0:T(2,128)(2,1)}), bf16[512,2,128]{2,1,0:T(2,128)(2,1)S(1)}, u32[]{:S(2)}, u32[]{:S(2)}) async-start(bf16[512,2,128]{2,1,0:T(2,128)(2,1)} %bitcast.27), calls=%async_computation.2 | async-start | bytes 524288 | tf_op jit(solution)/shard_map/all_to_all | solution.py:334
  136.9 25.0 %all-to-all-done.2 = bf16[512,2,128]{2,1,0:T(2,128)(2,1)S(1)} async-done(((bf16[512,2,128]{2,1,0:T(2,128)(2,1)}), bf16[512,2,128]{2,1,0:T(2,128)(2,1)S(1)}, u32[]{:S(2)}, u32[]{:S(2)}) %all-to-all-start.2) | async-done | bytes 262176 | tf_op jit(solution)/shard_map/all_to_all | solution.py:334
  161.9 0.2 convert_reduce_fusion
  162.1 1.3 fusion.5
  (5 shorter events, 0.1 us)
Async XLA Ops:
  1.9 42.6 %copy-start.9 = (f32[8,2]{0,1:T(2,128)S(1)}, f32[8,2]{0,1:T(2,128)}, u32[]{:S(2)}) copy-start(f32[8,2]{0,1:T(2,128)} %param.45) | copy-start | bytes 196
  1.9 42.7 %copy-start.12 = (s32[8,2]{0,1:T(2,128)S(1)}, s32[8,2]{0,1:T(2,128)}, u32[]{:S(2)}) copy-start(s32[8,2]{0,1:T(2,128)} %param.44) | copy-start | bytes 196
  1.9 43.6 %copy-start.10 = (bf16[1024]{0:T(1024)(128)(2,1)S(1)}, bf16[1024]{0:T(1024)(128)(2,1)}, u32[]{:S(2)}) copy-start(bf16[1024]{0:T(1024)(128)(2,1)} %param.39) | copy-start | bytes 6148
  30.2 64.4 %copy-start.2 = (bf16[3136,128]{1,0:T(8,128)(2,1)S(1)}, bf16[3136,128]{1,0:T(8,128)(2,1)}, u32[]{:S(2)}) copy-start(bf16[3136,128]{1,0:T(8,128)(2,1)} %get-tuple-element.12.refs_0_) | copy-start | bytes 2408452
  30.2 67.2 %collective-permute-start.3 = (bf16[3136,128]{1,0:T(8,128)(2,1)}, bf16[3136,128]{1,0:T(8,128)(2,1)S(1)}, u32[]{:S(2)}, u32[]{:S(2)}) collective-permute-start(bf16[3136,128]{1,0:T(8,128)(2,1)} %get-tuple-element.12.refs_0_), channel_id=1, source_target_pairs={{0,2},{1,3},{2,0},{3,1},{4,6},{5,7},{6,4},{7,5},{8,10},{9,11},{10,... | collective-permute-start | bytes 2408456 | tf_op jit(solution)/shard_map/ppermute | solution.py:287
  36.0 63.4 %collective-permute-start.2 = (bf16[3136,128]{1,0:T(8,128)(2,1)}, bf16[3136,128]{1,0:T(8,128)(2,1)S(1)}, u32[]{:S(2)}, u32[]{:S(2)}) collective-permute-start(bf16[3136,128]{1,0:T(8,128)(2,1)} %get-tuple-element.12.refs_0_), channel_id=1, source_target_pairs={{0,3},{1,0},{2,1},{3,2},{4,7},{5,4},{6,5},{7,6},{8,11},{9,8},{10,9... | collective-permute-start | bytes 2408456 | tf_op jit(solution)/shard_map/ppermute | solution.py:287
  38.6 63.1 %collective-permute-start.1 = (bf16[3136,128]{1,0:T(8,128)(2,1)}, bf16[3136,128]{1,0:T(8,128)(2,1)}, u32[]{:S(2)}, u32[]{:S(2)}) collective-permute-start(bf16[3136,128]{1,0:T(8,128)(2,1)} %get-tuple-element.12.refs_0_), channel_id=1, source_target_pairs={{0,1},{1,2},{2,3},{3,0},{4,5},{5,6},{6,7},{7,4},{8,9},{9,10},{10,1... | collective-permute-start | bytes 2408456 | tf_op jit(solution)/shard_map/ppermute | solution.py:287
  41.3 31.0 %all-to-all-start = ((bf16[4,8,1024]{2,1,0:T(8,128)(2,1)}), bf16[4,8,1024]{2,1,0:T(8,128)(2,1)S(1)}, u32[]{:S(2)}, u32[]{:S(2)}) async-start(bf16[4,8,1024]{2,1,0:T(8,128)(2,1)} %get-tuple-element.9), calls=%async_computation | async-start | bytes 131072 | tf_op jit(solution)/shard_map/all_to_all | solution.py:283
  72.2 0.6 copy-start.5
  74.6 29.1 %copy-start.11 = (bf16[1024]{0:T(1024)(128)(2,1)S(1)}, bf16[1024]{0:T(1024)(128)(2,1)}, u32[]{:S(2)}) copy-start(bf16[1024]{0:T(1024)(128)(2,1)} %param.40) | copy-start | bytes 6148
  74.6 29.1 %copy-start.7 = (bf16[1024,32]{0,1:T(8,128)(2,1)S(1)}, bf16[1024,32]{0,1:T(8,128)(2,1)}, u32[]{:S(2)}) copy-start(bf16[1024,32]{0,1:T(8,128)(2,1)} %param.42) | copy-start | bytes 196612
  74.6 29.2 %copy-start.8 = (bf16[1024,32]{0,1:T(8,128)(2,1)S(1)}, bf16[1024,32]{0,1:T(8,128)(2,1)}, u32[]{:S(2)}) copy-start(bf16[1024,32]{0,1:T(8,128)(2,1)} %param.41) | copy-start | bytes 196612
  74.6 42.7 %all-to-all-start.1 = ((bf16[640,2,128]{2,1,0:T(2,128)(2,1)}), bf16[640,2,128]{2,1,0:T(2,128)(2,1)S(1)}, u32[]{:S(2)}, u32[]{:S(2)}) async-start(bf16[640,2,128]{2,1,0:T(2,128)(2,1)} %bitcast.28), calls=%async_computation.1 | async-start | bytes 655360 | tf_op jit(solution)/shard_map/all_to_all | solution.py:316
  94.6 16.2 %collective-permute-start.4 = (bf16[3136,128]{1,0:T(8,128)(2,1)S(1)}, bf16[3136,128]{1,0:T(8,128)(2,1)}, u32[]{:S(2)}, u32[]{:S(2)}) collective-permute-start(bf16[3136,128]{1,0:T(8,128)(2,1)S(1)} %copy-done.2), channel_id=1, source_target_pairs={{0,4},{4,0},{1,5},{5,1},{2,6},{6,2},{3,7},{7,3},{8,12},{12,8},{9,1... | collective-permute-start | bytes 2408456 | tf_op jit(solution)/shard_map/ppermute | solution.py:22
  97.4 19.9 %copy-start.3 = (bf16[3136,128]{1,0:T(8,128)(2,1)}, bf16[3136,128]{1,0:T(8,128)(2,1)S(1)}, u32[]{:S(2)}) copy-start(bf16[3136,128]{1,0:T(8,128)(2,1)S(1)} %collective-permute-done.3.refs_3_) | copy-start | bytes 2408452
  97.4 19.9 %collective-permute-start.7 = (bf16[3136,128]{1,0:T(8,128)(2,1)S(1)}, bf16[3136,128]{1,0:T(8,128)(2,1)}, u32[]{:S(2)}, u32[]{:S(2)}) collective-permute-start(bf16[3136,128]{1,0:T(8,128)(2,1)S(1)} %collective-permute-done.3.refs_3_), channel_id=1, source_target_pairs={{0,4},{4,0},{1,5},{5,1},{2,6},{6,2},{3,7},{7,3},{8,12},{12,8},{9,1... | collective-permute-start | bytes 2408456 | tf_op jit(solution)/shard_map/ppermute | solution.py:22
  99.3 18.0 %copy-start.4 = (bf16[3136,128]{1,0:T(8,128)(2,1)}, bf16[3136,128]{1,0:T(8,128)(2,1)S(1)}, u32[]{:S(2)}) copy-start(bf16[3136,128]{1,0:T(8,128)(2,1)S(1)} %collective-permute-done.2.refs_2_) | copy-start | bytes 2408452
  99.4 17.9 %collective-permute-start.6 = (bf16[3136,128]{1,0:T(8,128)(2,1)S(1)}, bf16[3136,128]{1,0:T(8,128)(2,1)}, u32[]{:S(2)}, u32[]{:S(2)}) collective-permute-start(bf16[3136,128]{1,0:T(8,128)(2,1)S(1)} %collective-permute-done.2.refs_2_), channel_id=1, source_target_pairs={{0,4},{4,0},{1,5},{5,1},{2,6},{6,2},{3,7},{7,3},{8,12},{12,8},{9,1... | collective-permute-start | bytes 2408456 | tf_op jit(solution)/shard_map/ppermute | solution.py:22
  101.8 15.5 %collective-permute-start.5 = (bf16[3136,128]{1,0:T(8,128)(2,1)}, bf16[3136,128]{1,0:T(8,128)(2,1)}, u32[]{:S(2)}, u32[]{:S(2)}) collective-permute-start(bf16[3136,128]{1,0:T(8,128)(2,1)} %collective-permute-done.1.refs_1_), channel_id=1, source_target_pairs={{0,4},{4,0},{1,5},{5,1},{2,6},{6,2},{3,7},{7,3},{8,12},{12,8},{9,1... | collective-permute-start | bytes 2408456 | tf_op jit(solution)/shard_map/ppermute | solution.py:22
  103.8 13.5 %copy-start.1 = (bf16[128,1024]{1,0:T(8,128)(2,1)}, bf16[128,1024]{1,0:T(8,128)(2,1)S(1)}, u32[]{:S(2)}) copy-start(bf16[128,1024]{1,0:T(8,128)(2,1)S(1)} %fusion.4.front) | copy-start | bytes 786436
  103.8 6.9 %collective-permute-start = (bf16[128,1024]{1,0:T(8,128)(2,1)S(1)}, bf16[128,1024]{1,0:T(8,128)(2,1)S(1)}, u32[]{:S(2)}, u32[]{:S(2)}) collective-permute-start(bf16[128,1024]{1,0:T(8,128)(2,1)S(1)} %fusion.4.front), channel_id=1, source_target_pairs={{0,4},{4,0},{1,5},{5,1},{2,6},{6,2},{3,7},{7,3},{8,12},{12,8},{9,1... | collective-permute-start | bytes 786440 | tf_op jit(solution)/shard_map/ppermute | solution.py:22
  106.2 0.7 copy-start.13
  110.7 6.6 %copy-start.6 = (bf16[128,1024]{1,0:T(8,128)(2,1)}, bf16[128,1024]{1,0:T(8,128)(2,1)S(1)}, u32[]{:S(2)}) copy-start(bf16[128,1024]{1,0:T(8,128)(2,1)S(1)} %collective-permute-done.pair_front) | copy-start | bytes 786436
  117.3 0.7 copy-start
  124.2 37.7 %all-to-all-start.2 = ((bf16[512,2,128]{2,1,0:T(2,128)(2,1)}), bf16[512,2,128]{2,1,0:T(2,128)(2,1)S(1)}, u32[]{:S(2)}, u32[]{:S(2)}) async-start(bf16[512,2,128]{2,1,0:T(2,128)(2,1)} %bitcast.27), calls=%async_computation.2 | async-start | bytes 524288 | tf_op jit(solution)/shard_map/all_to_all | solution.py:334

commit v3 on v2

v3 whole, which is shorter than its diff:
```python
import jax
import jax.numpy as jnp
from jax import lax
from jax.experimental import pallas as pl
from jax.experimental.pallas import tpu as pltpu
from jax.sharding import Mesh
from jax.sharding import PartitionSpec as P

EP = ("ep_0", "ep_1", "ep_2")
PAIR = "ep_2"
LANES = 128
NOTE_ROWS = 2

epsilon = 1e-06

VMEM = pl.BlockSpec(memory_space=pltpu.VMEM)
SMEM = pl.BlockSpec(memory_space=pltpu.SMEM)
ANY = pl.BlockSpec(memory_space=pl.ANY)


def swap(shard):
    return lax.ppermute(shard, PAIR, [(0, 1), (1, 0)])


def scaled(values, gain):
    mean = jnp.mean(values * values, axis=-1, keepdims=True)
    return values * lax.rsqrt(mean + epsilon) * gain


def silu(values):
    return values / (1.0 + jnp.exp(-values))


def in_vmem(values):
    return pltpu.with_memory_space_constraint(values, pltpu.VMEM)


def ring_steps(members):
    return (0, 1, members - 1, *range(2, members - 1))


def wide_dot(left, right):
    return jnp.dot(left, right, preferred_element_type=jnp.float32)


def attend_kernel(
    lengths,
    forget_bias,
    norm_gain,
    query_gain,
    key_gain,
    forget_weight,
    tokens_hbm,
    query_weight_hbm,
    key_weight_hbm,
    value_weight_hbm,
    cum_hbm,
    keys_hbm,
    values_hbm,
    out_weight_hbm,
    expert_gate,
    expert_up,
    expert_down,
    shared_down,
    partial,
    packed,
    tokens,
    query_weight,
    key_weight,
    value_weight,
    cum,
    keys,
    values,
    out_weight,
    sems,
):
    copies = []

    def start(source, target):
        copy = pltpu.make_async_copy(source, target, sems.at[len(copies)])
        copy.start()
        copies.append(copy)
        return copy

    tokens_in = start(tokens_hbm, tokens)
    query_in = start(query_weight_hbm, query_weight)
    key_in = start(key_weight_hbm, key_weight)
    value_in = start(value_weight_hbm, value_weight)
    keys_in = start(keys_hbm, keys)
    cum_in = start(cum_hbm, cum)
    values_in = start(values_hbm, values)
    out_in = start(out_weight_hbm, out_weight)
    first_packed = len(copies)
    row = 0

    def pack(source, row):
        start(source, packed.at[pl.ds(row, source.shape[0]), :])
        return row + source.shape[0]

    row = pack(expert_gate, row)
    row = pack(expert_up, row)
    for block in range(expert_down.shape[1] // LANES):
        row = pack(expert_down.at[:, pl.ds(block * LANES, LANES)], row)
    for block in range(shared_down.shape[1] // LANES):
        row = pack(shared_down.at[:, pl.ds(block * LANES, LANES)], row)

    seqs, cache_len, head = keys.shape
    groups = query_weight.shape[1] // head
    tokens_in.wait()
    normed = scaled(tokens[...].astype(jnp.float32), norm_gain[...].astype(jnp.float32))
    normed = normed.astype(jnp.bfloat16)
    gain = query_gain[...].astype(jnp.float32)
    query_in.wait()
    wide = wide_dot(normed, query_weight[...])
    query = [scaled(wide[:, g * head : (g + 1) * head], gain) for g in range(groups)]
    query = jnp.concatenate(query, axis=0).astype(jnp.bfloat16)
    key_in.wait()
    new_key = scaled(wide_dot(normed, key_weight[...]), key_gain[...].astype(jnp.float32))
    new_key = new_key.astype(jnp.bfloat16).astype(jnp.float32)
    value_in.wait()
    new_value = wide_dot(normed, value_weight[...]).astype(jnp.bfloat16).astype(jnp.float32)
    products = normed.astype(jnp.float32) * forget_weight[...].astype(jnp.float32)
    forget = jnp.sum(products, axis=-1, keepdims=True) + forget_bias[0]
    new_log = jnp.minimum(forget, 0.0) - jnp.log1p(jnp.exp(-jnp.abs(forget)))

    rows = groups * seqs
    owner = lax.broadcasted_iota(jnp.int32, (rows, cache_len), 0) % seqs
    position = lax.broadcasted_iota(jnp.int32, (rows, cache_len), 1)
    scores = jnp.zeros((rows, cache_len), jnp.float32)
    decay = jnp.zeros((rows, cache_len), jnp.float32)
    length = jnp.zeros((rows, cache_len), jnp.int32)
    keys_in.wait()
    cum_in.wait()
    for b in range(seqs):
        mine = owner == b
        one = lax.dot_general(
            query, keys[b], (((1,), (1,)), ((), ())), preferred_element_type=jnp.float32
        )
        scores = jnp.where(mine, one, scores)
        decay = jnp.where(mine, cum[b], decay)
        length = jnp.where(mine, lengths[b], length)
    last = jnp.where(position == length - 1, decay, 0.0)
    last = jnp.sum(last, axis=-1, keepdims=True)
    bias = last - decay + jnp.concatenate([new_log] * groups, axis=0)
    score_scale = head ** (-0.5)
    past = jnp.where(position < length, scores * score_scale + bias, -jnp.inf)
    own = query.astype(jnp.float32) * jnp.concatenate([new_key] * groups, axis=0)
    own = jnp.sum(own, axis=-1, keepdims=True) * score_scale
    past_exp = jnp.exp(past)
    own_exp = jnp.exp(own)
    denominator = jnp.sum(past_exp, axis=-1, keepdims=True) + own_exp
    past_prob = (past_exp / denominator).astype(jnp.bfloat16)
    own_prob = (own_exp / denominator).astype(jnp.bfloat16).astype(jnp.float32)
    head_owner = owner[:, :head]
    mixed = jnp.zeros((rows, head), jnp.float32)
    values_in.wait()
    for b in range(seqs):
        mixed = jnp.where(head_owner == b, wide_dot(past_prob, values[b]), mixed)
    mixed = mixed + own_prob * jnp.concatenate([new_value] * groups, axis=0)
    heads_out = [mixed[g * seqs : (g + 1) * seqs] for g in range(groups)]
    heads_out = jnp.concatenate(heads_out, axis=1).astype(jnp.bfloat16)
    out_in.wait()
    product = wide_dot(heads_out, out_weight[...]).astype(jnp.bfloat16)
    for peer in range(partial.shape[0]):
        partial[peer] = product
    for copy in copies[first_packed:]:
        copy.wait()


def rows_kernel(partial, tokens, ffn_gain, routes, route_weights, residual, outgoing):
    member = lax.axis_index("tp")
    attended = jnp.sum(partial[...].astype(jnp.float32), axis=0)
    full = tokens[...].astype(jnp.float32) + attended
    seqs, width = full.shape
    members = partial.shape[0]
    slice_width = width // members
    for t in range(members):

        @pl.when(member == t)
        def _():
            residual[...] = full[:, t * slice_width : (t + 1) * slice_width]

    normed = scaled(full, ffn_gain[...].astype(jnp.float32))
    normed = normed.astype(jnp.bfloat16).astype(jnp.float32)
    norm_weights = route_weights[...]
    norm_weights = norm_weights / jnp.sum(norm_weights, axis=0, keepdims=True)
    high = norm_weights.astype(jnp.bfloat16).astype(jnp.float32)
    low = norm_weights - high
    marks = (routes[...].astype(jnp.float32), high, low)
    column = lax.broadcasted_iota(jnp.int32, routes.shape, 1)
    lane = lax.broadcasted_iota(jnp.int32, (1, LANES), 1)
    rows_here = lax.broadcasted_iota(jnp.int32, (seqs, width), 0)
    pieces = []
    for half in range(2):
        at = half * members + member
        row = jnp.sum(jnp.where(rows_here == at, normed, 0.0), axis=0, keepdims=True)
        mark = jnp.zeros((1, LANES), jnp.float32)
        for i, values in enumerate(marks):
            here = jnp.sum(jnp.where(column == at, values, 0.0), axis=1, keepdims=True)
            for j in range(2):
                mark = jnp.where(lane == 2 * i + j, here[j : j + 1], mark)
        pieces += [row[:, k : k + LANES] for k in range(0, width, LANES)]
        pieces += [mark, jnp.zeros_like(mark)]
    pattern = jnp.concatenate(pieces * 4, axis=0).astype(jnp.bfloat16)
    step = pattern.shape[0]
    for i in range(outgoing.shape[0] // step):
        outgoing[i * step : (i + 1) * step, :] = pattern


def share_kernel(rows, front, pair_front, *refs):
    sources, (out, wide, narrow, columns, staged, sems) = refs[:-6], refs[-6:]
    members = len(sources) // 2
    packs, arrivals = [sources[0]], [None]
    for i, source in enumerate(sources[1:]):
        copy = pltpu.make_async_copy(source, staged.at[i], sems.at[i])
        copy.start()
        packs.append(staged.at[i])
        arrivals.append(copy)
    member = lax.axis_index("tp")
    core = lax.axis_index(PAIR)
    experts = (lax.axis_index(EP), lax.axis_index(EP) + 1 - 2 * core)
    width = front.shape[1]
    count = narrow.shape[0]
    blocks = width // LANES
    stride = blocks + NOTE_ROWS
    wide[...] = rows[...].astype(jnp.float32)
    for k in range(blocks):
        piece = wide[pl.ds(k, count, stride=stride), :]
        narrow[:, k * LANES : (k + 1) * LANES] = piece.astype(jnp.bfloat16)
    marks = wide[pl.ds(blocks, count, stride=stride), :]
    values = narrow[...]
    down_start = 2 * width
    shared_start = down_start + blocks * LANES
    per_member = blocks // members
    units = (packs[0].shape[0] - shared_start) // per_member

    fronts = [
        lax.dot_general(
            values, each[...], (((1,), (1,)), ((), ())), preferred_element_type=jnp.float32
        )
        for each in (front, pair_front)
    ]
    mix_gate = 1.0 / (1.0 + jnp.exp(-fronts[0][:, 2 * units : 2 * units + 1]))
    hidden = []
    for side in range(2):
        me = experts[side].astype(jnp.float32)
        weight = jnp.zeros((count, 1), jnp.float32)
        for j in range(2):
            chosen = marks[:, j : j + 1] == me
            norm_weight = marks[:, 2 + j : 3 + j] + marks[:, 4 + j : 5 + j]
            weight = weight + jnp.where(chosen, norm_weight, 0.0)
        for s in range(members):
            pack = packs[side * members + s]
            if arrivals[side * members + s] is not None:
                arrivals[side * members + s].wait()
            gate = wide_dot(values, pack[:width, :])
            up = wide_dot(values, pack[width : 2 * width, :])
            hidden.append((weight, (silu(gate) * up).astype(jnp.bfloat16)))
    shared = [silu(pre[:, :units]) * pre[:, units : 2 * units] for pre in fronts]
    shared = [each.astype(jnp.bfloat16) for each in shared]
    for s, step in enumerate(ring_steps(members)):
        origin = (member + members - step) % members
        for k in range(per_member):
            rows_of = pl.ds(shared_start + k * units, units)
            dense = wide_dot(shared[0], packs[s][rows_of, :])
            dense = dense + wide_dot(shared[1], packs[members + s][rows_of, :])
            columns[origin * per_member + k] = mix_gate * dense

    for k in range(blocks):
        total = columns[k]
        for side in range(2):
            first = down_start + k * LANES
            routed = jnp.zeros((count, LANES), jnp.float32)
            for s in range(members):
                weight, each = hidden[side * members + s]
                pack = packs[side * members + s]
                routed = routed + wide_dot(each, pack[first : first + LANES, :])
            total = total + weight * routed
        wide[pl.ds(k, count, stride=blocks), :] = total
    out[...] = wide[: count * blocks, :].astype(jnp.bfloat16)


def per_device(
    tokens,
    lengths,
    cache_keys,
    cache_values,
    cache_cum,
    norm_gain,
    query_weight,
    key_weight,
    value_weight,
    forget_weight,
    forget_bias,
    query_gain,
    key_gain,
    out_weight,
    ffn_gain,
    mix_weight,
    shared_gate,
    shared_up,
    shared_down,
    routes,
    route_weights,
    expert_gate,
    expert_up,
    expert_down,
):
    seqs, width = tokens.shape
    cache_len, head = cache_keys.shape[1], cache_keys.shape[3]
    peers = lax.axis_size(EP)
    members = lax.axis_size("tp")
    blocks = width // LANES
    units = shared_gate.shape[1]
    hidden = expert_gate.shape[2]
    pack_rows = 2 * width + hidden * blocks + units * shared_down.shape[1] // LANES
    copies = 2 + blocks + shared_down.shape[1] // LANES

    big = [
        tokens,
        query_weight,
        key_weight,
        value_weight,
        cache_cum,
        cache_keys.reshape(seqs, cache_len, head),
        cache_values.reshape(seqs, cache_len, head),
        out_weight,
    ]
    partial, packed = pl.pallas_call(
        attend_kernel,
        in_specs=[SMEM, SMEM] + [VMEM] * 4 + [ANY] * (len(big) + 4),
        out_specs=[VMEM, VMEM],
        out_shape=[
            pltpu.VMEM((members, seqs, width), jnp.bfloat16),
            pltpu.VMEM((pack_rows, LANES), jnp.bfloat16),
        ],
        scratch_shapes=[pltpu.VMEM(each.shape, each.dtype) for each in big]
        + [pltpu.SemaphoreType.DMA((copies + len(big),))],
        name="attend",
    )(
        lengths,
        forget_bias,
        norm_gain,
        query_gain,
        key_gain,
        forget_weight.reshape(1, width),
        *big,
        expert_gate[0],
        expert_up[0],
        expert_down[0],
        shared_down,
    )
    partial = lax.all_to_all(partial, "tp", 0, 0, tiled=True)
    packs = [packed]
    for step in ring_steps(members)[1:]:
        ring = [(i, (i + step) % members) for i in range(members)]
        packs.append(lax.ppermute(packed, "tp", ring))

    front = [shared_gate.T, shared_up.T, mix_weight[None]]
    front = jnp.concatenate(front, axis=0)
    front = jnp.pad(front, ((0, LANES - front.shape[0]), (0, 0)))

    sub_rows = peers * (blocks + NOTE_ROWS)
    residual, outgoing = pl.pallas_call(
        rows_kernel,
        in_specs=[VMEM] * 5,
        out_specs=[VMEM, VMEM],
        out_shape=[
            jax.ShapeDtypeStruct((seqs, width // members), jnp.float32),
            pltpu.VMEM((sub_rows, LANES), jnp.bfloat16),
        ],
        name="rows",
    )(in_vmem(partial), tokens, ffn_gain, routes.T, route_weights.T)
    own_rows = lax.all_to_all(outgoing.reshape(-1, 2, LANES), EP, 0, 0, tiled=True)

    pair_front = swap(front)
    pair_packs = []
    for pack in packs:
        pair_packs.append(swap(pack))
    total = pl.pallas_call(
        share_kernel,
        in_specs=[VMEM] * 4 + [ANY] * (2 * members - 1),
        out_specs=VMEM,
        out_shape=pltpu.VMEM((peers * blocks, LANES), jnp.bfloat16),
        scratch_shapes=[
            pltpu.VMEM((sub_rows, LANES), jnp.float32),
            pltpu.VMEM((peers, width), jnp.bfloat16),
            pltpu.VMEM((blocks, peers, LANES), jnp.float32),
            pltpu.VMEM((2 * members - 1, pack_rows, LANES), jnp.bfloat16),
            pltpu.SemaphoreType.DMA((2 * members - 1,)),
        ],
        name="share",
    )(
        *map(in_vmem, (own_rows.reshape(sub_rows, LANES), front, pair_front, packed)),
        *packs[1:],
        *pair_packs,
    )
    returned = lax.all_to_all(total.reshape(-1, 2, LANES), (*EP, "tp"), 0, 0, tiled=True)
    returned = returned.reshape(peers // 2, seqs, -1, LANES).astype(jnp.float32)
    returned = jnp.sum(returned, axis=0).reshape(seqs, -1)
    return (residual + returned).astype(jnp.bfloat16)


def solution(mesh):
    finer = Mesh(mesh.devices.reshape(16, 4, 2, mesh.shape["tp"]), ("ep_0", "ep_1", "ep_2", "tp"))
    placed = (
        P(EP, None),
        P(EP),
        P(EP, None, "tp", None),
        P(EP, None, "tp", None),
        P(EP, "tp", None),
        P(),
        P(None, "tp"),
        P(None, "tp"),
        P(None, "tp"),
        P(None, "tp"),
        P("tp"),
        P(),
        P(),
        P("tp", None),
        P(),
        P(),
        P(None, EP),
        P(None, EP),
        P(EP, "tp"),
        P(EP, None),
        P(EP, None),
        P(EP, None, "tp"),
        P(EP, None, "tp"),
        P(EP, "tp", None),
    )

    return jax.shard_map(
        per_device, mesh=finer, in_specs=placed, out_specs=P(EP, "tp"), check_vma=False
    )
```

time: 164 us -> 134 us (0.82)
  blocking collectives: 0 us -> 68.2 us
  waiting for transfers between devices: 57.7 us -> 11.1 us
  Pallas kernels: 36.2 us -> 9.62 us
  starting transfers between devices: 58.4 us -> 42.3 us
  local copies, waits for them, and re-layouts: 5.31 us -> 0.47 us
  between operations: 3.49 us -> 0.82 us
    all_to_all x0 -> x2, blocking collectives: none -> 68.2 us  [the longest x1 37.4 us: per_device(): lax.all_to_all(total.reshape(-1, 2, LANES), (*EP, 'tp'), 0, 0, tiled=True)]
    all_to_all x2 -> x0, waiting for transfers between devices: 51.1 us -> none  [the longest x1 26.1 us: per_device(): partial = lax.all_to_all(partial, 'tp', 0, 0, tiled=True)]
    pallas_call x3, Pallas kernels: 36.2 us -> 9.62 us  [the longest x1 4.18 us: per_device(): pl.pallas_call(share_kernel, in_specs=[VMEM] * 4 + [ANY] * (2 * members -...]
    all_to_all x2 -> x0, starting transfers between devices: 16 us -> none  [the longest x1 12.7 us: per_device(): lax.all_to_all(total.reshape(-1, 2, LANES), (*EP, 'tp'), 0, 0, tiled=True)]
    all_to_all x1, waiting for transfers between devices: 6.53 us -> 9.96 us  [per_device(): lax.all_to_all(outgoing.reshape(-1, 2, LANES), EP, 0, 0, tiled=True)]
    broadcast_in_dim x2 -> x0, local copies, waits for them, and re-layouts: 1.87 us -> none  [the longest x1 1.28 us: per_device(): norm_gain[None]]
    unnamed x30 -> x10, local copies, waits for them, and re-layouts: 2.14 us -> 0.47 us
  transfers between devices with their start and end apart: 11 -> 9, of which waited for: 3 -> 2; matrix products, arithmetic and copies ran while one was open for 2% -> 0% of each run, Pallas kernels for 1% -> 1%
where the time goes in v3:
time: 134 us; the launch traced here: 133 us
  blocking collectives  68.2 us (51%)
  starting transfers between devices  42.3 us (32%)
  waiting for transfers between devices  11.1 us (8%)
  Pallas kernels  9.62 us (7%)
    all_to_all x1, blocking collectives, per_device(): lax.all_to_all(total.reshape(-1, 2, LANES), (*EP, 'tp'), 0, 0, tiled=True)  37.4 us
    all_to_all x1, blocking collectives, per_device(): partial = lax.all_to_all(partial, 'tp', 0, 0, tiled=True)  30.8 us
    all_to_all x1, starting transfers between devices, per_device(): lax.all_to_all(outgoing.reshape(-1, 2, LANES), EP, 0, 0, tiled=True)  20 us
    ppermute x5, starting transfers between devices, swap(): return lax.ppermute(shard, PAIR, [(0, 1), (1, 0)])  11.5 us
    ppermute x3, starting transfers between devices, per_device(): packs.append(lax.ppermute(packed, 'tp', ring))  10.9 us
    all_to_all x1, waiting for transfers between devices, per_device(): lax.all_to_all(outgoing.reshape(-1, 2, LANES), EP, 0, 0, tiled=True)  9.96 us
    pallas_call x1, Pallas kernels, per_device(): pl.pallas_call(share_kernel, in_specs=[VMEM] * 4 + [ANY] * (2 * members -...  4.18 us
    pallas_call x1, Pallas kernels, per_device(): pl.pallas_call(attend_kernel, in_specs=[SMEM, SMEM] + [VMEM] * 4 + [ANY]...  3.82 us
  transfers between devices with their start and end apart: 9, of which 2 were waited for; matrix products, arithmetic and copies ran while one was open for 0% of the time, Pallas kernels for 1%

profile of v3, /device:TPU:1, one launch (start us, length us, event | category | flops | bytes accessed | tf_op | source)
XLA Modules:
  0.0 133.4 jit_solution(6819144564691492356)
XLA Ops:
  0.7 3.8 %attend.1 = (bf16[4,8,1024]{2,1,0:T(8,128)(2,1)S(1)}, bf16[3136,128]{1,0:T(8,128)(2,1)S(1)}) custom-call(s32[8]{0:T(128)} %lengths.1, f32[1]{0:T(128)S(6)} %copy.27.forget_bias, bf16[1024]{0:T(1024)(128)(2,1)} %norm_gain.1, bf16[128]{0:T(256)(128)(2,1)} %query_gain.1, bf16[128]{0:T(256)(128)(2,1)} %key_gain.1, bf16[1,1024]{1,0:T(2,128)(2,1)} %bitcast.31, ...), custom_call_target="tpu_custom_call" | custom-call | tf_op jit(solution)/shard_map/attend/pallas_call | solution.py:329
  4.5 5.6 %collective-permute-start.3 = (bf16[3136,128]{1,0:T(8,128)(2,1)S(1)}, bf16[3136,128]{1,0:T(8,128)(2,1)}, u32[]{:S(2)}, u32[]{:S(2)}) collective-permute-start(bf16[3136,128]{1,0:T(8,128)(2,1)S(1)} %get-tuple-element.12.refs_0_), channel_id=1, source_target_pairs={{0,2},{1,3},{2,0},{3,1},{4,6},{5,7},{6,4},{7,5},{8,10},{9,11},{10,... | collective-permute-start | bytes 2408456 | tf_op jit(solution)/shard_map/ppermute | solution.py:357
  10.1 2.7 %collective-permute-start.2 = (bf16[3136,128]{1,0:T(8,128)(2,1)S(1)}, bf16[3136,128]{1,0:T(8,128)(2,1)}, u32[]{:S(2)}, u32[]{:S(2)}) collective-permute-start(bf16[3136,128]{1,0:T(8,128)(2,1)S(1)} %get-tuple-element.12.refs_0_), channel_id=1, source_target_pairs={{0,3},{1,0},{2,1},{3,2},{4,7},{5,4},{6,5},{7,6},{8,11},{9,8},{10,9... | collective-permute-start | bytes 2408456 | tf_op jit(solution)/shard_map/ppermute | solution.py:357
  12.8 2.6 %collective-permute-start.1 = (bf16[3136,128]{1,0:T(8,128)(2,1)S(1)}, bf16[3136,128]{1,0:T(8,128)(2,1)}, u32[]{:S(2)}, u32[]{:S(2)}) collective-permute-start(bf16[3136,128]{1,0:T(8,128)(2,1)S(1)} %get-tuple-element.12.refs_0_), channel_id=1, source_target_pairs={{0,1},{1,2},{2,3},{3,0},{4,5},{5,6},{6,7},{7,4},{8,9},{9,10},{10,1... | collective-permute-start | bytes 2408456 | tf_op jit(solution)/shard_map/ppermute | solution.py:357
  15.4 30.8 %all_to_all.15.partial = bf16[4,8,1024]{2,1,0:T(8,128)(2,1)S(1)} all-to-all(bf16[4,8,1024]{2,1,0:T(8,128)(2,1)S(1)} %get-tuple-element.9), channel_id=1, replica_groups=mesh['ep_0'=16,'ep_1'=4,'ep_2'=2,'tp'=4] {'tp'}, dimensions={0} | all-to-all | bytes 131072 | tf_op jit(solution)/shard_map/all_to_all | solution.py:353
  46.2 1.6 %rows.1 = (f32[8,256]{1,0:T(8,128)}, bf16[1280,128]{1,0:T(8,128)(2,1)}) custom-call(bf16[4,8,1024]{2,1,0:T(8,128)(2,1)S(1)} %all_to_all.15.partial, bf16[8,1024]{1,0:T(8,128)(2,1)} %tokens.1, bf16[1024]{0:T(1024)(128)(2,1)} %ffn_gain.1, s32[2,8]{1,0:T(2,128)} %bitcast.32, f32[2,8]{1,0:T(2,128)} %bitcast.33), custom_call_target="tpu_custom_call" | custom-call | tf_op jit(solution)/shard_map/rows/pallas_call | solution.py:364
  47.8 0.0 copy-start.4
  47.8 0.0 copy-start.1
  47.8 0.0 copy-start.2
  47.8 20.0 %all-to-all-start.1 = ((bf16[640,2,128]{2,1,0:T(2,128)(2,1)}), bf16[640,2,128]{2,1,0:T(2,128)(2,1)S(1)}, u32[]{:S(2)}, u32[]{:S(2)}) async-start(bf16[640,2,128]{2,1,0:T(2,128)(2,1)} %bitcast.8), calls=%async_computation.1 | async-start | bytes 655360 | tf_op jit(solution)/shard_map/all_to_all | solution.py:374
  67.8 2.8 %collective-permute-start.4 = (bf16[3136,128]{1,0:T(8,128)(2,1)S(1)}, bf16[3136,128]{1,0:T(8,128)(2,1)S(1)}, u32[]{:S(2)}, u32[]{:S(2)}) collective-permute-start(bf16[3136,128]{1,0:T(8,128)(2,1)S(1)} %get-tuple-element.12.refs_0_), channel_id=1, source_target_pairs={{0,4},{4,0},{1,5},{5,1},{2,6},{6,2},{3,7},{7,3},{8,12},{12,8},{9,1... | collective-permute-start | bytes 2408456 | tf_op jit(solution)/shard_map/ppermute | solution.py:22
  70.6 0.0 collective-permute-done.3.refs_3_
  70.6 1.9 %collective-permute-start.7 = (bf16[3136,128]{1,0:T(8,128)(2,1)}, bf16[3136,128]{1,0:T(8,128)(2,1)}, u32[]{:S(2)}, u32[]{:S(2)}) collective-permute-start(bf16[3136,128]{1,0:T(8,128)(2,1)} %collective-permute-done.3.refs_3_), channel_id=1, source_target_pairs={{0,4},{4,0},{1,5},{5,1},{2,6},{6,2},{3,7},{7,3},{8,12},{12,8},{9,1... | collective-permute-start | bytes 2408456 | tf_op jit(solution)/shard_map/ppermute | solution.py:22
  72.5 0.0 collective-permute-done.2.refs_2_
  72.5 2.4 %collective-permute-start.6 = (bf16[3136,128]{1,0:T(8,128)(2,1)}, bf16[3136,128]{1,0:T(8,128)(2,1)}, u32[]{:S(2)}, u32[]{:S(2)}) collective-permute-start(bf16[3136,128]{1,0:T(8,128)(2,1)} %collective-permute-done.2.refs_2_), channel_id=1, source_target_pairs={{0,4},{4,0},{1,5},{5,1},{2,6},{6,2},{3,7},{7,3},{8,12},{12,8},{9,1... | collective-permute-start | bytes 2408456 | tf_op jit(solution)/shard_map/ppermute | solution.py:22
  75.0 0.0 collective-permute-done.1.refs_1_
  75.0 1.9 %collective-permute-start.5 = (bf16[3136,128]{1,0:T(8,128)(2,1)}, bf16[3136,128]{1,0:T(8,128)(2,1)}, u32[]{:S(2)}, u32[]{:S(2)}) collective-permute-start(bf16[3136,128]{1,0:T(8,128)(2,1)} %collective-permute-done.1.refs_1_), channel_id=1, source_target_pairs={{0,4},{4,0},{1,5},{5,1},{2,6},{6,2},{3,7},{7,3},{8,12},{12,8},{9,1... | collective-permute-start | bytes 2408456 | tf_op jit(solution)/shard_map/ppermute | solution.py:22
  76.9 0.0 copy-done.4
  76.9 0.0 copy-done.1
  76.9 0.0 copy-done.2
  77.0 2.4 %collective-permute-start = (bf16[128,1024]{1,0:T(8,128)(2,1)S(1)}, bf16[128,1024]{1,0:T(8,128)(2,1)S(1)}, u32[]{:S(2)}, u32[]{:S(2)}) collective-permute-start(bf16[128,1024]{1,0:T(8,128)(2,1)S(1)} %fusion.4.front), channel_id=1, source_target_pairs={{0,4},{4,0},{1,5},{5,1},{2,6},{6,2},{3,7},{7,3},{8,12},{12,8},{9,1... | collective-permute-start | bytes 786440 | tf_op jit(solution)/shard_map/ppermute | solution.py:22
  79.4 1.1 collective-permute-done.pair_front
  80.5 0.0 collective-permute-done.4.refs_4_
  80.5 0.0 copy-start
  80.5 10.0 %all-to-all-done.1 = bf16[640,2,128]{2,1,0:T(2,128)(2,1)S(1)} async-done(((bf16[640,2,128]{2,1,0:T(2,128)(2,1)}), bf16[640,2,128]{2,1,0:T(2,128)(2,1)S(1)}, u32[]{:S(2)}, u32[]{:S(2)}) %all-to-all-start.1) | async-done | bytes 327712 | tf_op jit(solution)/shard_map/all_to_all | solution.py:374
  90.5 0.0 collective-permute-done.7.refs_7_
  90.5 0.0 collective-permute-done.6.refs_6_
  90.5 0.0 collective-permute-done.5.refs_5_
  90.5 0.0 copy-done
  90.5 4.2 %share.1 = bf16[1024,128]{1,0:T(8,128)(2,1)S(1)} custom-call(bf16[1280,128]{1,0:T(8,128)(2,1)S(1)} %bitcast.20, bf16[128,1024]{1,0:T(8,128)(2,1)S(1)} %fusion.4.front, bf16[128,1024]{1,0:T(8,128)(2,1)S(1)} %collective-permute-done.pair_front, bf16[3136,128]{1,0:T(8,128)(2,1)S(1)} %get-tuple-element.12.refs_0_, ...), custom_call_target="tpu_custom_call" | custom-call | tf_op jit(solution)/shard_map/share/pallas_call | solution.py:380
  94.7 37.4 %all_to_all.16 = bf16[512,2,128]{2,1,0:T(2,128)(2,1)S(1)} all-to-all(bf16[512,2,128]{2,1,0:T(2,128)(2,1)S(1)} %bitcast.21), channel_id=1, replica_groups=mesh['ep_0'=16,'ep_1'=4,'ep_2'=2,'tp'=4] {'ep_0','ep_1','ep_2','tp'}, dimensions={0} | all-to-all | bytes 524288 | tf_op jit(solution)/shard_map/all_to_all | solution.py:398
  132.1 0.0 copy-start.3
  132.1 0.2 convert_reduce_fusion
  132.4 0.5 copy-done.3
  132.8 0.6 fusion.5
  (2 shorter events, 0.0 us)
Async XLA Ops:
  4.5 66.1 %collective-permute-start.3 = (bf16[3136,128]{1,0:T(8,128)(2,1)S(1)}, bf16[3136,128]{1,0:T(8,128)(2,1)}, u32[]{:S(2)}, u32[]{:S(2)}) collective-permute-start(bf16[3136,128]{1,0:T(8,128)(2,1)S(1)} %get-tuple-element.12.refs_0_), channel_id=1, source_target_pairs={{0,2},{1,3},{2,0},{3,1},{4,6},{5,7},{6,4},{7,5},{8,10},{9,11},{10,... | collective-permute-start | bytes 2408456 | tf_op jit(solution)/shard_map/ppermute | solution.py:357
  10.1 62.4 %collective-permute-start.2 = (bf16[3136,128]{1,0:T(8,128)(2,1)S(1)}, bf16[3136,128]{1,0:T(8,128)(2,1)}, u32[]{:S(2)}, u32[]{:S(2)}) collective-permute-start(bf16[3136,128]{1,0:T(8,128)(2,1)S(1)} %get-tuple-element.12.refs_0_), channel_id=1, source_target_pairs={{0,3},{1,0},{2,1},{3,2},{4,7},{5,4},{6,5},{7,6},{8,11},{9,8},{10,9... | collective-permute-start | bytes 2408456 | tf_op jit(solution)/shard_map/ppermute | solution.py:357
  12.8 62.1 %collective-permute-start.1 = (bf16[3136,128]{1,0:T(8,128)(2,1)S(1)}, bf16[3136,128]{1,0:T(8,128)(2,1)}, u32[]{:S(2)}, u32[]{:S(2)}) collective-permute-start(bf16[3136,128]{1,0:T(8,128)(2,1)S(1)} %get-tuple-element.12.refs_0_), channel_id=1, source_target_pairs={{0,1},{1,2},{2,3},{3,0},{4,5},{5,6},{6,7},{7,4},{8,9},{9,10},{10,1... | collective-permute-start | bytes 2408456 | tf_op jit(solution)/shard_map/ppermute | solution.py:357
  47.8 29.1 %copy-start.4 = (bf16[1024]{0:T(1024)(128)(2,1)S(1)}, bf16[1024]{0:T(1024)(128)(2,1)}, u32[]{:S(2)}) copy-start(bf16[1024]{0:T(1024)(128)(2,1)} %param.39) | copy-start | bytes 6148
  47.8 29.1 %copy-start.1 = (bf16[1024,32]{0,1:T(8,128)(2,1)S(1)}, bf16[1024,32]{0,1:T(8,128)(2,1)}, u32[]{:S(2)}) copy-start(bf16[1024,32]{0,1:T(8,128)(2,1)} %param.41) | copy-start | bytes 196612
  47.8 29.1 %copy-start.2 = (bf16[1024,32]{0,1:T(8,128)(2,1)S(1)}, bf16[1024,32]{0,1:T(8,128)(2,1)}, u32[]{:S(2)}) copy-start(bf16[1024,32]{0,1:T(8,128)(2,1)} %param.40) | copy-start | bytes 196612
  47.8 42.7 %all-to-all-start.1 = ((bf16[640,2,128]{2,1,0:T(2,128)(2,1)}), bf16[640,2,128]{2,1,0:T(2,128)(2,1)S(1)}, u32[]{:S(2)}, u32[]{:S(2)}) async-start(bf16[640,2,128]{2,1,0:T(2,128)(2,1)} %bitcast.8), calls=%async_computation.1 | async-start | bytes 655360 | tf_op jit(solution)/shard_map/all_to_all | solution.py:374
  67.8 12.7 %collective-permute-start.4 = (bf16[3136,128]{1,0:T(8,128)(2,1)S(1)}, bf16[3136,128]{1,0:T(8,128)(2,1)S(1)}, u32[]{:S(2)}, u32[]{:S(2)}) collective-permute-start(bf16[3136,128]{1,0:T(8,128)(2,1)S(1)} %get-tuple-element.12.refs_0_), channel_id=1, source_target_pairs={{0,4},{4,0},{1,5},{5,1},{2,6},{6,2},{3,7},{7,3},{8,12},{12,8},{9,1... | collective-permute-start | bytes 2408456 | tf_op jit(solution)/shard_map/ppermute | solution.py:22
  70.6 19.9 %collective-permute-start.7 = (bf16[3136,128]{1,0:T(8,128)(2,1)}, bf16[3136,128]{1,0:T(8,128)(2,1)}, u32[]{:S(2)}, u32[]{:S(2)}) collective-permute-start(bf16[3136,128]{1,0:T(8,128)(2,1)} %collective-permute-done.3.refs_3_), channel_id=1, source_target_pairs={{0,4},{4,0},{1,5},{5,1},{2,6},{6,2},{3,7},{7,3},{8,12},{12,8},{9,1... | collective-permute-start | bytes 2408456 | tf_op jit(solution)/shard_map/ppermute | solution.py:22
  72.5 18.0 %collective-permute-start.6 = (bf16[3136,128]{1,0:T(8,128)(2,1)}, bf16[3136,128]{1,0:T(8,128)(2,1)}, u32[]{:S(2)}, u32[]{:S(2)}) collective-permute-start(bf16[3136,128]{1,0:T(8,128)(2,1)} %collective-permute-done.2.refs_2_), channel_id=1, source_target_pairs={{0,4},{4,0},{1,5},{5,1},{2,6},{6,2},{3,7},{7,3},{8,12},{12,8},{9,1... | collective-permute-start | bytes 2408456 | tf_op jit(solution)/shard_map/ppermute | solution.py:22
  75.0 15.5 %collective-permute-start.5 = (bf16[3136,128]{1,0:T(8,128)(2,1)}, bf16[3136,128]{1,0:T(8,128)(2,1)}, u32[]{:S(2)}, u32[]{:S(2)}) collective-permute-start(bf16[3136,128]{1,0:T(8,128)(2,1)} %collective-permute-done.1.refs_1_), channel_id=1, source_target_pairs={{0,4},{4,0},{1,5},{5,1},{2,6},{6,2},{3,7},{7,3},{8,12},{12,8},{9,1... | collective-permute-start | bytes 2408456 | tf_op jit(solution)/shard_map/ppermute | solution.py:22
  77.0 3.6 %collective-permute-start = (bf16[128,1024]{1,0:T(8,128)(2,1)S(1)}, bf16[128,1024]{1,0:T(8,128)(2,1)S(1)}, u32[]{:S(2)}, u32[]{:S(2)}) collective-permute-start(bf16[128,1024]{1,0:T(8,128)(2,1)S(1)} %fusion.4.front), channel_id=1, source_target_pairs={{0,4},{4,0},{1,5},{5,1},{2,6},{6,2},{3,7},{7,3},{8,12},{12,8},{9,1... | collective-permute-start | bytes 786440 | tf_op jit(solution)/shard_map/ppermute | solution.py:22
  80.5 10.0 %copy-start = (bf16[3136,128]{1,0:T(8,128)(2,1)}, bf16[3136,128]{1,0:T(8,128)(2,1)S(1)}, u32[]{:S(2)}) copy-start(bf16[3136,128]{1,0:T(8,128)(2,1)S(1)} %collective-permute-done.4.refs_4_) | copy-start | bytes 2408452
  132.1 0.7 copy-start.3

commit v4 on v3

--- a/solution.py
+++ b/solution.py
@@ -35,8 +35,13 @@
     return pltpu.with_memory_space_constraint(values, pltpu.VMEM)
 
 
-def ring_steps(members):
-    return (0, 1, members - 1, *range(2, members - 1))
+def shifted(shard, step, members):
+    pairs = []
+    for core, sign in enumerate((1, -1)):
+        for t in range(members):
+            target = (t + sign * step) % members
+            pairs.append((core * members + t, core * members + target))
+    return lax.ppermute(shard, (PAIR, "tp"), pairs)
 
 
 def wide_dot(left, right):
@@ -207,15 +212,14 @@
         outgoing[i * step : (i + 1) * step, :] = pattern
 
 
-def share_kernel(rows, front, pair_front, *refs):
+def share_kernel(rows, front, pair_front, packed, *refs):
     sources, (out, wide, narrow, columns, staged, sems) = refs[:-6], refs[-6:]
-    members = len(sources) // 2
-    packs, arrivals = [sources[0]], [None]
-    for i, source in enumerate(sources[1:]):
-        copy = pltpu.make_async_copy(source, staged.at[i], sems.at[i])
-        copy.start()
-        packs.append(staged.at[i])
-        arrivals.append(copy)
+    copies = []
+    for i, source in enumerate(sources):
+        copies.append(pltpu.make_async_copy(source, staged.at[i], sems.at[i]))
+        copies[-1].start()
+    packs = [packed] + [staged.at[i] for i in range(len(sources))]
+    members = len(packs) // 2
     member = lax.axis_index("tp")
     core = lax.axis_index(PAIR)
     experts = (lax.axis_index(EP), lax.axis_index(EP) + 1 - 2 * core)
@@ -223,11 +227,19 @@
     count = narrow.shape[0]
     blocks = width // LANES
     stride = blocks + NOTE_ROWS
+    lines = lax.axis_size("ep_1") * 2
+    depth = count // lines
     wide[...] = rows[...].astype(jnp.float32)
-    for k in range(blocks):
-        piece = wide[pl.ds(k, count, stride=stride), :]
-        narrow[:, k * LANES : (k + 1) * LANES] = piece.astype(jnp.bfloat16)
-    marks = wide[pl.ds(blocks, count, stride=stride), :]
+    marks = []
+    for line in range(lines):
+        for k in range(blocks + 1):
+            piece = wide[pl.ds(line * stride + k, depth, stride=lines * stride), :]
+            if k < blocks:
+                at = (slice(line * depth, (line + 1) * depth), slice(k * LANES, (k + 1) * LANES))
+                narrow[at] = piece.astype(jnp.bfloat16)
+            else:
+                marks.append(piece)
+    marks = jnp.concatenate(marks, axis=0)
     values = narrow[...]
     down_start = 2 * width
     shared_start = down_start + blocks * LANES
@@ -250,22 +262,23 @@
             norm_weight = marks[:, 2 + j : 3 + j] + marks[:, 4 + j : 5 + j]
             weight = weight + jnp.where(chosen, norm_weight, 0.0)
         for s in range(members):
-            pack = packs[side * members + s]
-            if arrivals[side * members + s] is not None:
-                arrivals[side * members + s].wait()
-            gate = wide_dot(values, pack[:width, :])
-            up = wide_dot(values, pack[width : 2 * width, :])
+            at = side * members + s
+            if at:
+                copies[at - 1].wait()
+            gate = wide_dot(values, packs[at][:width, :])
+            up = wide_dot(values, packs[at][width : 2 * width, :])
             hidden.append((weight, (silu(gate) * up).astype(jnp.bfloat16)))
     shared = [silu(pre[:, :units]) * pre[:, units : 2 * units] for pre in fronts]
     shared = [each.astype(jnp.bfloat16) for each in shared]
-    for s, step in enumerate(ring_steps(members)):
-        origin = (member + members - step) % members
+    ahead = jnp.where(core == 0, members - 1, 1)
+    origins = (0, ahead, members - ahead, 2)
+    for s, pair in enumerate((0, 2, 1, 3)):
+        origin = (member + origins[s]) % members
         for k in range(per_member):
             rows_of = pl.ds(shared_start + k * units, units)
             dense = wide_dot(shared[0], packs[s][rows_of, :])
-            dense = dense + wide_dot(shared[1], packs[members + s][rows_of, :])
+            dense = dense + wide_dot(shared[1], packs[members + pair][rows_of, :])
             columns[origin * per_member + k] = mix_gate * dense
-
     for k in range(blocks):
         total = columns[k]
         for side in range(2):
@@ -276,8 +289,43 @@
                 pack = packs[side * members + s]
                 routed = routed + wide_dot(each, pack[first : first + LANES, :])
             total = total + weight * routed
-        wide[pl.ds(k, count, stride=blocks), :] = total
+        for line in range(lines):
+            first = line // 2 * depth * 2 * blocks + k // per_member * depth * 2 * per_member
+            first = first + line % 2 * per_member + k % per_member
+            piece = total[line * depth : (line + 1) * depth]
+            wide[pl.ds(first, depth, stride=2 * per_member), :] = piece
     out[...] = wide[: count * blocks, :].astype(jnp.bfloat16)
+
+
+def fold_kernel(parts, out, wide, small):
+    sources = lax.axis_size("ep_1")
+    members = lax.axis_size("tp")
+    rows = parts.shape[0] // sources
+    wide[...] = parts[...].astype(jnp.float32)
+    total = wide[:rows, :]
+    for i in range(1, sources):
+        total = total + wide[i * rows : (i + 1) * rows, :]
+    wide[:rows, :] = total
+    halves = 2
+    count = rows // members // halves
+    for t in range(members):
+        for j in range(halves):
+            piece = wide[pl.ds(t * count * halves + j, count, stride=halves), :]
+            small[pl.ds(t * halves + j, count, stride=members * halves), :] = piece
+    out[...] = small[...].astype(jnp.bfloat16)
+
+
+def finish_kernel(parts, residual, out, small):
+    rows = small.shape[0]
+    total = parts[:rows, :].astype(jnp.float32)
+    for i in range(1, parts.shape[0] // rows):
+        total = total + parts[i * rows : (i + 1) * rows, :].astype(jnp.float32)
+    small[...] = total
+    seqs = residual.shape[0]
+    for j in range(rows // seqs):
+        piece = small[pl.ds(j, seqs, stride=rows // seqs), :]
+        columns = slice(j * LANES, (j + 1) * LANES)
+        out[:, columns] = (residual[:, columns] + piece).astype(jnp.bfloat16)
 
 
 def per_device(
@@ -351,10 +399,10 @@
         shared_down,
     )
     partial = lax.all_to_all(partial, "tp", 0, 0, tiled=True)
-    packs = [packed]
-    for step in ring_steps(members)[1:]:
-        ring = [(i, (i + step) % members) for i in range(members)]
-        packs.append(lax.ppermute(packed, "tp", ring))
+    ahead = shifted(packed, 1, members)
+    behind = shifted(packed, -1, members)
+    across = shifted(ahead, 1, members)
+    packs = [packed, ahead, behind, across]
 
     front = [shared_gate.T, shared_up.T, mix_weight[None]]
     front = jnp.concatenate(front, axis=0)
@@ -366,11 +414,11 @@
         in_specs=[VMEM] * 5,
         out_specs=[VMEM, VMEM],
         out_shape=[
-            jax.ShapeDtypeStruct((seqs, width // members), jnp.float32),
+            pltpu.VMEM((seqs, width // members), jnp.float32),
             pltpu.VMEM((sub_rows, LANES), jnp.bfloat16),
         ],
         name="rows",
-    )(in_vmem(partial), tokens, ffn_gain, routes.T, route_weights.T)
+    )(*map(in_vmem, (partial, tokens, ffn_gain, routes.T, route_weights.T)))
     own_rows = lax.all_to_all(outgoing.reshape(-1, 2, LANES), EP, 0, 0, tiled=True)
 
     pair_front = swap(front)
@@ -395,10 +443,29 @@
         *packs[1:],
         *pair_packs,
     )
-    returned = lax.all_to_all(total.reshape(-1, 2, LANES), (*EP, "tp"), 0, 0, tiled=True)
-    returned = returned.reshape(peers // 2, seqs, -1, LANES).astype(jnp.float32)
-    returned = jnp.sum(returned, axis=0).reshape(seqs, -1)
-    return (residual + returned).astype(jnp.bfloat16)
+    parts = lax.all_to_all(total.reshape(-1, 2, LANES), ("ep_1", "tp"), 0, 0, tiled=True)
+    parts = parts.reshape(-1, LANES)
+    rows = parts.shape[0] // lax.axis_size("ep_1")
+    parts = pl.pallas_call(
+        fold_kernel,
+        in_specs=[VMEM],
+        out_specs=VMEM,
+        out_shape=pltpu.VMEM((rows, LANES), jnp.bfloat16),
+        scratch_shapes=[
+            pltpu.VMEM(parts.shape, jnp.float32),
+            pltpu.VMEM((rows, LANES), jnp.float32),
+        ],
+        name="fold",
+    )(in_vmem(parts))
+    parts = lax.all_to_all(parts.reshape(-1, 2, LANES), ("ep_0", PAIR), 0, 0, tiled=True)
+    return pl.pallas_call(
+        finish_kernel,
+        in_specs=[VMEM] * 2,
+        out_specs=VMEM,
+        out_shape=jax.ShapeDtypeStruct((seqs, width // members), jnp.bfloat16),
+        scratch_shapes=[pltpu.VMEM((seqs * width // members // LANES, LANES), jnp.float32)],
+        name="finish",
+    )(in_vmem(parts.reshape(-1, LANES)), in_vmem(residual))
 
 
 def solution(mesh):

time: 134 us -> 125 us (0.933)
  blocking collectives: 68.2 us -> 43.8 us
  starting transfers between devices: 42.3 us -> 51.3 us
  waiting for transfers between devices: 11.1 us -> 18.3 us
    all_to_all x1, blocking collectives: 30.8 us -> 12.4 us  [per_device(): partial = lax.all_to_all(partial, 'tp', 0, 0, tiled=True)]
    all_to_all x1, starting transfers between devices: 20 us -> 27.3 us  [per_device(): lax.all_to_all(outgoing.reshape(-1, 2, LANES), EP, 0, 0, tiled=True)]
    ppermute x3, waiting for transfers between devices: 0.01 us -> 7.16 us  [shifted(): return lax.ppermute(shard, (PAIR, 'tp'), pairs)]
    all_to_all x1 -> x2, blocking collectives: 37.4 us -> 31.4 us  [the longest x1 17.6 us: per_device(): lax.all_to_all(parts.reshape(-1, 2, LANES), ('ep_0', PAIR), 0, 0, tiled=T...]
    ppermute x3, starting transfers between devices: 10.9 us -> 12.5 us  [shifted(): return lax.ppermute(shard, (PAIR, 'tp'), pairs)]
  transfers between devices with their start and end apart: 9 -> 9, of which waited for: 2 -> 3; matrix products, arithmetic and copies ran while one was open for 0% -> 0% of each run, Pallas kernels for 1% -> 1%
where the time goes in v4:
time: 125 us
  starting transfers between devices  51.3 us (41%)
  blocking collectives  43.8 us (35%)
  waiting for transfers between devices  18.3 us (15%)
  Pallas kernels  9.74 us (8%)
    all_to_all x1, starting transfers between devices, per_device(): lax.all_to_all(outgoing.reshape(-1, 2, LANES), EP, 0, 0, tiled=True)  27.3 us
    all_to_all x1, blocking collectives, per_device(): lax.all_to_all(parts.reshape(-1, 2, LANES), ('ep_0', PAIR), 0, 0, tiled=T...  17.6 us
    all_to_all x1, blocking collectives, per_device(): lax.all_to_all(total.reshape(-1, 2, LANES), ('ep_1', 'tp'), 0, 0, tiled=T...  13.8 us
    ppermute x3, starting transfers between devices, shifted(): return lax.ppermute(shard, (PAIR, 'tp'), pairs)  12.5 us
    all_to_all x1, blocking collectives, per_device(): partial = lax.all_to_all(partial, 'tp', 0, 0, tiled=True)  12.4 us
    ppermute x5, starting transfers between devices, swap(): return lax.ppermute(shard, PAIR, [(0, 1), (1, 0)])  11.5 us
    all_to_all x1, waiting for transfers between devices, per_device(): lax.all_to_all(outgoing.reshape(-1, 2, LANES), EP, 0, 0, tiled=True)  9.97 us
    ppermute x3, waiting for transfers between devices, shifted(): return lax.ppermute(shard, (PAIR, 'tp'), pairs)  7.16 us
  transfers between devices with their start and end apart: 9, of which 3 were waited for; matrix products, arithmetic and copies ran while one was open for 0% of the time, Pallas kernels for 1%

profile of v4, /device:TPU:1, one launch (start us, length us, event | category | flops | bytes accessed | tf_op | source)
XLA Modules:
  0.0 124.7 jit_solution(9151362450684052878)
XLA Ops:
  0.7 3.8 %attend.1 = (bf16[4,8,1024]{2,1,0:T(8,128)(2,1)S(1)}, bf16[3136,128]{1,0:T(8,128)(2,1)S(1)}) custom-call(s32[8]{0:T(128)} %lengths.1, f32[1]{0:T(128)S(6)} %copy.25.forget_bias, bf16[1024]{0:T(1024)(128)(2,1)} %norm_gain.1, bf16[128]{0:T(256)(128)(2,1)} %query_gain.1, bf16[128]{0:T(256)(128)(2,1)} %key_gain.1, bf16[1,1024]{1,0:T(2,128)(2,1)} %bitcast.30, ...), custom_call_target="tpu_custom_call" | custom-call | tf_op jit(solution)/shard_map/attend/pallas_call | solution.py:377
  4.5 5.5 %collective-permute-start.1 = (bf16[3136,128]{1,0:T(8,128)(2,1)S(1)}, bf16[3136,128]{1,0:T(8,128)(2,1)}, u32[]{:S(2)}, u32[]{:S(2)}) collective-permute-start(bf16[3136,128]{1,0:T(8,128)(2,1)S(1)} %get-tuple-element.11.packed), channel_id=1, source_target_pairs={{0,1},{1,2},{2,3},{3,0},{4,7},{5,4},{6,5},{7,6},{8,9},{9,10},{10,1... | collective-permute-start | bytes 2408456 | tf_op jit(solution)/shard_map/ppermute | solution.py:44
  9.9 1.9 %collective-permute-start.2 = (bf16[3136,128]{1,0:T(8,128)(2,1)S(1)}, bf16[3136,128]{1,0:T(8,128)(2,1)}, u32[]{:S(2)}, u32[]{:S(2)}) collective-permute-start(bf16[3136,128]{1,0:T(8,128)(2,1)S(1)} %get-tuple-element.11.packed), channel_id=1, source_target_pairs={{0,3},{1,0},{2,1},{3,2},{4,5},{5,6},{6,7},{7,4},{8,11},{9,8},{10,9... | collective-permute-start | bytes 2408456 | tf_op jit(solution)/shard_map/ppermute | solution.py:44
  11.9 7.2 %collective-permute-done.1.refs_0_ = bf16[3136,128]{1,0:T(8,128)(2,1)} collective-permute-done((bf16[3136,128]{1,0:T(8,128)(2,1)S(1)}, bf16[3136,128]{1,0:T(8,128)(2,1)}, u32[]{:S(2)}, u32[]{:S(2)}) %collective-permute-start.1) | collective-permute-done | bytes 802848 | tf_op jit(solution)/shard_map/ppermute | solution.py:44
  19.0 5.1 %collective-permute-start.3 = (bf16[3136,128]{1,0:T(8,128)(2,1)}, bf16[3136,128]{1,0:T(8,128)(2,1)}, u32[]{:S(2)}, u32[]{:S(2)}) collective-permute-start(bf16[3136,128]{1,0:T(8,128)(2,1)} %collective-permute-done.1.refs_0_), channel_id=1, source_target_pairs={{0,1},{1,2},{2,3},{3,0},{4,7},{5,4},{6,5},{7,6},{8,9},{9,10},{10,1... | collective-permute-start | bytes 2408456 | tf_op jit(solution)/shard_map/ppermute | solution.py:44
  24.2 0.0 copy-start
  24.2 0.0 copy-start.3
  24.2 12.4 %all_to_all.20.partial = bf16[4,8,1024]{2,1,0:T(8,128)(2,1)S(1)} all-to-all(bf16[4,8,1024]{2,1,0:T(8,128)(2,1)S(1)} %get-tuple-element.9), channel_id=1, replica_groups=mesh['ep_0'=16,'ep_1'=4,'ep_2'=2,'tp'=4] {'tp'}, dimensions={0} | all-to-all | bytes 131072 | tf_op jit(solution)/shard_map/all_to_all | solution.py:401
  36.6 0.0 copy-start.1
  36.6 0.0 copy-start.2
  36.6 0.0 copy-done
  36.6 0.0 copy-done.3
  36.6 0.7 copy-done.1
  37.3 0.0 copy-done.2
  37.3 0.9 rows.1
  38.2 0.0 copy-start.7
  38.2 0.0 copy-start.5
  38.2 0.0 copy-start.6
  38.2 27.3 %all-to-all-start.1 = ((bf16[640,2,128]{2,1,0:T(2,128)(2,1)}), bf16[640,2,128]{2,1,0:T(2,128)(2,1)S(1)}, u32[]{:S(2)}, u32[]{:S(2)}) async-start(bf16[640,2,128]{2,1,0:T(2,128)(2,1)} %bitcast.8), calls=%async_computation.1 | async-start | bytes 655360 | tf_op jit(solution)/shard_map/all_to_all | solution.py:422
  65.5 2.8 %collective-permute-start.4 = (bf16[3136,128]{1,0:T(8,128)(2,1)S(1)}, bf16[3136,128]{1,0:T(8,128)(2,1)S(1)}, u32[]{:S(2)}, u32[]{:S(2)}) collective-permute-start(bf16[3136,128]{1,0:T(8,128)(2,1)S(1)} %get-tuple-element.11.packed), channel_id=1, source_target_pairs={{0,4},{4,0},{1,5},{5,1},{2,6},{6,2},{3,7},{7,3},{8,12},{12,8},{9,1... | collective-permute-start | bytes 2408456 | tf_op jit(solution)/shard_map/ppermute | solution.py:22
  68.3 1.9 %collective-permute-start.5 = (bf16[3136,128]{1,0:T(8,128)(2,1)}, bf16[3136,128]{1,0:T(8,128)(2,1)}, u32[]{:S(2)}, u32[]{:S(2)}) collective-permute-start(bf16[3136,128]{1,0:T(8,128)(2,1)} %collective-permute-done.1.refs_0_), channel_id=1, source_target_pairs={{0,4},{4,0},{1,5},{5,1},{2,6},{6,2},{3,7},{7,3},{8,12},{12,8},{9,1... | collective-permute-start | bytes 2408456 | tf_op jit(solution)/shard_map/ppermute | solution.py:22
  70.3 0.0 collective-permute-done.2.refs_1_
  70.3 2.4 %collective-permute-start.6 = (bf16[3136,128]{1,0:T(8,128)(2,1)}, bf16[3136,128]{1,0:T(8,128)(2,1)}, u32[]{:S(2)}, u32[]{:S(2)}) collective-permute-start(bf16[3136,128]{1,0:T(8,128)(2,1)} %collective-permute-done.2.refs_1_), channel_id=1, source_target_pairs={{0,4},{4,0},{1,5},{5,1},{2,6},{6,2},{3,7},{7,3},{8,12},{12,8},{9,1... | collective-permute-start | bytes 2408456 | tf_op jit(solution)/shard_map/ppermute | solution.py:22
  72.7 0.0 collective-permute-done.3.refs_2_
  72.7 1.9 %collective-permute-start.7 = (bf16[3136,128]{1,0:T(8,128)(2,1)}, bf16[3136,128]{1,0:T(8,128)(2,1)}, u32[]{:S(2)}, u32[]{:S(2)}) collective-permute-start(bf16[3136,128]{1,0:T(8,128)(2,1)} %collective-permute-done.3.refs_2_), channel_id=1, source_target_pairs={{0,4},{4,0},{1,5},{5,1},{2,6},{6,2},{3,7},{7,3},{8,12},{12,8},{9,1... | collective-permute-start | bytes 2408456 | tf_op jit(solution)/shard_map/ppermute | solution.py:22
  74.6 0.0 copy-done.7
  74.7 0.0 copy-done.5
  74.7 0.0 copy-done.6
  74.7 2.4 %collective-permute-start = (bf16[128,1024]{1,0:T(8,128)(2,1)S(1)}, bf16[128,1024]{1,0:T(8,128)(2,1)S(1)}, u32[]{:S(2)}, u32[]{:S(2)}) collective-permute-start(bf16[128,1024]{1,0:T(8,128)(2,1)S(1)} %fusion.4.front), channel_id=1, source_target_pairs={{0,4},{4,0},{1,5},{5,1},{2,6},{6,2},{3,7},{7,3},{8,12},{12,8},{9,1... | collective-permute-start | bytes 786440 | tf_op jit(solution)/shard_map/ppermute | solution.py:22
  77.1 1.1 collective-permute-done.pair_front
  78.3 0.0 collective-permute-done.4.refs_3_
  78.3 0.0 copy-start.4
  78.3 10.0 %all-to-all-done.1 = bf16[640,2,128]{2,1,0:T(2,128)(2,1)S(1)} async-done(((bf16[640,2,128]{2,1,0:T(2,128)(2,1)}), bf16[640,2,128]{2,1,0:T(2,128)(2,1)S(1)}, u32[]{:S(2)}, u32[]{:S(2)}) %all-to-all-start.1) | async-done | bytes 327712 | tf_op jit(solution)/shard_map/all_to_all | solution.py:422
  88.2 0.0 collective-permute-done.6.refs_5_
  88.2 0.0 collective-permute-done.5.refs_4_
  88.2 0.0 collective-permute-done.7.refs_6_
  88.2 0.0 copy-done.4
  88.3 4.3 %share.1 = bf16[1024,128]{1,0:T(8,128)(2,1)S(1)} custom-call(bf16[1280,128]{1,0:T(8,128)(2,1)S(1)} %bitcast.16, bf16[128,1024]{1,0:T(8,128)(2,1)S(1)} %fusion.4.front, bf16[128,1024]{1,0:T(8,128)(2,1)S(1)} %collective-permute-done.pair_front, bf16[3136,128]{1,0:T(8,128)(2,1)S(1)} %get-tuple-element.11.packed, ...), custom_call_target="tpu_custom_call" | custom-call | tf_op jit(solution)/shard_map/share/pallas_call | solution.py:428
  92.6 13.8 %all_to_all.21 = bf16[512,2,128]{2,1,0:T(2,128)(2,1)S(1)} all-to-all(bf16[512,2,128]{2,1,0:T(2,128)(2,1)S(1)} %bitcast.17), channel_id=1, replica_groups=mesh['ep_0'=16,'ep_1'=4,'ep_2'=2,'tp'=4] {'ep_1','tp'}, dimensions={0} | all-to-all | bytes 524288 | tf_op jit(solution)/shard_map/all_to_all | solution.py:446
  106.4 0.1 fold.1
  106.5 17.6 %all_to_all.22 = bf16[128,2,128]{2,1,0:T(2,128)(2,1)S(1)} all-to-all(bf16[128,2,128]{2,1,0:T(2,128)(2,1)S(1)} %bitcast.19), channel_id=1, replica_groups=mesh['ep_0'=16,'ep_1'=4,'ep_2'=2,'tp'=4] {'ep_0','ep_2'}, dimensions={0} | all-to-all | bytes 131072 | tf_op jit(solution)/shard_map/all_to_all | solution.py:460
  124.0 0.6 finish.1
  (2 shorter events, 0.0 us)
Async XLA Ops:
  4.5 14.6 %collective-permute-start.1 = (bf16[3136,128]{1,0:T(8,128)(2,1)S(1)}, bf16[3136,128]{1,0:T(8,128)(2,1)}, u32[]{:S(2)}, u32[]{:S(2)}) collective-permute-start(bf16[3136,128]{1,0:T(8,128)(2,1)S(1)} %get-tuple-element.11.packed), channel_id=1, source_target_pairs={{0,1},{1,2},{2,3},{3,0},{4,7},{5,4},{6,5},{7,6},{8,9},{9,10},{10,1... | collective-permute-start | bytes 2408456 | tf_op jit(solution)/shard_map/ppermute | solution.py:44
  9.9 60.3 %collective-permute-start.2 = (bf16[3136,128]{1,0:T(8,128)(2,1)S(1)}, bf16[3136,128]{1,0:T(8,128)(2,1)}, u32[]{:S(2)}, u32[]{:S(2)}) collective-permute-start(bf16[3136,128]{1,0:T(8,128)(2,1)S(1)} %get-tuple-element.11.packed), channel_id=1, source_target_pairs={{0,3},{1,0},{2,1},{3,2},{4,5},{5,6},{6,7},{7,4},{8,11},{9,8},{10,9... | collective-permute-start | bytes 2408456 | tf_op jit(solution)/shard_map/ppermute | solution.py:44
  19.0 53.7 %collective-permute-start.3 = (bf16[3136,128]{1,0:T(8,128)(2,1)}, bf16[3136,128]{1,0:T(8,128)(2,1)}, u32[]{:S(2)}, u32[]{:S(2)}) collective-permute-start(bf16[3136,128]{1,0:T(8,128)(2,1)} %collective-permute-done.1.refs_0_), channel_id=1, source_target_pairs={{0,1},{1,2},{2,3},{3,0},{4,7},{5,4},{6,5},{7,6},{8,9},{9,10},{10,1... | collective-permute-start | bytes 2408456 | tf_op jit(solution)/shard_map/ppermute | solution.py:44
  24.2 12.5 %copy-start = (bf16[8,1024]{1,0:T(8,128)(2,1)S(1)}, bf16[8,1024]{1,0:T(8,128)(2,1)}, u32[]{:S(2)}) copy-start(bf16[8,1024]{1,0:T(8,128)(2,1)} %tokens.1) | copy-start | bytes 49156
  24.2 12.5 %copy-start.3 = (f32[8,2]{0,1:T(2,128)S(1)}, f32[8,2]{0,1:T(2,128)}, u32[]{:S(2)}) copy-start(f32[8,2]{0,1:T(2,128)} %param.44) | copy-start | bytes 196
  36.6 0.7 copy-start.1
  36.6 0.7 copy-start.2
  38.2 36.4 %copy-start.7 = (bf16[1024]{0:T(1024)(128)(2,1)S(1)}, bf16[1024]{0:T(1024)(128)(2,1)}, u32[]{:S(2)}) copy-start(bf16[1024]{0:T(1024)(128)(2,1)} %param.39) | copy-start | bytes 6148
  38.2 36.4 %copy-start.5 = (bf16[1024,32]{0,1:T(8,128)(2,1)S(1)}, bf16[1024,32]{0,1:T(8,128)(2,1)}, u32[]{:S(2)}) copy-start(bf16[1024,32]{0,1:T(8,128)(2,1)} %param.41) | copy-start | bytes 196612
  38.2 36.5 %copy-start.6 = (bf16[1024,32]{0,1:T(8,128)(2,1)S(1)}, bf16[1024,32]{0,1:T(8,128)(2,1)}, u32[]{:S(2)}) copy-start(bf16[1024,32]{0,1:T(8,128)(2,1)} %param.40) | copy-start | bytes 196612
  38.2 50.0 %all-to-all-start.1 = ((bf16[640,2,128]{2,1,0:T(2,128)(2,1)}), bf16[640,2,128]{2,1,0:T(2,128)(2,1)S(1)}, u32[]{:S(2)}, u32[]{:S(2)}) async-start(bf16[640,2,128]{2,1,0:T(2,128)(2,1)} %bitcast.8), calls=%async_computation.1 | async-start | bytes 655360 | tf_op jit(solution)/shard_map/all_to_all | solution.py:422
  65.5 12.7 %collective-permute-start.4 = (bf16[3136,128]{1,0:T(8,128)(2,1)S(1)}, bf16[3136,128]{1,0:T(8,128)(2,1)S(1)}, u32[]{:S(2)}, u32[]{:S(2)}) collective-permute-start(bf16[3136,128]{1,0:T(8,128)(2,1)S(1)} %get-tuple-element.11.packed), channel_id=1, source_target_pairs={{0,4},{4,0},{1,5},{5,1},{2,6},{6,2},{3,7},{7,3},{8,12},{12,8},{9,1... | collective-permute-start | bytes 2408456 | tf_op jit(solution)/shard_map/ppermute | solution.py:22
  68.3 19.9 %collective-permute-start.5 = (bf16[3136,128]{1,0:T(8,128)(2,1)}, bf16[3136,128]{1,0:T(8,128)(2,1)}, u32[]{:S(2)}, u32[]{:S(2)}) collective-permute-start(bf16[3136,128]{1,0:T(8,128)(2,1)} %collective-permute-done.1.refs_0_), channel_id=1, source_target_pairs={{0,4},{4,0},{1,5},{5,1},{2,6},{6,2},{3,7},{7,3},{8,12},{12,8},{9,1... | collective-permute-start | bytes 2408456 | tf_op jit(solution)/shard_map/ppermute | solution.py:22
  70.3 18.0 %collective-permute-start.6 = (bf16[3136,128]{1,0:T(8,128)(2,1)}, bf16[3136,128]{1,0:T(8,128)(2,1)}, u32[]{:S(2)}, u32[]{:S(2)}) collective-permute-start(bf16[3136,128]{1,0:T(8,128)(2,1)} %collective-permute-done.2.refs_1_), channel_id=1, source_target_pairs={{0,4},{4,0},{1,5},{5,1},{2,6},{6,2},{3,7},{7,3},{8,12},{12,8},{9,1... | collective-permute-start | bytes 2408456 | tf_op jit(solution)/shard_map/ppermute | solution.py:22
  72.7 15.5 %collective-permute-start.7 = (bf16[3136,128]{1,0:T(8,128)(2,1)}, bf16[3136,128]{1,0:T(8,128)(2,1)}, u32[]{:S(2)}, u32[]{:S(2)}) collective-permute-start(bf16[3136,128]{1,0:T(8,128)(2,1)} %collective-permute-done.3.refs_2_), channel_id=1, source_target_pairs={{0,4},{4,0},{1,5},{5,1},{2,6},{6,2},{3,7},{7,3},{8,12},{12,8},{9,1... | collective-permute-start | bytes 2408456 | tf_op jit(solution)/shard_map/ppermute | solution.py:22
  74.7 3.6 %collective-permute-start = (bf16[128,1024]{1,0:T(8,128)(2,1)S(1)}, bf16[128,1024]{1,0:T(8,128)(2,1)S(1)}, u32[]{:S(2)}, u32[]{:S(2)}) collective-permute-start(bf16[128,1024]{1,0:T(8,128)(2,1)S(1)} %fusion.4.front), channel_id=1, source_target_pairs={{0,4},{4,0},{1,5},{5,1},{2,6},{6,2},{3,7},{7,3},{8,12},{12,8},{9,1... | collective-permute-start | bytes 786440 | tf_op jit(solution)/shard_map/ppermute | solution.py:22
  78.3 10.0 %copy-start.4 = (bf16[3136,128]{1,0:T(8,128)(2,1)}, bf16[3136,128]{1,0:T(8,128)(2,1)S(1)}, u32[]{:S(2)}) copy-start(bf16[3136,128]{1,0:T(8,128)(2,1)S(1)} %collective-permute-done.4.refs_3_) | copy-start | bytes 2408452

commit v5 on v4

v5 whole, which is shorter than its diff:
```python
import jax
import jax.numpy as jnp
from jax import lax
from jax.experimental import pallas as pl
from jax.experimental.pallas import tpu as pltpu
from jax.sharding import Mesh
from jax.sharding import PartitionSpec as P

EP = ("ep_0", "ep_1", "ep_2")
PAIR = "ep_2"
LANES = 128
NOTE_ROWS = 2

epsilon = 1e-06

VMEM = pl.BlockSpec(memory_space=pltpu.VMEM)
SMEM = pl.BlockSpec(memory_space=pltpu.SMEM)
ANY = pl.BlockSpec(memory_space=pl.ANY)


def swap(shard):
    return lax.ppermute(shard, PAIR, [(0, 1), (1, 0)])


def scaled(values, gain):
    mean = jnp.mean(values * values, axis=-1, keepdims=True)
    return values * lax.rsqrt(mean + epsilon) * gain


def silu(values):
    return values / (1.0 + jnp.exp(-values))


def in_vmem(values):
    return pltpu.with_memory_space_constraint(values, pltpu.VMEM)


def shifted(shard, step, members):
    pairs = []
    for core, sign in enumerate((1, -1)):
        for t in range(members):
            target = (t + sign * step) % members
            pairs.append((core * members + t, core * members + target))
    return lax.ppermute(shard, (PAIR, "tp"), pairs)


def wide_dot(left, right):
    return jnp.dot(left, right, preferred_element_type=jnp.float32)


def attend_kernel(*refs):
    inputs, outputs, scratch = refs[:20], refs[20:23], refs[23:]
    partial, packed, notes = outputs
    locals_, sems = scratch[:-1], scratch[-1]
    expert_gate, expert_up, expert_down, shared_down = inputs[16:]
    copies = []

    def start(source, target):
        copy = pltpu.make_async_copy(source, target, sems.at[len(copies)])
        copy.start()
        copies.append(copy)

    for source, target in zip(inputs[:16], locals_):
        start(source, target)
    tokens, norm_gain, query_weight, query_gain, key_weight, key_gain = locals_[:6]
    value_weight, forget_weight, forget_bias, keys, cum, lengths = locals_[6:12]
    values, out_weight, routes, route_weights = locals_[12:]
    first_packed = len(copies)
    row = 0

    def pack(source, row):
        start(source, packed.at[pl.ds(row, source.shape[0]), :])
        return row + source.shape[0]

    row = pack(expert_gate, row)
    row = pack(expert_up, row)
    for block in range(expert_down.shape[1] // LANES):
        row = pack(expert_down.at[:, pl.ds(block * LANES, LANES)], row)
    for block in range(shared_down.shape[1] // LANES):
        row = pack(shared_down.at[:, pl.ds(block * LANES, LANES)], row)

    seqs, cache_len, head = keys.shape
    groups = query_weight.shape[1] // head
    for copy in copies[:3]:
        copy.wait()
    normed = scaled(tokens[...].astype(jnp.float32), norm_gain[...].astype(jnp.float32))
    normed = normed.astype(jnp.bfloat16)
    for copy in copies[3:9]:
        copy.wait()
    gain = query_gain[...].astype(jnp.float32)
    wide = wide_dot(normed, query_weight[...])
    query = [scaled(wide[:, g * head : (g + 1) * head], gain) for g in range(groups)]
    query = jnp.concatenate(query, axis=0).astype(jnp.bfloat16)
    new_key = scaled(wide_dot(normed, key_weight[...]), key_gain[...].astype(jnp.float32))
    new_key = new_key.astype(jnp.bfloat16).astype(jnp.float32)
    new_value = wide_dot(normed, value_weight[...]).astype(jnp.bfloat16).astype(jnp.float32)
    products = normed.astype(jnp.float32) * forget_weight[...].astype(jnp.float32)
    forget = jnp.sum(products, axis=-1, keepdims=True) + forget_bias[0]
    new_log = jnp.minimum(forget, 0.0) - jnp.log1p(jnp.exp(-jnp.abs(forget)))

    rows = groups * seqs
    owner = lax.broadcasted_iota(jnp.int32, (rows, cache_len), 0) % seqs
    position = lax.broadcasted_iota(jnp.int32, (rows, cache_len), 1)
    scores = jnp.zeros((rows, cache_len), jnp.float32)
    decay = jnp.zeros((rows, cache_len), jnp.float32)
    length = jnp.zeros((rows, cache_len), jnp.int32)
    for copy in copies[9:12]:
        copy.wait()
    for b in range(seqs):
        mine = owner == b
        one = lax.dot_general(
            query, keys[b], (((1,), (1,)), ((), ())), preferred_element_type=jnp.float32
        )
        scores = jnp.where(mine, one, scores)
        decay = jnp.where(mine, cum[b], decay)
        length = jnp.where(mine, lengths[b], length)
    last = jnp.where(position == length - 1, decay, 0.0)
    last = jnp.sum(last, axis=-1, keepdims=True)
    bias = last - decay + jnp.concatenate([new_log] * groups, axis=0)
    score_scale = head ** (-0.5)
    past = jnp.where(position < length, scores * score_scale + bias, -jnp.inf)
    own = query.astype(jnp.float32) * jnp.concatenate([new_key] * groups, axis=0)
    own = jnp.sum(own, axis=-1, keepdims=True) * score_scale
    past_exp = jnp.exp(past)
    own_exp = jnp.exp(own)
    denominator = jnp.sum(past_exp, axis=-1, keepdims=True) + own_exp
    past_prob = (past_exp / denominator).astype(jnp.bfloat16)
    own_prob = (own_exp / denominator).astype(jnp.bfloat16).astype(jnp.float32)
    head_owner = owner[:, :head]
    mixed = jnp.zeros((rows, head), jnp.float32)
    copies[12].wait()
    for b in range(seqs):
        mixed = jnp.where(head_owner == b, wide_dot(past_prob, values[b]), mixed)
    mixed = mixed + own_prob * jnp.concatenate([new_value] * groups, axis=0)
    heads_out = [mixed[g * seqs : (g + 1) * seqs] for g in range(groups)]
    heads_out = jnp.concatenate(heads_out, axis=1).astype(jnp.bfloat16)
    copies[13].wait()
    product = wide_dot(heads_out, out_weight[...]).astype(jnp.bfloat16)
    for peer in range(partial.shape[0]):
        partial[peer] = product

    copies[14].wait()
    copies[15].wait()
    members = partial.shape[0]
    member = lax.axis_index("tp")
    norm_weights = route_weights[...]
    norm_weights = norm_weights / jnp.sum(norm_weights, axis=0, keepdims=True)
    high = norm_weights.astype(jnp.bfloat16).astype(jnp.float32)
    marks = (routes[...].astype(jnp.float32), high, norm_weights - high)
    column = lax.broadcasted_iota(jnp.int32, routes.shape, 1)
    lane = lax.broadcasted_iota(jnp.int32, (1, LANES), 1)
    lines = []
    for half in range(2):
        at = half * members + member
        line = jnp.zeros((1, LANES), jnp.float32)
        for i, mark in enumerate(marks):
            here = jnp.sum(jnp.where(column == at, mark, 0.0), axis=1, keepdims=True)
            for j in range(2):
                line = jnp.where(lane == 2 * i + j, here[j : j + 1], line)
        lines.append(line)
    notes[...] = jnp.concatenate(lines + [jnp.zeros((6, LANES), jnp.float32)], axis=0)
    for copy in copies[first_packed:]:
        copy.wait()


def rows_kernel(partial, tokens, ffn_gain, notes, residual, outgoing):
    member = lax.axis_index("tp")
    attended = jnp.sum(partial[...].astype(jnp.float32), axis=0)
    full = tokens[...].astype(jnp.float32) + attended
    seqs, width = full.shape
    members = partial.shape[0]
    slice_width = width // members
    for t in range(members):

        @pl.when(member == t)
        def _():
            residual[...] = full[:, t * slice_width : (t + 1) * slice_width]

    normed = scaled(full, ffn_gain[...].astype(jnp.float32))
    normed = normed.astype(jnp.bfloat16).astype(jnp.float32)
    rows_here = lax.broadcasted_iota(jnp.int32, (seqs, width), 0)
    pieces = []
    for half in range(2):
        at = half * members + member
        row = jnp.sum(jnp.where(rows_here == at, normed, 0.0), axis=0, keepdims=True)
        pieces += [row[:, k : k + LANES] for k in range(0, width, LANES)]
        pieces += [notes[half : half + 1, :], jnp.zeros((1, LANES), jnp.float32)]
    pattern = jnp.concatenate(pieces * 4, axis=0).astype(jnp.bfloat16)
    step = pattern.shape[0]
    for i in range(outgoing.shape[0] // step):
        outgoing[i * step : (i + 1) * step, :] = pattern


def share_kernel(rows, front, packed, *refs):
    sources, (out, wide, narrow, columns, staged, sems) = refs[:-6], refs[-6:]
    copies = []
    for i, source in enumerate(sources):
        copies.append(pltpu.make_async_copy(source, staged.at[i], sems.at[i]))
        copies[-1].start()
    packs = [packed] + [staged.at[i] for i in range(len(sources))]
    members = len(packs)
    member = lax.axis_index("tp")
    core = lax.axis_index(PAIR)
    me = lax.axis_index(EP).astype(jnp.float32)
    width = front.shape[1]
    count = narrow.shape[0]
    blocks = width // LANES
    stride = blocks + NOTE_ROWS
    lines = lax.axis_size("ep_1") * 2
    depth = count // lines
    wide[: rows.shape[0], :] = rows[...].astype(jnp.float32)
    marks = []
    for line in range(lines):
        for k in range(blocks + 1):
            piece = wide[pl.ds(line * stride + k, depth, stride=lines * stride), :]
            if k < blocks:
                at = (slice(line * depth, (line + 1) * depth), slice(k * LANES, (k + 1) * LANES))
                narrow[at] = piece.astype(jnp.bfloat16)
            else:
                marks.append(piece)
    marks = jnp.concatenate(marks, axis=0)
    weight = jnp.zeros((count, 1), jnp.float32)
    for j in range(2):
        norm_weight = marks[:, 2 + j : 3 + j] + marks[:, 4 + j : 5 + j]
        weight = weight + jnp.where(marks[:, j : j + 1] == me, norm_weight, 0.0)
    values = narrow[...]
    down_start = 2 * width
    shared_start = down_start + blocks * LANES
    per_member = blocks // members
    units = (packs[0].shape[0] - shared_start) // per_member

    pre = lax.dot_general(
        values, front[...], (((1,), (1,)), ((), ())), preferred_element_type=jnp.float32
    )
    mix_gate = 1.0 / (1.0 + jnp.exp(-pre[:, 2 * units : 2 * units + 1]))
    shared = (silu(pre[:, :units]) * pre[:, units : 2 * units]).astype(jnp.bfloat16)
    hidden = []
    for s in range(members):
        if s:
            copies[s - 1].wait()
        both = jnp.concatenate([packs[s][:width, :], packs[s][width : 2 * width, :]], axis=1)
        both = wide_dot(values, both)
        hidden.append((silu(both[:, :LANES]) * both[:, LANES:]).astype(jnp.bfloat16))
    halves = [jnp.concatenate(hidden[i : i + 2], axis=1) for i in range(0, members, 2)]
    ahead = jnp.where(core == 0, members - 1, 1)
    for s, origin in enumerate((0, ahead, members - ahead, 2)):
        dense = [
            packs[s][pl.ds(shared_start + k * units, units), :] for k in range(per_member)
        ]
        dense = wide_dot(shared, jnp.concatenate(dense, axis=1))
        columns[(member + origin) % members] = mix_gate * dense
    for n in range(members):
        firsts = [down_start + (n * per_member + k) * LANES for k in range(per_member)]
        total = columns[n]
        for i in range(len(halves)):
            down = [
                jnp.concatenate(
                    [packs[2 * i + s][first : first + LANES, :] for s in range(2)], axis=0
                )
                for first in firsts
            ]
            total = total + weight * wide_dot(halves[i], jnp.concatenate(down, axis=1))
        for k in range(per_member):
            for line in range(lines):
                first = line // 2 * depth * 2 * blocks + n * depth * 2 * per_member
                first = first + line % 2 * per_member + k
                piece = total[line * depth : (line + 1) * depth, k * LANES : (k + 1) * LANES]
                wide[pl.ds(first, depth, stride=2 * per_member), :] = piece
    out[...] = wide[: count * blocks, :].astype(out.dtype)


def add_kernel(own, pair, out):
    out[...] = (own[...] + pair[...].astype(jnp.float32)).astype(jnp.bfloat16)


def fold_kernel(parts, out, wide, small):
    sources = lax.axis_size("ep_1")
    members = lax.axis_size("tp")
    rows = parts.shape[0] // sources
    wide[...] = parts[...].astype(jnp.float32)
    total = wide[:rows, :]
    for i in range(1, sources):
        total = total + wide[i * rows : (i + 1) * rows, :]
    wide[:rows, :] = total
    halves = 2
    count = rows // members // halves
    for t in range(members):
        for j in range(halves):
            piece = wide[pl.ds(t * count * halves + j, count, stride=halves), :]
            small[pl.ds(t * halves + j, count, stride=members * halves), :] = piece
    out[...] = small[...].astype(jnp.bfloat16)


def finish_kernel(parts, residual, out, small):
    rows = small.shape[0]
    total = parts[:rows, :].astype(jnp.float32)
    for i in range(1, parts.shape[0] // rows):
        total = total + parts[i * rows : (i + 1) * rows, :].astype(jnp.float32)
    small[...] = total
    seqs = residual.shape[0]
    for j in range(rows // seqs):
        piece = small[pl.ds(j, seqs, stride=rows // seqs), :]
        columns = slice(j * LANES, (j + 1) * LANES)
        out[:, columns] = (residual[:, columns] + piece).astype(jnp.bfloat16)


def per_device(
    tokens,
    lengths,
    cache_keys,
    cache_values,
    cache_cum,
    norm_gain,
    query_weight,
    key_weight,
    value_weight,
    forget_weight,
    forget_bias,
    query_gain,
    key_gain,
    out_weight,
    ffn_gain,
    mix_weight,
    shared_gate,
    shared_up,
    shared_down,
    routes,
    route_weights,
    expert_gate,
    expert_up,
    expert_down,
):
    seqs, width = tokens.shape
    cache_len, head = cache_keys.shape[1], cache_keys.shape[3]
    peers = lax.axis_size(EP)
    members = lax.axis_size("tp")
    blocks = width // LANES
    units = shared_gate.shape[1]
    hidden = expert_gate.shape[2]
    pack_rows = 2 * width + hidden * blocks + units * shared_down.shape[1] // LANES
    copies = 2 + blocks + shared_down.shape[1] // LANES

    local = [
        tokens,
        norm_gain,
        query_weight,
        query_gain,
        key_weight,
        key_gain,
        value_weight,
        forget_weight.reshape(1, width),
        forget_bias,
        cache_keys.reshape(seqs, cache_len, head),
        cache_cum,
        lengths,
        cache_values.reshape(seqs, cache_len, head),
        out_weight,
        routes.T,
        route_weights.T,
    ]
    spaces = [pltpu.SMEM if each is forget_bias or each is lengths else pltpu.VMEM for each in local]
    partial, packed, notes = pl.pallas_call(
        attend_kernel,
        in_specs=[ANY] * (len(local) + 4),
        out_specs=[VMEM] * 3,
        out_shape=[
            pltpu.VMEM((members, seqs, width), jnp.bfloat16),
            pltpu.VMEM((pack_rows, LANES), jnp.bfloat16),
            pltpu.VMEM((8, LANES), jnp.float32),
        ],
        scratch_shapes=[space(each.shape, each.dtype) for space, each in zip(spaces, local)]
        + [pltpu.SemaphoreType.DMA((copies + len(local),))],
        name="attend",
    )(*local, expert_gate[0], expert_up[0], expert_down[0], shared_down)
    partial = lax.all_to_all(partial, "tp", 0, 0, tiled=True)
    ahead = shifted(packed, 1, members)
    behind = shifted(packed, -1, members)
    across = shifted(ahead, 1, members)
    packs = [packed, ahead, behind, across]

    front = [shared_gate.T, shared_up.T, mix_weight[None]]
    front = jnp.concatenate(front, axis=0)
    front = jnp.pad(front, ((0, LANES - front.shape[0]), (0, 0)))

    sub_rows = peers * (blocks + NOTE_ROWS)
    residual, outgoing = pl.pallas_call(
        rows_kernel,
        in_specs=[VMEM] * 4,
        out_specs=[VMEM, VMEM],
        out_shape=[
            pltpu.VMEM((seqs, width // members), jnp.float32),
            pltpu.VMEM((sub_rows, LANES), jnp.bfloat16),
        ],
        name="rows",
    )(*map(in_vmem, (partial, tokens, ffn_gain, notes)))
    own_rows = lax.all_to_all(outgoing.reshape(-1, 2, LANES), EP[:2], 0, 0, tiled=True)


    def share(rows, dtype):
        return pl.pallas_call(
            share_kernel,
            in_specs=[VMEM] * 3 + [ANY] * (members - 1),
            out_specs=VMEM,
            out_shape=pltpu.VMEM((peers * blocks, LANES), dtype),
            scratch_shapes=[
                pltpu.VMEM((sub_rows, LANES), jnp.float32),
                pltpu.VMEM((peers, width), jnp.bfloat16),
                pltpu.VMEM((members, peers, width // members), jnp.float32),
                pltpu.VMEM((members - 1, pack_rows, LANES), jnp.bfloat16),
                pltpu.SemaphoreType.DMA((members - 1,)),
            ],
            name="share",
        )(*map(in_vmem, (rows.reshape(sub_rows, LANES), front, packed)), *packs[1:])

    pair_rows = swap(own_rows)
    own_share = share(own_rows, jnp.float32)
    pair_share = share(pair_rows, jnp.bfloat16)
    pair_share = swap(pair_share)
    total = pl.pallas_call(
        add_kernel,
        in_specs=[VMEM] * 2,
        out_specs=VMEM,
        out_shape=pltpu.VMEM(own_share.shape, jnp.bfloat16),
        name="add",
    )(in_vmem(own_share), in_vmem(pair_share))
    parts = lax.all_to_all(total.reshape(-1, 2, LANES), ("ep_1", "tp"), 0, 0, tiled=True)
    parts = parts.reshape(-1, LANES)
    rows = parts.shape[0] // lax.axis_size("ep_1")
    parts = pl.pallas_call(
        fold_kernel,
        in_specs=[VMEM],
        out_specs=VMEM,
        out_shape=pltpu.VMEM((rows, LANES), jnp.bfloat16),
        scratch_shapes=[
            pltpu.VMEM(parts.shape, jnp.float32),
            pltpu.VMEM((rows, LANES), jnp.float32),
        ],
        name="fold",
    )(in_vmem(parts))
    parts = lax.all_to_all(parts.reshape(-1, 2, LANES), EP[0], 0, 0, tiled=True)
    return pl.pallas_call(
        finish_kernel,
        in_specs=[VMEM] * 2,
        out_specs=VMEM,
        out_shape=jax.ShapeDtypeStruct((seqs, width // members), jnp.bfloat16),
        scratch_shapes=[pltpu.VMEM((seqs * width // members // LANES, LANES), jnp.float32)],
        name="finish",
    )(in_vmem(parts.reshape(-1, LANES)), in_vmem(residual))


def solution(mesh):
    finer = Mesh(mesh.devices.reshape(16, 4, 2, mesh.shape["tp"]), ("ep_0", "ep_1", "ep_2", "tp"))
    placed = (
        P(EP, None),
        P(EP),
        P(EP, None, "tp", None),
        P(EP, None, "tp", None),
        P(EP, "tp", None),
        P(),
        P(None, "tp"),
        P(None, "tp"),
        P(None, "tp"),
        P(None, "tp"),
        P("tp"),
        P(),
        P(),
        P("tp", None),
        P(),
        P(),
        P(None, EP),
        P(None, EP),
        P(EP, "tp"),
        P(EP, None),
        P(EP, None),
        P(EP, None, "tp"),
        P(EP, None, "tp"),
        P(EP, "tp", None),
    )

    return jax.shard_map(
        per_device, mesh=finer, in_specs=placed, out_specs=P(EP, "tp"), check_vma=False
    )
```

time: 125 us -> 117 us (0.936)
  waiting for transfers between devices: 18.3 us -> 13.9 us
  starting transfers between devices: 51.3 us -> 47.9 us
    ppermute x5 -> x2, starting transfers between devices: 11.5 us -> 21.7 us  [swap(): return lax.ppermute(shard, PAIR, [(0, 1), (1, 0)])]
    all_to_all x1, starting transfers between devices: 27.3 us -> 18.4 us  [per_device(): lax.all_to_all(outgoing.reshape(-1, 2, LANES), EP[:2], 0, 0, tiled=True)]
    all_to_all x1, waiting for transfers between devices: 9.97 us -> 1.55 us  [per_device(): lax.all_to_all(outgoing.reshape(-1, 2, LANES), EP[:2], 0, 0, tiled=True)]
    all_to_all x1, blocking collectives: 17.6 us -> 22.8 us  [per_device(): parts = lax.all_to_all(parts.reshape(-1, 2, LANES), EP[0], 0, 0, tiled=True)]
    ppermute x3, starting transfers between devices: 12.5 us -> 7.77 us  [shifted(): return lax.ppermute(shard, (PAIR, 'tp'), pairs)]
    ppermute x3, waiting for transfers between devices: 7.16 us -> 11.3 us  [shifted(): return lax.ppermute(shard, (PAIR, 'tp'), pairs)]
    all_to_all x1, blocking collectives: 12.4 us -> 9.28 us  [per_device(): partial = lax.all_to_all(partial, 'tp', 0, 0, tiled=True)]
    all_to_all x1, blocking collectives: 13.8 us -> 11.5 us  [per_device(): lax.all_to_all(total.reshape(-1, 2, LANES), ('ep_1', 'tp'), 0, 0, tiled=T...]
  transfers between devices with their start and end apart: 9 -> 6, of which waited for: 3 -> 4; matrix products, arithmetic and copies ran while one was open for 0% -> 0% of each run, Pallas kernels for 1% -> 2%
where the time goes in v5:
time: 117 us; the launch traced here: 115 us
  starting transfers between devices  47.9 us (41%)
  blocking collectives  43.5 us (37%)
  waiting for transfers between devices  13.9 us (12%)
  Pallas kernels  9.27 us (8%)
    all_to_all x1, blocking collectives, per_device(): parts = lax.all_to_all(parts.reshape(-1, 2, LANES), EP[0], 0, 0, tiled=True)  22.8 us
    ppermute x2, starting transfers between devices, swap(): return lax.ppermute(shard, PAIR, [(0, 1), (1, 0)])  21.7 us
    all_to_all x1, starting transfers between devices, per_device(): lax.all_to_all(outgoing.reshape(-1, 2, LANES), EP[:2], 0, 0, tiled=True)  18.4 us
    all_to_all x1, blocking collectives, per_device(): lax.all_to_all(total.reshape(-1, 2, LANES), ('ep_1', 'tp'), 0, 0, tiled=T...  11.5 us
    ppermute x3, waiting for transfers between devices, shifted(): return lax.ppermute(shard, (PAIR, 'tp'), pairs)  11.3 us
    all_to_all x1, blocking collectives, per_device(): partial = lax.all_to_all(partial, 'tp', 0, 0, tiled=True)  9.28 us
    ppermute x3, starting transfers between devices, shifted(): return lax.ppermute(shard, (PAIR, 'tp'), pairs)  7.77 us
    pallas_call x2, Pallas kernels, share(): pl.pallas_call(share_kernel, in_specs=[VMEM] * 3 + [ANY] * (members - 1),...  4.69 us
  transfers between devices with their start and end apart: 6, of which 4 were waited for; matrix products, arithmetic and copies ran while one was open for 0% of the time, Pallas kernels for 2%

profile of v5, /device:TPU:1, one launch (start us, length us, event | category | flops | bytes accessed | tf_op | source)
XLA Modules:
  0.0 115.5 jit_solution(344964377813712963)
XLA Ops:
  0.7 3.0 %attend.1 = (bf16[4,8,1024]{2,1,0:T(8,128)(2,1)S(1)}, bf16[3136,128]{1,0:T(8,128)(2,1)S(1)}, f32[8,128]{1,0:T(8,128)S(1)}) custom-call(bf16[8,1024]{1,0:T(8,128)(2,1)} %tokens.1, bf16[1024]{0:T(1024)(128)(2,1)} %refs_1_.1, bf16[1024,256]{1,0:T(8,128)(2,1)} %refs_2_.1, bf16[128]{0:T(256)(128)(2,1)} %refs_3_.1, bf16[1024,128]{1,0:T(8,128)(2,1)} %refs_4_.1, ...), custom_call_target="tpu_custom_call" | custom-call | tf_op jit(solution)/shard_map/attend/pallas_call | solution.py:362
  3.6 0.0 copy-start
  3.6 0.0 copy-start.1
  3.7 9.3 %all_to_all.20.partial = bf16[4,8,1024]{2,1,0:T(8,128)(2,1)S(1)} all-to-all(bf16[4,8,1024]{2,1,0:T(8,128)(2,1)S(1)} %get-tuple-element.10), channel_id=1, replica_groups=mesh['ep_0'=16,'ep_1'=4,'ep_2'=2,'tp'=4] {'tp'}, dimensions={0} | all-to-all | bytes 131072 | tf_op jit(solution)/shard_map/all_to_all | solution.py:375
  12.9 0.0 copy-done
  12.9 0.0 copy-done.1
  12.9 0.9 rows.1
  13.8 0.0 copy-start.6
  13.8 0.0 copy-start.4
  13.8 0.0 copy-start.5
  13.8 18.4 %all-to-all-start.1 = ((bf16[640,2,128]{2,1,0:T(2,128)(2,1)}), bf16[640,2,128]{2,1,0:T(2,128)(2,1)S(1)}, u32[]{:S(2)}, u32[]{:S(2)}) async-start(bf16[640,2,128]{2,1,0:T(2,128)(2,1)} %bitcast.8), calls=%async_computation.1 | async-start | bytes 655360 | tf_op jit(solution)/shard_map/all_to_all | solution.py:396
  32.2 2.8 %collective-permute-start = (bf16[3136,128]{1,0:T(8,128)(2,1)S(1)}, bf16[3136,128]{1,0:T(8,128)(2,1)S(1)}, u32[]{:S(2)}, u32[]{:S(2)}) collective-permute-start(bf16[3136,128]{1,0:T(8,128)(2,1)S(1)} %get-tuple-element.13.packed), channel_id=1, source_target_pairs={{0,1},{1,2},{2,3},{3,0},{4,7},{5,4},{6,5},{7,6},{8,9},{9,10},{10,1... | collective-permute-start | bytes 2408456 | tf_op jit(solution)/shard_map/ppermute | solution.py:44
  35.0 2.5 %collective-permute-start.1 = (bf16[3136,128]{1,0:T(8,128)(2,1)S(1)}, bf16[3136,128]{1,0:T(8,128)(2,1)S(1)}, u32[]{:S(2)}, u32[]{:S(2)}) collective-permute-start(bf16[3136,128]{1,0:T(8,128)(2,1)S(1)} %get-tuple-element.13.packed), channel_id=1, source_target_pairs={{0,3},{1,0},{2,1},{3,2},{4,5},{5,6},{6,7},{7,4},{8,11},{9,8},{10,9... | collective-permute-start | bytes 2408456 | tf_op jit(solution)/shard_map/ppermute | solution.py:44
  37.5 11.2 %collective-permute-done.refs_0_ = bf16[3136,128]{1,0:T(8,128)(2,1)S(1)} collective-permute-done((bf16[3136,128]{1,0:T(8,128)(2,1)S(1)}, bf16[3136,128]{1,0:T(8,128)(2,1)S(1)}, u32[]{:S(2)}, u32[]{:S(2)}) %collective-permute-start) | collective-permute-done | bytes 802848 | tf_op jit(solution)/shard_map/ppermute | solution.py:44
  48.7 0.0 copy-start.2
  48.7 2.5 %collective-permute-start.2 = (bf16[3136,128]{1,0:T(8,128)(2,1)S(1)}, bf16[3136,128]{1,0:T(8,128)(2,1)}, u32[]{:S(2)}, u32[]{:S(2)}) collective-permute-start(bf16[3136,128]{1,0:T(8,128)(2,1)S(1)} %collective-permute-done.refs_0_), channel_id=1, source_target_pairs={{0,1},{1,2},{2,3},{3,0},{4,7},{5,4},{6,5},{7,6},{8,9},{9,10},{10,1... | collective-permute-start | bytes 2408456 | tf_op jit(solution)/shard_map/ppermute | solution.py:44
  51.2 1.6 %all-to-all-done.1 = bf16[640,2,128]{2,1,0:T(2,128)(2,1)S(1)} async-done(((bf16[640,2,128]{2,1,0:T(2,128)(2,1)}), bf16[640,2,128]{2,1,0:T(2,128)(2,1)S(1)}, u32[]{:S(2)}, u32[]{:S(2)}) %all-to-all-start.1) | async-done | bytes 327712 | tf_op jit(solution)/shard_map/all_to_all | solution.py:396
  52.8 9.5 %collective-permute-start.3 = (bf16[640,2,128]{2,1,0:T(2,128)(2,1)S(1)}, bf16[640,2,128]{2,1,0:T(2,128)(2,1)S(1)}, u32[]{:S(2)}, u32[]{:S(2)}) collective-permute-start(bf16[640,2,128]{2,1,0:T(2,128)(2,1)S(1)} %all-to-all-done.1), channel_id=1, source_target_pairs={{0,4},{4,0},{1,5},{5,1},{2,6},{6,2},{3,7},{7,3},{8,12},{12,8},{9,1... | collective-permute-start | bytes 983048 | tf_op jit(solution)/shard_map/ppermute | solution.py:22
  62.3 0.0 copy-done.6
  62.3 0.0 copy-done.4
  62.3 0.0 copy-done.5
  62.4 0.0 collective-permute-done.1.refs_1_
  62.4 0.0 copy-start.3
  62.4 0.1 collective-permute-done.2.refs_2_
  62.5 1.1 collective-permute-done.3
  63.5 0.0 copy-done.3
  63.5 0.0 copy-done.2
  63.5 2.3 %share.3 = bf16[1024,128]{1,0:T(8,128)(2,1)S(1)} custom-call(bf16[1280,128]{1,0:T(8,128)(2,1)S(1)} %bitcast.20, bf16[128,1024]{1,0:T(8,128)(2,1)S(1)} %fusion.4.front, bf16[3136,128]{1,0:T(8,128)(2,1)S(1)} %get-tuple-element.13.packed, bf16[3136,128]{1,0:T(8,128)(2,1)} %copy-done.2, bf16[3136,128]{1,0:T(8,128)(2,1)} %copy-done.3, ...), custom_call_target="tpu_custom_call" | custom-call | tf_op jit(solution)/shard_map/share/pallas_call | solution.py:400
  65.9 12.2 %collective-permute-start.4 = (bf16[1024,128]{1,0:T(8,128)(2,1)S(1)}, bf16[1024,128]{1,0:T(8,128)(2,1)S(1)}, u32[]{:S(2)}, u32[]{:S(2)}) collective-permute-start(bf16[1024,128]{1,0:T(8,128)(2,1)S(1)} %share.3), channel_id=1, source_target_pairs={{0,4},{4,0},{1,5},{5,1},{2,6},{6,2},{3,7},{7,3},{8,12},{12,8},{9,1... | collective-permute-start | bytes 786440 | tf_op jit(solution)/shard_map/ppermute | solution.py:22
  78.1 2.3 %share.2.own = f32[1024,128]{1,0:T(8,128)S(1)} custom-call(bf16[1280,128]{1,0:T(8,128)(2,1)S(1)} %bitcast.17, bf16[128,1024]{1,0:T(8,128)(2,1)S(1)} %fusion.4.front, bf16[3136,128]{1,0:T(8,128)(2,1)S(1)} %get-tuple-element.13.packed, bf16[3136,128]{1,0:T(8,128)(2,1)} %copy-done.2, bf16[3136,128]{1,0:T(8,128)(2,1)} %copy-done.3, ...), custom_call_target="tpu_custom_call" | custom-call | tf_op jit(solution)/shard_map/share/pallas_call | solution.py:400
  80.5 0.0 collective-permute-done.4.pair
  80.5 11.5 %all_to_all.21 = bf16[512,2,128]{2,1,0:T(2,128)(2,1)S(1)} all-to-all(bf16[512,2,128]{2,1,0:T(2,128)(2,1)S(1)} %bitcast.19), channel_id=1, replica_groups=mesh['ep_0'=16,'ep_1'=4,'ep_2'=2,'tp'=4] {'ep_1','tp'}, dimensions={0} | all-to-all | bytes 524288 | tf_op jit(solution)/shard_map/all_to_all | solution.py:426
  92.0 0.1 fold.1
  92.1 22.8 %all_to_all.22 = bf16[128,2,128]{2,1,0:T(2,128)(2,1)S(1)} all-to-all(bf16[128,2,128]{2,1,0:T(2,128)(2,1)S(1)} %bitcast.21), channel_id=1, replica_groups=mesh['ep_0'=16,'ep_1'=4,'ep_2'=2,'tp'=4] {'ep_0'}, dimensions={0} | all-to-all | bytes 131072 | tf_op jit(solution)/shard_map/all_to_all | solution.py:440
  114.8 0.6 finish.1
  (3 shorter events, 0.1 us)
Async XLA Ops:
  3.6 9.3 %copy-start = (bf16[8,1024]{1,0:T(8,128)(2,1)S(1)}, bf16[8,1024]{1,0:T(8,128)(2,1)}, u32[]{:S(2)}) copy-start(bf16[8,1024]{1,0:T(8,128)(2,1)} %tokens.1) | copy-start | bytes 49156
  3.6 9.3 %copy-start.1 = (bf16[1024]{0:T(1024)(128)(2,1)S(1)}, bf16[1024]{0:T(1024)(128)(2,1)}, u32[]{:S(2)}) copy-start(bf16[1024]{0:T(1024)(128)(2,1)} %ffn_gain.1) | copy-start | bytes 6148
  13.8 48.5 %copy-start.6 = (bf16[1024]{0:T(1024)(128)(2,1)S(1)}, bf16[1024]{0:T(1024)(128)(2,1)}, u32[]{:S(2)}) copy-start(bf16[1024]{0:T(1024)(128)(2,1)} %param.39) | copy-start | bytes 6148
  13.8 48.5 %copy-start.4 = (bf16[1024,32]{0,1:T(8,128)(2,1)S(1)}, bf16[1024,32]{0,1:T(8,128)(2,1)}, u32[]{:S(2)}) copy-start(bf16[1024,32]{0,1:T(8,128)(2,1)} %param.41) | copy-start | bytes 196612
  13.8 48.5 %copy-start.5 = (bf16[1024,32]{0,1:T(8,128)(2,1)S(1)}, bf16[1024,32]{0,1:T(8,128)(2,1)}, u32[]{:S(2)}) copy-start(bf16[1024,32]{0,1:T(8,128)(2,1)} %param.40) | copy-start | bytes 196612
  13.8 38.9 %all-to-all-start.1 = ((bf16[640,2,128]{2,1,0:T(2,128)(2,1)}), bf16[640,2,128]{2,1,0:T(2,128)(2,1)S(1)}, u32[]{:S(2)}, u32[]{:S(2)}) async-start(bf16[640,2,128]{2,1,0:T(2,128)(2,1)} %bitcast.8), calls=%async_computation.1 | async-start | bytes 655360 | tf_op jit(solution)/shard_map/all_to_all | solution.py:396
  32.2 16.5 %collective-permute-start = (bf16[3136,128]{1,0:T(8,128)(2,1)S(1)}, bf16[3136,128]{1,0:T(8,128)(2,1)S(1)}, u32[]{:S(2)}, u32[]{:S(2)}) collective-permute-start(bf16[3136,128]{1,0:T(8,128)(2,1)S(1)} %get-tuple-element.13.packed), channel_id=1, source_target_pairs={{0,1},{1,2},{2,3},{3,0},{4,7},{5,4},{6,5},{7,6},{8,9},{9,10},{10,1... | collective-permute-start | bytes 2408456 | tf_op jit(solution)/shard_map/ppermute | solution.py:44
  35.0 27.3 %collective-permute-start.1 = (bf16[3136,128]{1,0:T(8,128)(2,1)S(1)}, bf16[3136,128]{1,0:T(8,128)(2,1)S(1)}, u32[]{:S(2)}, u32[]{:S(2)}) collective-permute-start(bf16[3136,128]{1,0:T(8,128)(2,1)S(1)} %get-tuple-element.13.packed), channel_id=1, source_target_pairs={{0,3},{1,0},{2,1},{3,2},{4,5},{5,6},{6,7},{7,4},{8,11},{9,8},{10,9... | collective-permute-start | bytes 2408456 | tf_op jit(solution)/shard_map/ppermute | solution.py:44
  48.7 14.8 %copy-start.2 = (bf16[3136,128]{1,0:T(8,128)(2,1)}, bf16[3136,128]{1,0:T(8,128)(2,1)S(1)}, u32[]{:S(2)}) copy-start(bf16[3136,128]{1,0:T(8,128)(2,1)S(1)} %collective-permute-done.refs_0_) | copy-start | bytes 2408452
  48.7 13.7 %collective-permute-start.2 = (bf16[3136,128]{1,0:T(8,128)(2,1)S(1)}, bf16[3136,128]{1,0:T(8,128)(2,1)}, u32[]{:S(2)}, u32[]{:S(2)}) collective-permute-start(bf16[3136,128]{1,0:T(8,128)(2,1)S(1)} %collective-permute-done.refs_0_), channel_id=1, source_target_pairs={{0,1},{1,2},{2,3},{3,0},{4,7},{5,4},{6,5},{7,6},{8,9},{9,10},{10,1... | collective-permute-start | bytes 2408456 | tf_op jit(solution)/shard_map/ppermute | solution.py:44
  52.8 10.8 %collective-permute-start.3 = (bf16[640,2,128]{2,1,0:T(2,128)(2,1)S(1)}, bf16[640,2,128]{2,1,0:T(2,128)(2,1)S(1)}, u32[]{:S(2)}, u32[]{:S(2)}) collective-permute-start(bf16[640,2,128]{2,1,0:T(2,128)(2,1)S(1)} %all-to-all-done.1), channel_id=1, source_target_pairs={{0,4},{4,0},{1,5},{5,1},{2,6},{6,2},{3,7},{7,3},{8,12},{12,8},{9,1... | collective-permute-start | bytes 983048 | tf_op jit(solution)/shard_map/ppermute | solution.py:22
  62.4 1.2 %copy-start.3 = (bf16[3136,128]{1,0:T(8,128)(2,1)}, bf16[3136,128]{1,0:T(8,128)(2,1)S(1)}, u32[]{:S(2)}) copy-start(bf16[3136,128]{1,0:T(8,128)(2,1)S(1)} %collective-permute-done.1.refs_1_) | copy-start | bytes 2408452
  65.9 14.6 %collective-permute-start.4 = (bf16[1024,128]{1,0:T(8,128)(2,1)S(1)}, bf16[1024,128]{1,0:T(8,128)(2,1)S(1)}, u32[]{:S(2)}, u32[]{:S(2)}) collective-permute-start(bf16[1024,128]{1,0:T(8,128)(2,1)S(1)} %share.3), channel_id=1, source_target_pairs={{0,4},{4,0},{1,5},{5,1},{2,6},{6,2},{3,7},{7,3},{8,12},{12,8},{9,1... | collective-permute-start | bytes 786440 | tf_op jit(solution)/shard_map/ppermute | solution.py:22

commit v6 on v5

--- a/solution.py
+++ b/solution.py
@@ -9,7 +9,6 @@
 EP = ("ep_0", "ep_1", "ep_2")
 PAIR = "ep_2"
 LANES = 128
-NOTE_ROWS = 2
 
 epsilon = 1e-06
 
@@ -184,93 +183,152 @@
         at = half * members + member
         row = jnp.sum(jnp.where(rows_here == at, normed, 0.0), axis=0, keepdims=True)
         pieces += [row[:, k : k + LANES] for k in range(0, width, LANES)]
-        pieces += [notes[half : half + 1, :], jnp.zeros((1, LANES), jnp.float32)]
-    pattern = jnp.concatenate(pieces * 4, axis=0).astype(jnp.bfloat16)
+    pieces.append(notes[:2, :])
+    pattern = jnp.concatenate(pieces * 8, axis=0).astype(jnp.bfloat16)
     step = pattern.shape[0]
     for i in range(outgoing.shape[0] // step):
         outgoing[i * step : (i + 1) * step, :] = pattern
 
 
-def share_kernel(rows, front, packed, *refs):
-    sources, (out, wide, narrow, columns, staged, sems) = refs[:-6], refs[-6:]
+def place_columns(target, values, n, depth, lines, blocks, per_member):
+    for k in range(per_member):
+        for line in range(lines):
+            first = line // 2 * depth * 2 * blocks + n * depth * 2 * per_member
+            first = first + line % 2 * per_member + k
+            piece = values[line * depth : (line + 1) * depth, k * LANES : (k + 1) * LANES]
+            target[pl.ds(first, depth, stride=2 * per_member), :] = piece
+
+
+def hidden_of(values, pack, width):
+    both = jnp.concatenate([pack[:width, :], pack[width : 2 * width, :]], axis=1)
+    both = wide_dot(values, both)
+    return (silu(both[:, :LANES]) * both[:, LANES:]).astype(jnp.bfloat16)
+
+
+def down_of(packs, first, per_member):
+    columns = []
+    for k in range(per_member):
+        rows = slice(first + k * LANES, first + (k + 1) * LANES)
+        columns.append(jnp.concatenate([pack[rows, :] for pack in packs], axis=0))
+    return jnp.concatenate(columns, axis=1)
+
+
+def share_kernel(rows, front, pair_front, resident, *refs):
+    sources, refs = refs[:-7], refs[-7:]
+    out, narrow, aside, wide, columns, staged, sems = refs
     copies = []
     for i, source in enumerate(sources):
         copies.append(pltpu.make_async_copy(source, staged.at[i], sems.at[i]))
         copies[-1].start()
-    packs = [packed] + [staged.at[i] for i in range(len(sources))]
-    members = len(packs)
+    members = lax.axis_size("tp")
+    packs = [staged.at[i] for i in range(len(sources))]
+    packs.insert(members, resident)
     member = lax.axis_index("tp")
     core = lax.axis_index(PAIR)
-    me = lax.axis_index(EP).astype(jnp.float32)
+    experts = (lax.axis_index(EP), lax.axis_index(EP) + 1 - 2 * core)
     width = front.shape[1]
     count = narrow.shape[0]
     blocks = width // LANES
-    stride = blocks + NOTE_ROWS
+    stride = 2 * blocks + 2
     lines = lax.axis_size("ep_1") * 2
     depth = count // lines
     wide[: rows.shape[0], :] = rows[...].astype(jnp.float32)
     marks = []
     for line in range(lines):
+        chip, half = line // 2, line % 2
         for k in range(blocks + 1):
-            piece = wide[pl.ds(line * stride + k, depth, stride=lines * stride), :]
+            first = chip * stride + (half * blocks + k if k < blocks else 2 * blocks + half)
+            piece = wide[pl.ds(first, depth, stride=lines // 2 * stride), :]
             if k < blocks:
                 at = (slice(line * depth, (line + 1) * depth), slice(k * LANES, (k + 1) * LANES))
                 narrow[at] = piece.astype(jnp.bfloat16)
             else:
                 marks.append(piece)
     marks = jnp.concatenate(marks, axis=0)
-    weight = jnp.zeros((count, 1), jnp.float32)
-    for j in range(2):
-        norm_weight = marks[:, 2 + j : 3 + j] + marks[:, 4 + j : 5 + j]
-        weight = weight + jnp.where(marks[:, j : j + 1] == me, norm_weight, 0.0)
+    weights = []
+    for expert in experts:
+        weight = jnp.zeros((count, 1), jnp.float32)
+        for j in range(2):
+            norm_weight = marks[:, 2 + j : 3 + j] + marks[:, 4 + j : 5 + j]
+            chosen = marks[:, j : j + 1] == expert.astype(jnp.float32)
+            weight = weight + jnp.where(chosen, norm_weight, 0.0)
+        weights.append(weight)
     values = narrow[...]
     down_start = 2 * width
     shared_start = down_start + blocks * LANES
     per_member = blocks // members
-    units = (packs[0].shape[0] - shared_start) // per_member
-
-    pre = lax.dot_general(
-        values, front[...], (((1,), (1,)), ((), ())), preferred_element_type=jnp.float32
-    )
-    mix_gate = 1.0 / (1.0 + jnp.exp(-pre[:, 2 * units : 2 * units + 1]))
-    shared = (silu(pre[:, :units]) * pre[:, units : 2 * units]).astype(jnp.bfloat16)
+    units = (resident.shape[0] - shared_start) // per_member
+
+    fronts = [
+        lax.dot_general(
+            values, each[...], (((1,), (1,)), ((), ())), preferred_element_type=jnp.float32
+        )
+        for each in (front, pair_front)
+    ]
+    mix_gate = 1.0 / (1.0 + jnp.exp(-fronts[0][:, 2 * units : 2 * units + 1]))
+    shared = [silu(pre[:, :units]) * pre[:, units : 2 * units] for pre in fronts]
+    shared = [each.astype(jnp.bfloat16) for each in shared]
+    lane = lax.broadcasted_iota(jnp.int32, aside.shape, 1)
+    scalars = jnp.where(lane == 0, weights[1], mix_gate)
+    aside[...] = scalars
+    aside[:, LANES - units :] = shared[1].astype(jnp.float32)
+
     hidden = []
-    for s in range(members):
-        if s:
-            copies[s - 1].wait()
-        both = jnp.concatenate([packs[s][:width, :], packs[s][width : 2 * width, :]], axis=1)
-        both = wide_dot(values, both)
-        hidden.append((silu(both[:, :LANES]) * both[:, LANES:]).astype(jnp.bfloat16))
-    halves = [jnp.concatenate(hidden[i : i + 2], axis=1) for i in range(0, members, 2)]
+    first_hidden = hidden_of(values, resident, width)
+    for copy, pack in zip(copies, packs[:members] + packs[members + 1 :]):
+        copy.wait()
+        hidden.append(hidden_of(values, pack, width))
+    hidden.insert(members, first_hidden)
     ahead = jnp.where(core == 0, members - 1, 1)
-    for s, origin in enumerate((0, ahead, members - ahead, 2)):
-        dense = [
-            packs[s][pl.ds(shared_start + k * units, units), :] for k in range(per_member)
-        ]
-        dense = wide_dot(shared, jnp.concatenate(dense, axis=1))
-        columns[(member + origin) % members] = mix_gate * dense
+    origins = (0, ahead, members - ahead, 2)
+    for s, pair in enumerate((0, 2, 1, None)):
+        dense = wide_dot(shared[0], dense_of(packs[s], shared_start, units, per_member))
+        if pair is not None:
+            other = dense_of(packs[members + pair], shared_start, units, per_member)
+            dense = dense + wide_dot(shared[1], other)
+        columns[(member + origins[s]) % members] = mix_gate * dense
     for n in range(members):
-        firsts = [down_start + (n * per_member + k) * LANES for k in range(per_member)]
+        first = down_start + n * per_member * LANES
         total = columns[n]
-        for i in range(len(halves)):
-            down = [
-                jnp.concatenate(
-                    [packs[2 * i + s][first : first + LANES, :] for s in range(2)], axis=0
-                )
-                for first in firsts
-            ]
-            total = total + weight * wide_dot(halves[i], jnp.concatenate(down, axis=1))
-        for k in range(per_member):
-            for line in range(lines):
-                first = line // 2 * depth * 2 * blocks + n * depth * 2 * per_member
-                first = first + line % 2 * per_member + k
-                piece = total[line * depth : (line + 1) * depth, k * LANES : (k + 1) * LANES]
-                wide[pl.ds(first, depth, stride=2 * per_member), :] = piece
-    out[...] = wide[: count * blocks, :].astype(out.dtype)
-
-
-def add_kernel(own, pair, out):
-    out[...] = (own[...] + pair[...].astype(jnp.float32)).astype(jnp.bfloat16)
+        for side in range(2):
+            routed = jnp.zeros((count, per_member * LANES), jnp.float32)
+            for i in range(side * members, min((side + 1) * members, len(packs)), 2):
+                group = packs[i : min(i + 2, len(packs))]
+                left = jnp.concatenate(hidden[i : i + len(group)], axis=1)
+                routed = routed + wide_dot(left, down_of(group, first, per_member))
+            total = total + weights[side] * routed
+        place_columns(out, total, n, depth, lines, blocks, per_member)
+
+
+def dense_of(pack, shared_start, units, per_member):
+    parts = [pack[pl.ds(shared_start + k * units, units), :] for k in range(per_member)]
+    return jnp.concatenate(parts, axis=1)
+
+
+def last_kernel(partial, narrow, aside, pack, out, wide, columns):
+    members = lax.axis_size("tp")
+    member = lax.axis_index("tp")
+    count, width = narrow.shape
+    blocks = width // LANES
+    per_member = blocks // members
+    lines = lax.axis_size("ep_1") * 2
+    depth = count // lines
+    down_start = 2 * width
+    shared_start = down_start + blocks * LANES
+    units = (pack.shape[0] - shared_start) // per_member
+    weight = aside[:, 0:1]
+    mix_gate = aside[:, 1:2]
+    shared = aside[:, LANES - units :].astype(jnp.bfloat16)
+    hidden = hidden_of(narrow[...], pack, width)
+    dense = mix_gate * wide_dot(shared, dense_of(pack, shared_start, units, per_member))
+    columns[...] = jnp.zeros(columns.shape, jnp.float32)
+    columns[(member + 2) % members] = dense
+    for n in range(members):
+        first = down_start + n * per_member * LANES
+        routed = wide_dot(hidden, down_of([pack], first, per_member))
+        total = columns[n] + weight * routed
+        place_columns(wide, total, n, depth, lines, blocks, per_member)
+    out[...] = (partial[...] + wide[...]).astype(jnp.bfloat16)
 
 
 def fold_kernel(parts, out, wide, small):
@@ -382,7 +440,7 @@
     front = jnp.concatenate(front, axis=0)
     front = jnp.pad(front, ((0, LANES - front.shape[0]), (0, 0)))
 
-    sub_rows = peers * (blocks + NOTE_ROWS)
+    sub_rows = peers * (blocks + 1)
     residual, outgoing = pl.pallas_call(
         rows_kernel,
         in_specs=[VMEM] * 4,
@@ -396,33 +454,40 @@
     own_rows = lax.all_to_all(outgoing.reshape(-1, 2, LANES), EP[:2], 0, 0, tiled=True)
 
 
-    def share(rows, dtype):
-        return pl.pallas_call(
-            share_kernel,
-            in_specs=[VMEM] * 3 + [ANY] * (members - 1),
-            out_specs=VMEM,
-            out_shape=pltpu.VMEM((peers * blocks, LANES), dtype),
-            scratch_shapes=[
-                pltpu.VMEM((sub_rows, LANES), jnp.float32),
-                pltpu.VMEM((peers, width), jnp.bfloat16),
-                pltpu.VMEM((members, peers, width // members), jnp.float32),
-                pltpu.VMEM((members - 1, pack_rows, LANES), jnp.bfloat16),
-                pltpu.SemaphoreType.DMA((members - 1,)),
-            ],
-            name="share",
-        )(*map(in_vmem, (rows.reshape(sub_rows, LANES), front, packed)), *packs[1:])
-
-    pair_rows = swap(own_rows)
-    own_share = share(own_rows, jnp.float32)
-    pair_share = share(pair_rows, jnp.bfloat16)
-    pair_share = swap(pair_share)
+    pair_front = swap(front)
+    pair_packs = []
+    for pack in packs:
+        pair_packs.append(swap(pack))
+    streamed = packs + pair_packs[1:-1]
+    local_columns = pltpu.VMEM((members, peers, width // members), jnp.float32)
+    partial_share, narrow, aside = pl.pallas_call(
+        share_kernel,
+        in_specs=[VMEM] * 4 + [ANY] * len(streamed),
+        out_specs=[VMEM] * 3,
+        out_shape=[
+            pltpu.VMEM((peers * blocks, LANES), jnp.float32),
+            pltpu.VMEM((peers, width), jnp.bfloat16),
+            pltpu.VMEM((peers, LANES), jnp.float32),
+        ],
+        scratch_shapes=[
+            pltpu.VMEM((sub_rows, LANES), jnp.float32),
+            local_columns,
+            pltpu.VMEM((len(streamed), pack_rows, LANES), jnp.bfloat16),
+            pltpu.SemaphoreType.DMA((len(streamed),)),
+        ],
+        name="share",
+    )(
+        *map(in_vmem, (own_rows.reshape(sub_rows, LANES), front, pair_front, pair_packs[0])),
+        *streamed,
+    )
     total = pl.pallas_call(
-        add_kernel,
-        in_specs=[VMEM] * 2,
+        last_kernel,
+        in_specs=[VMEM] * 4,
         out_specs=VMEM,
-        out_shape=pltpu.VMEM(own_share.shape, jnp.bfloat16),
-        name="add",
-    )(in_vmem(own_share), in_vmem(pair_share))
+        out_shape=pltpu.VMEM((peers * blocks, LANES), jnp.bfloat16),
+        scratch_shapes=[pltpu.VMEM((peers * blocks, LANES), jnp.float32), local_columns],
+        name="last",
+    )(*map(in_vmem, (partial_share, narrow, aside)), pair_packs[-1])
     parts = lax.all_to_all(total.reshape(-1, 2, LANES), ("ep_1", "tp"), 0, 0, tiled=True)
     parts = parts.reshape(-1, LANES)
     rows = parts.shape[0] // lax.axis_size("ep_1")

time: 117 us -> 120 us (1.026)
  waiting for transfers between devices: 13.9 us -> 8.32 us
  blocking collectives: 43.5 us -> 47.2 us
  starting transfers between devices: 47.9 us -> 50 us
  local copies, waits for them, and re-layouts: 0.04 us -> 2.06 us
    ppermute x2 -> x5, starting transfers between devices: 21.7 us -> 16 us  [swap(): return lax.ppermute(shard, PAIR, [(0, 1), (1, 0)])]
    ppermute x3, starting transfers between devices: 7.77 us -> 12.5 us  [shifted(): return lax.ppermute(shard, (PAIR, 'tp'), pairs)]
    ppermute x3, waiting for transfers between devices: 11.3 us -> 7.16 us  [shifted(): return lax.ppermute(shard, (PAIR, 'tp'), pairs)]
    all_to_all x1, blocking collectives: 11.5 us -> 15.1 us  [per_device(): lax.all_to_all(total.reshape(-1, 2, LANES), ('ep_1', 'tp'), 0, 0, tiled=T...]
    all_to_all x1, starting transfers between devices: 18.4 us -> 21.6 us  [per_device(): lax.all_to_all(outgoing.reshape(-1, 2, LANES), EP[:2], 0, 0, tiled=True)]
    all_to_all x1, blocking collectives: 9.28 us -> 12.4 us  [per_device(): partial = lax.all_to_all(partial, 'tp', 0, 0, tiled=True)]
    all_to_all x1, blocking collectives: 22.8 us -> 19.7 us  [per_device(): parts = lax.all_to_all(parts.reshape(-1, 2, LANES), EP[0], 0, 0, tiled=True)]
    unnamed x14 -> x16, local copies, waits for them, and re-layouts: 0.03 us -> 2.06 us
  transfers between devices with their start and end apart: 6 -> 9, of which waited for: 4 -> 2; matrix products, arithmetic and copies ran while one was open for 0% -> 0% of each run, Pallas kernels for 2% -> 4%
where the time goes in v6:
time: 120 us; the launch traced here: 118 us
  starting transfers between devices  50 us (42%)
  blocking collectives  47.2 us (39%)
  Pallas kernels  9.82 us (8%)
  waiting for transfers between devices  8.32 us (7%)
  local copies, waits for them, and re-layouts  2.06 us (2%)
    all_to_all x1, starting transfers between devices, per_device(): lax.all_to_all(outgoing.reshape(-1, 2, LANES), EP[:2], 0, 0, tiled=True)  21.6 us
    all_to_all x1, blocking collectives, per_device(): parts = lax.all_to_all(parts.reshape(-1, 2, LANES), EP[0], 0, 0, tiled=True)  19.7 us
    ppermute x5, starting transfers between devices, swap(): return lax.ppermute(shard, PAIR, [(0, 1), (1, 0)])  16 us
    all_to_all x1, blocking collectives, per_device(): lax.all_to_all(total.reshape(-1, 2, LANES), ('ep_1', 'tp'), 0, 0, tiled=T...  15.1 us
    ppermute x3, starting transfers between devices, shifted(): return lax.ppermute(shard, (PAIR, 'tp'), pairs)  12.5 us
    all_to_all x1, blocking collectives, per_device(): partial = lax.all_to_all(partial, 'tp', 0, 0, tiled=True)  12.4 us
    ppermute x3, waiting for transfers between devices, shifted(): return lax.ppermute(shard, (PAIR, 'tp'), pairs)  7.16 us
    pallas_call x1, Pallas kernels, per_device(): pl.pallas_call(share_kernel, in_specs=[VMEM] * 4 + [ANY] * len(streamed),...  3.59 us
  transfers between devices with their start and end apart: 9, of which 2 were waited for; matrix products, arithmetic and copies ran while one was open for 0% of the time, Pallas kernels for 4%

profile of v6, /device:TPU:1, one launch (start us, length us, event | category | flops | bytes accessed | tf_op | source)
XLA Modules:
  0.0 118.3 jit_solution(13803387352585681762)
XLA Ops:
  0.7 3.0 %attend.1 = (bf16[4,8,1024]{2,1,0:T(8,128)(2,1)S(1)}, bf16[3136,128]{1,0:T(8,128)(2,1)S(1)}, f32[8,128]{1,0:T(8,128)S(1)}) custom-call(bf16[8,1024]{1,0:T(8,128)(2,1)} %tokens.1, bf16[1024]{0:T(1024)(128)(2,1)} %refs_1_.1, bf16[1024,256]{1,0:T(8,128)(2,1)} %refs_2_.1, bf16[128]{0:T(256)(128)(2,1)} %refs_3_.1, bf16[1024,128]{1,0:T(8,128)(2,1)} %refs_4_.1, ...), custom_call_target="tpu_custom_call" | custom-call | tf_op jit(solution)/shard_map/attend/pallas_call | solution.py:420
  3.6 0.0 copy-start
  3.6 5.5 %collective-permute-start.2 = (bf16[3136,128]{1,0:T(8,128)(2,1)S(1)}, bf16[3136,128]{1,0:T(8,128)(2,1)}, u32[]{:S(2)}, u32[]{:S(2)}) collective-permute-start(bf16[3136,128]{1,0:T(8,128)(2,1)S(1)} %get-tuple-element.16.refs_0_), channel_id=1, source_target_pairs={{0,1},{1,2},{2,3},{3,0},{4,7},{5,4},{6,5},{7,6},{8,9},{9,10},{10,1... | collective-permute-start | bytes 2408456 | tf_op jit(solution)/shard_map/ppermute | solution.py:43
  9.1 1.9 %collective-permute-start.3 = (bf16[3136,128]{1,0:T(8,128)(2,1)S(1)}, bf16[3136,128]{1,0:T(8,128)(2,1)}, u32[]{:S(2)}, u32[]{:S(2)}) collective-permute-start(bf16[3136,128]{1,0:T(8,128)(2,1)S(1)} %get-tuple-element.16.refs_0_), channel_id=1, source_target_pairs={{0,3},{1,0},{2,1},{3,2},{4,5},{5,6},{6,7},{7,4},{8,11},{9,8},{10,9... | collective-permute-start | bytes 2408456 | tf_op jit(solution)/shard_map/ppermute | solution.py:43
  11.0 7.2 %collective-permute-done.2.refs_1_ = bf16[3136,128]{1,0:T(8,128)(2,1)} collective-permute-done((bf16[3136,128]{1,0:T(8,128)(2,1)S(1)}, bf16[3136,128]{1,0:T(8,128)(2,1)}, u32[]{:S(2)}, u32[]{:S(2)}) %collective-permute-start.2) | collective-permute-done | bytes 802848 | tf_op jit(solution)/shard_map/ppermute | solution.py:43
  18.2 5.1 %collective-permute-start.4 = (bf16[3136,128]{1,0:T(8,128)(2,1)}, bf16[3136,128]{1,0:T(8,128)(2,1)}, u32[]{:S(2)}, u32[]{:S(2)}) collective-permute-start(bf16[3136,128]{1,0:T(8,128)(2,1)} %collective-permute-done.2.refs_1_), channel_id=1, source_target_pairs={{0,1},{1,2},{2,3},{3,0},{4,7},{5,4},{6,5},{7,6},{8,9},{9,10},{10,1... | collective-permute-start | bytes 2408456 | tf_op jit(solution)/shard_map/ppermute | solution.py:43
  23.3 0.0 copy-start.3
  23.3 0.0 copy-start.4
  23.3 12.4 %all_to_all.20.partial = bf16[4,8,1024]{2,1,0:T(8,128)(2,1)S(1)} all-to-all(bf16[4,8,1024]{2,1,0:T(8,128)(2,1)S(1)} %get-tuple-element.13), channel_id=1, replica_groups=mesh['ep_0'=16,'ep_1'=4,'ep_2'=2,'tp'=4] {'tp'}, dimensions={0} | all-to-all | bytes 131072 | tf_op jit(solution)/shard_map/all_to_all | solution.py:433
  35.8 0.0 copy-done.3
  35.8 0.0 copy-done.4
  35.8 0.9 rows.1
  36.7 0.0 copy-start.7
  36.7 0.0 copy-start.5
  36.7 0.0 copy-start.6
  36.7 21.6 %all-to-all-start.1 = ((bf16[576,2,128]{2,1,0:T(2,128)(2,1)}), bf16[576,2,128]{2,1,0:T(2,128)(2,1)S(1)}, u32[]{:S(2)}, u32[]{:S(2)}) async-start(bf16[576,2,128]{2,1,0:T(2,128)(2,1)} %bitcast.8), calls=%async_computation.1 | async-start | bytes 589824 | tf_op jit(solution)/shard_map/all_to_all | solution.py:454
  58.2 7.3 %collective-permute-start.1 = (bf16[3136,128]{1,0:T(8,128)(2,1)S(1)}, bf16[3136,128]{1,0:T(8,128)(2,1)S(1)}, u32[]{:S(2)}, u32[]{:S(2)}) collective-permute-start(bf16[3136,128]{1,0:T(8,128)(2,1)S(1)} %get-tuple-element.16.refs_0_), channel_id=1, source_target_pairs={{0,4},{4,0},{1,5},{5,1},{2,6},{6,2},{3,7},{7,3},{8,12},{12,8},{9,1... | collective-permute-start | bytes 2408456 | tf_op jit(solution)/shard_map/ppermute | solution.py:21
  65.6 1.9 %collective-permute-start.5 = (bf16[3136,128]{1,0:T(8,128)(2,1)}, bf16[3136,128]{1,0:T(8,128)(2,1)}, u32[]{:S(2)}, u32[]{:S(2)}) collective-permute-start(bf16[3136,128]{1,0:T(8,128)(2,1)} %collective-permute-done.2.refs_1_), channel_id=1, source_target_pairs={{0,4},{4,0},{1,5},{5,1},{2,6},{6,2},{3,7},{7,3},{8,12},{12,8},{9,1... | collective-permute-start | bytes 2408456 | tf_op jit(solution)/shard_map/ppermute | solution.py:21
  67.5 0.0 collective-permute-done.3.refs_2_
  67.5 2.4 %collective-permute-start.6 = (bf16[3136,128]{1,0:T(8,128)(2,1)}, bf16[3136,128]{1,0:T(8,128)(2,1)}, u32[]{:S(2)}, u32[]{:S(2)}) collective-permute-start(bf16[3136,128]{1,0:T(8,128)(2,1)} %collective-permute-done.3.refs_2_), channel_id=1, source_target_pairs={{0,4},{4,0},{1,5},{5,1},{2,6},{6,2},{3,7},{7,3},{8,12},{12,8},{9,1... | collective-permute-start | bytes 2408456 | tf_op jit(solution)/shard_map/ppermute | solution.py:21
  69.9 0.0 collective-permute-done.4.refs_3_
  69.9 1.9 %collective-permute-start.7 = (bf16[3136,128]{1,0:T(8,128)(2,1)}, bf16[3136,128]{1,0:T(8,128)(2,1)}, u32[]{:S(2)}, u32[]{:S(2)}) collective-permute-start(bf16[3136,128]{1,0:T(8,128)(2,1)} %collective-permute-done.4.refs_3_), channel_id=1, source_target_pairs={{0,4},{4,0},{1,5},{5,1},{2,6},{6,2},{3,7},{7,3},{8,12},{12,8},{9,1... | collective-permute-start | bytes 2408456 | tf_op jit(solution)/shard_map/ppermute | solution.py:21
  71.9 0.0 copy-done.7
  71.9 0.0 copy-done.5
  71.9 0.0 copy-done.6
  71.9 2.4 %collective-permute-start = (bf16[128,1024]{1,0:T(8,128)(2,1)S(1)}, bf16[128,1024]{1,0:T(8,128)(2,1)S(1)}, u32[]{:S(2)}, u32[]{:S(2)}) collective-permute-start(bf16[128,1024]{1,0:T(8,128)(2,1)S(1)} %fusion.4.front), channel_id=1, source_target_pairs={{0,4},{4,0},{1,5},{5,1},{2,6},{6,2},{3,7},{7,3},{8,12},{12,8},{9,1... | collective-permute-start | bytes 786440 | tf_op jit(solution)/shard_map/ppermute | solution.py:21
  74.3 1.1 collective-permute-done.pair_front
  75.5 0.0 collective-permute-done.1.resident
  75.5 0.0 copy-start.1
  75.5 0.9 copy-done.1
  76.4 0.0 all-to-all-done.1
  76.4 0.0 copy-done
  76.4 0.0 collective-permute-done.5.refs_4_
  76.4 0.0 collective-permute-done.6.refs_5_
  76.4 0.0 copy-start.2
  76.4 1.1 copy-done.2
  77.5 3.6 %share.1 = (f32[1024,128]{1,0:T(8,128)S(1)}, bf16[128,1024]{1,0:T(8,128)(2,1)S(1)}, f32[128,128]{1,0:T(8,128)S(1)}) custom-call(bf16[1152,128]{1,0:T(8,128)(2,1)S(1)} %bitcast.16, bf16[128,1024]{1,0:T(8,128)(2,1)S(1)} %fusion.4.front, bf16[128,1024]{1,0:T(8,128)(2,1)S(1)} %collective-permute-done.pair_front, bf16[3136,128]{1,0:T(8,128)(2,1)S(1)} %copy-done.2, ...), custom_call_target="tpu_custom_call" | custom-call | tf_op jit(solution)/shard_map/share/pallas_call | solution.py:463
  81.2 0.0 collective-permute-done.7.pack
  81.2 1.7 %last.1 = bf16[1024,128]{1,0:T(8,128)(2,1)S(1)} custom-call(f32[1024,128]{1,0:T(8,128)S(1)} %get-tuple-element.17.partial, bf16[128,1024]{1,0:T(8,128)(2,1)S(1)} %get-tuple-element.18.narrow, f32[128,128]{1,0:T(8,128)S(1)} %get-tuple-element.19.aside, bf16[3136,128]{1,0:T(8,128)(2,1)} %collective-permute-done.7.pack), custom_call_target="tpu_custom_call" | custom-call | tf_op jit(solution)/shard_map/last/pallas_call | solution.py:483
  82.9 15.1 %all_to_all.21 = bf16[512,2,128]{2,1,0:T(2,128)(2,1)S(1)} all-to-all(bf16[512,2,128]{2,1,0:T(2,128)(2,1)S(1)} %bitcast.18), channel_id=1, replica_groups=mesh['ep_0'=16,'ep_1'=4,'ep_2'=2,'tp'=4] {'ep_1','tp'}, dimensions={0} | all-to-all | bytes 524288 | tf_op jit(solution)/shard_map/all_to_all | solution.py:491
  97.9 0.1 fold.1
  98.0 19.7 %all_to_all.22 = bf16[128,2,128]{2,1,0:T(2,128)(2,1)S(1)} all-to-all(bf16[128,2,128]{2,1,0:T(2,128)(2,1)S(1)} %bitcast.19), channel_id=1, replica_groups=mesh['ep_0'=16,'ep_1'=4,'ep_2'=2,'tp'=4] {'ep_0'}, dimensions={0} | all-to-all | bytes 131072 | tf_op jit(solution)/shard_map/all_to_all | solution.py:505
  117.7 0.6 finish.1
  (2 shorter events, 0.0 us)
Async XLA Ops:
  3.6 72.8 %copy-start = (bf16[3136,128]{1,0:T(8,128)(2,1)}, bf16[3136,128]{1,0:T(8,128)(2,1)S(1)}, u32[]{:S(2)}) copy-start(bf16[3136,128]{1,0:T(8,128)(2,1)S(1)} %get-tuple-element.16.refs_0_) | copy-start | bytes 2408452
  3.6 14.6 %collective-permute-start.2 = (bf16[3136,128]{1,0:T(8,128)(2,1)S(1)}, bf16[3136,128]{1,0:T(8,128)(2,1)}, u32[]{:S(2)}, u32[]{:S(2)}) collective-permute-start(bf16[3136,128]{1,0:T(8,128)(2,1)S(1)} %get-tuple-element.16.refs_0_), channel_id=1, source_target_pairs={{0,1},{1,2},{2,3},{3,0},{4,7},{5,4},{6,5},{7,6},{8,9},{9,10},{10,1... | collective-permute-start | bytes 2408456 | tf_op jit(solution)/shard_map/ppermute | solution.py:43
  9.1 58.4 %collective-permute-start.3 = (bf16[3136,128]{1,0:T(8,128)(2,1)S(1)}, bf16[3136,128]{1,0:T(8,128)(2,1)}, u32[]{:S(2)}, u32[]{:S(2)}) collective-permute-start(bf16[3136,128]{1,0:T(8,128)(2,1)S(1)} %get-tuple-element.16.refs_0_), channel_id=1, source_target_pairs={{0,3},{1,0},{2,1},{3,2},{4,5},{5,6},{6,7},{7,4},{8,11},{9,8},{10,9... | collective-permute-start | bytes 2408456 | tf_op jit(solution)/shard_map/ppermute | solution.py:43
  18.2 51.7 %collective-permute-start.4 = (bf16[3136,128]{1,0:T(8,128)(2,1)}, bf16[3136,128]{1,0:T(8,128)(2,1)}, u32[]{:S(2)}, u32[]{:S(2)}) collective-permute-start(bf16[3136,128]{1,0:T(8,128)(2,1)} %collective-permute-done.2.refs_1_), channel_id=1, source_target_pairs={{0,1},{1,2},{2,3},{3,0},{4,7},{5,4},{6,5},{7,6},{8,9},{9,10},{10,1... | collective-permute-start | bytes 2408456 | tf_op jit(solution)/shard_map/ppermute | solution.py:43
  23.3 12.5 %copy-start.3 = (bf16[8,1024]{1,0:T(8,128)(2,1)S(1)}, bf16[8,1024]{1,0:T(8,128)(2,1)}, u32[]{:S(2)}) copy-start(bf16[8,1024]{1,0:T(8,128)(2,1)} %tokens.1) | copy-start | bytes 49156
  23.3 12.4 %copy-start.4 = (bf16[1024]{0:T(1024)(128)(2,1)S(1)}, bf16[1024]{0:T(1024)(128)(2,1)}, u32[]{:S(2)}) copy-start(bf16[1024]{0:T(1024)(128)(2,1)} %ffn_gain.1) | copy-start | bytes 6148
  36.7 35.2 %copy-start.7 = (bf16[1024]{0:T(1024)(128)(2,1)S(1)}, bf16[1024]{0:T(1024)(128)(2,1)}, u32[]{:S(2)}) copy-start(bf16[1024]{0:T(1024)(128)(2,1)} %param.39) | copy-start | bytes 6148
  36.7 35.2 %copy-start.5 = (bf16[1024,32]{0,1:T(8,128)(2,1)S(1)}, bf16[1024,32]{0,1:T(8,128)(2,1)}, u32[]{:S(2)}) copy-start(bf16[1024,32]{0,1:T(8,128)(2,1)} %param.41) | copy-start | bytes 196612
  36.7 35.2 %copy-start.6 = (bf16[1024,32]{0,1:T(8,128)(2,1)S(1)}, bf16[1024,32]{0,1:T(8,128)(2,1)}, u32[]{:S(2)}) copy-start(bf16[1024,32]{0,1:T(8,128)(2,1)} %param.40) | copy-start | bytes 196612
  36.7 39.7 %all-to-all-start.1 = ((bf16[576,2,128]{2,1,0:T(2,128)(2,1)}), bf16[576,2,128]{2,1,0:T(2,128)(2,1)S(1)}, u32[]{:S(2)}, u32[]{:S(2)}) async-start(bf16[576,2,128]{2,1,0:T(2,128)(2,1)} %bitcast.8), calls=%async_computation.1 | async-start | bytes 589824 | tf_op jit(solution)/shard_map/all_to_all | solution.py:454
  58.2 17.2 %collective-permute-start.1 = (bf16[3136,128]{1,0:T(8,128)(2,1)S(1)}, bf16[3136,128]{1,0:T(8,128)(2,1)S(1)}, u32[]{:S(2)}, u32[]{:S(2)}) collective-permute-start(bf16[3136,128]{1,0:T(8,128)(2,1)S(1)} %get-tuple-element.16.refs_0_), channel_id=1, source_target_pairs={{0,4},{4,0},{1,5},{5,1},{2,6},{6,2},{3,7},{7,3},{8,12},{12,8},{9,1... | collective-permute-start | bytes 2408456 | tf_op jit(solution)/shard_map/ppermute | solution.py:21
  65.6 10.8 %collective-permute-start.5 = (bf16[3136,128]{1,0:T(8,128)(2,1)}, bf16[3136,128]{1,0:T(8,128)(2,1)}, u32[]{:S(2)}, u32[]{:S(2)}) collective-permute-start(bf16[3136,128]{1,0:T(8,128)(2,1)} %collective-permute-done.2.refs_1_), channel_id=1, source_target_pairs={{0,4},{4,0},{1,5},{5,1},{2,6},{6,2},{3,7},{7,3},{8,12},{12,8},{9,1... | collective-permute-start | bytes 2408456 | tf_op jit(solution)/shard_map/ppermute | solution.py:21
  67.5 8.9 %collective-permute-start.6 = (bf16[3136,128]{1,0:T(8,128)(2,1)}, bf16[3136,128]{1,0:T(8,128)(2,1)}, u32[]{:S(2)}, u32[]{:S(2)}) collective-permute-start(bf16[3136,128]{1,0:T(8,128)(2,1)} %collective-permute-done.3.refs_2_), channel_id=1, source_target_pairs={{0,4},{4,0},{1,5},{5,1},{2,6},{6,2},{3,7},{7,3},{8,12},{12,8},{9,1... | collective-permute-start | bytes 2408456 | tf_op jit(solution)/shard_map/ppermute | solution.py:21
  69.9 11.2 %collective-permute-start.7 = (bf16[3136,128]{1,0:T(8,128)(2,1)}, bf16[3136,128]{1,0:T(8,128)(2,1)}, u32[]{:S(2)}, u32[]{:S(2)}) collective-permute-start(bf16[3136,128]{1,0:T(8,128)(2,1)} %collective-permute-done.4.refs_3_), channel_id=1, source_target_pairs={{0,4},{4,0},{1,5},{5,1},{2,6},{6,2},{3,7},{7,3},{8,12},{12,8},{9,1... | collective-permute-start | bytes 2408456 | tf_op jit(solution)/shard_map/ppermute | solution.py:21
  71.9 3.6 %collective-permute-start = (bf16[128,1024]{1,0:T(8,128)(2,1)S(1)}, bf16[128,1024]{1,0:T(8,128)(2,1)S(1)}, u32[]{:S(2)}, u32[]{:S(2)}) collective-permute-start(bf16[128,1024]{1,0:T(8,128)(2,1)S(1)} %fusion.4.front), channel_id=1, source_target_pairs={{0,4},{4,0},{1,5},{5,1},{2,6},{6,2},{3,7},{7,3},{8,12},{12,8},{9,1... | collective-permute-start | bytes 786440 | tf_op jit(solution)/shard_map/ppermute | solution.py:21
  75.5 0.9 copy-start.1
  76.4 1.1 copy-start.2

commit v7 on v6

--- a/solution.py
+++ b/solution.py
@@ -213,38 +213,47 @@
     return jnp.concatenate(columns, axis=1)
 
 
-def share_kernel(rows, front, pair_front, resident, *refs):
-    sources, refs = refs[:-7], refs[-7:]
-    out, narrow, aside, wide, columns, staged, sems = refs
+def share_kernel(rows, resident, *refs):
+    sources, refs = refs[:-10], refs[-10:]
+    out, narrow, aside, wide, columns, staged, fronts_in, marks_in, sems, front_sems = refs
     copies = []
-    for i, source in enumerate(sources):
+    for i, source in enumerate(sources[2:]):
         copies.append(pltpu.make_async_copy(source, staged.at[i], sems.at[i]))
-        copies[-1].start()
+    front_copies = []
+    for i, source in enumerate(sources[:2]):
+        front_copies.append(pltpu.make_async_copy(source, fronts_in.at[i], front_sems.at[i]))
+    for copy in copies[:1] + front_copies + copies[1:]:
+        copy.start()
     members = lax.axis_size("tp")
-    packs = [staged.at[i] for i in range(len(sources))]
-    packs.insert(members, resident)
+    packs = [resident] + [staged.at[i] for i in range(len(copies))]
     member = lax.axis_index("tp")
     core = lax.axis_index(PAIR)
     experts = (lax.axis_index(EP), lax.axis_index(EP) + 1 - 2 * core)
-    width = front.shape[1]
+    width = fronts_in.shape[2]
     count = narrow.shape[0]
     blocks = width // LANES
     stride = 2 * blocks + 2
     lines = lax.axis_size("ep_1") * 2
     depth = count // lines
-    wide[: rows.shape[0], :] = rows[...].astype(jnp.float32)
-    marks = []
-    for line in range(lines):
+    share_rows = rows.shape[0] // lines
+
+    @pl.loop(0, lines)
+    def _(line):
+        at = pl.ds(pl.multiple_of(line * share_rows, share_rows), share_rows)
+        wide[at, :] = rows[at, :].astype(jnp.float32)
+
+    @pl.loop(0, lines)
+    def _(line):
         chip, half = line // 2, line % 2
-        for k in range(blocks + 1):
-            first = chip * stride + (half * blocks + k if k < blocks else 2 * blocks + half)
+        at = pl.ds(pl.multiple_of(line * depth, depth), depth)
+        for k in range(blocks):
+            first = chip * stride + half * blocks + k
             piece = wide[pl.ds(first, depth, stride=lines // 2 * stride), :]
-            if k < blocks:
-                at = (slice(line * depth, (line + 1) * depth), slice(k * LANES, (k + 1) * LANES))
-                narrow[at] = piece.astype(jnp.bfloat16)
-            else:
-                marks.append(piece)
-    marks = jnp.concatenate(marks, axis=0)
+            narrow[at, k * LANES : (k + 1) * LANES] = piece.astype(jnp.bfloat16)
+        first = chip * stride + 2 * blocks + half
+        marks_in[at, :] = wide[pl.ds(first, depth, stride=lines // 2 * stride), :]
+
+    marks = marks_in[...]
     weights = []
     for expert in experts:
         weight = jnp.zeros((count, 1), jnp.float32)
@@ -259,11 +268,14 @@
     per_member = blocks // members
     units = (resident.shape[0] - shared_start) // per_member
 
+    hidden = [hidden_of(values, resident, width)]
+    for copy in front_copies:
+        copy.wait()
     fronts = [
         lax.dot_general(
             values, each[...], (((1,), (1,)), ((), ())), preferred_element_type=jnp.float32
         )
-        for each in (front, pair_front)
+        for each in (fronts_in.at[0], fronts_in.at[1])
     ]
     mix_gate = 1.0 / (1.0 + jnp.exp(-fronts[0][:, 2 * units : 2 * units + 1]))
     shared = [silu(pre[:, :units]) * pre[:, units : 2 * units] for pre in fronts]
@@ -273,12 +285,9 @@
     aside[...] = scalars
     aside[:, LANES - units :] = shared[1].astype(jnp.float32)
 
-    hidden = []
-    first_hidden = hidden_of(values, resident, width)
-    for copy, pack in zip(copies, packs[:members] + packs[members + 1 :]):
+    for copy, pack in zip(copies, packs[1:]):
         copy.wait()
         hidden.append(hidden_of(values, pack, width))
-    hidden.insert(members, first_hidden)
     ahead = jnp.where(core == 0, members - 1, 1)
     origins = (0, ahead, members - ahead, 2)
     for s, pair in enumerate((0, 2, 1, None)):
@@ -305,7 +314,12 @@
     return jnp.concatenate(parts, axis=1)
 
 
-def last_kernel(partial, narrow, aside, pack, out, wide, columns):
+def last_kernel(partial, narrow, aside, source, out, wide, columns, pack, sems):
+    split = 2 * narrow.shape[1]
+    copies = []
+    for i, rows in enumerate((pl.ds(0, split), pl.ds(split, source.shape[0] - split))):
+        copies.append(pltpu.make_async_copy(source.at[rows, :], pack.at[rows, :], sems.at[i]))
+        copies[-1].start()
     members = lax.axis_size("tp")
     member = lax.axis_index("tp")
     count, width = narrow.shape
@@ -319,7 +333,9 @@
     weight = aside[:, 0:1]
     mix_gate = aside[:, 1:2]
     shared = aside[:, LANES - units :].astype(jnp.bfloat16)
+    copies[0].wait()
     hidden = hidden_of(narrow[...], pack, width)
+    copies[1].wait()
     dense = mix_gate * wide_dot(shared, dense_of(pack, shared_start, units, per_member))
     columns[...] = jnp.zeros(columns.shape, jnp.float32)
     columns[(member + 2) % members] = dense
@@ -458,11 +474,11 @@
     pair_packs = []
     for pack in packs:
         pair_packs.append(swap(pack))
-    streamed = packs + pair_packs[1:-1]
+    streamed = packs[1:] + pair_packs[:-1]
     local_columns = pltpu.VMEM((members, peers, width // members), jnp.float32)
     partial_share, narrow, aside = pl.pallas_call(
         share_kernel,
-        in_specs=[VMEM] * 4 + [ANY] * len(streamed),
+        in_specs=[VMEM] * 2 + [ANY] * (2 + len(streamed)),
         out_specs=[VMEM] * 3,
         out_shape=[
             pltpu.VMEM((peers * blocks, LANES), jnp.float32),
@@ -473,19 +489,29 @@
             pltpu.VMEM((sub_rows, LANES), jnp.float32),
             local_columns,
             pltpu.VMEM((len(streamed), pack_rows, LANES), jnp.bfloat16),
+            pltpu.VMEM((2, LANES, width), jnp.bfloat16),
+            pltpu.VMEM((peers, LANES), jnp.float32),
             pltpu.SemaphoreType.DMA((len(streamed),)),
+            pltpu.SemaphoreType.DMA((2,)),
         ],
         name="share",
     )(
-        *map(in_vmem, (own_rows.reshape(sub_rows, LANES), front, pair_front, pair_packs[0])),
+        *map(in_vmem, (own_rows.reshape(sub_rows, LANES), packed)),
+        front,
+        pair_front,
         *streamed,
     )
     total = pl.pallas_call(
         last_kernel,
-        in_specs=[VMEM] * 4,
+        in_specs=[VMEM] * 3 + [ANY],
         out_specs=VMEM,
         out_shape=pltpu.VMEM((peers * blocks, LANES), jnp.bfloat16),
-        scratch_shapes=[pltpu.VMEM((peers * blocks, LANES), jnp.float32), local_columns],
+        scratch_shapes=[
+            pltpu.VMEM((peers * blocks, LANES), jnp.float32),
+            local_columns,
+            pltpu.VMEM((pack_rows, LANES), jnp.bfloat16),
+            pltpu.SemaphoreType.DMA((2,)),
+        ],
         name="last",
     )(*map(in_vmem, (partial_share, narrow, aside)), pair_packs[-1])
     parts = lax.all_to_all(total.reshape(-1, 2, LANES), ("ep_1", "tp"), 0, 0, tiled=True)

time: 120 us -> 120 us (level)
  Pallas kernels: 9.82 us -> 11.2 us
    pallas_call x2, Pallas kernels: 5.29 us -> 6.68 us  [the longest x1 4.94 us: per_device(): pl.pallas_call(share_kernel, in_specs=[VMEM] * 2 + [ANY] * (2 + len(strea...]
  transfers between devices with their start and end apart: 9 -> 9, of which waited for: 2 -> 3; matrix products, arithmetic and copies ran while one was open for 0% -> 0% of each run, Pallas kernels for 4% -> 5%
where the time goes in v7:
time: 120 us; the launch traced here: 118 us
  starting transfers between devices  49.6 us (41%)
  blocking collectives  46.4 us (39%)
  Pallas kernels  11.2 us (9%)
  waiting for transfers between devices  9.24 us (8%)
    all_to_all x1, starting transfers between devices, per_device(): lax.all_to_all(outgoing.reshape(-1, 2, LANES), EP[:2], 0, 0, tiled=True)  21.4 us
    all_to_all x1, blocking collectives, per_device(): parts = lax.all_to_all(parts.reshape(-1, 2, LANES), EP[0], 0, 0, tiled=True)  18.6 us
    ppermute x5, starting transfers between devices, swap(): return lax.ppermute(shard, PAIR, [(0, 1), (1, 0)])  15.9 us
    all_to_all x1, blocking collectives, per_device(): lax.all_to_all(total.reshape(-1, 2, LANES), ('ep_1', 'tp'), 0, 0, tiled=T...  15.3 us
    all_to_all x1, blocking collectives, per_device(): partial = lax.all_to_all(partial, 'tp', 0, 0, tiled=True)  12.5 us
    ppermute x3, starting transfers between devices, shifted(): return lax.ppermute(shard, (PAIR, 'tp'), pairs)  12.4 us
    ppermute x3, waiting for transfers between devices, shifted(): return lax.ppermute(shard, (PAIR, 'tp'), pairs)  7.16 us
    pallas_call x1, Pallas kernels, per_device(): pl.pallas_call(share_kernel, in_specs=[VMEM] * 2 + [ANY] * (2 + len(strea...  4.94 us
  transfers between devices with their start and end apart: 9, of which 3 were waited for; matrix products, arithmetic and copies ran while one was open for 0% of the time, Pallas kernels for 5%

profile of v7, /device:TPU:1, one launch (start us, length us, event | category | flops | bytes accessed | tf_op | source)
XLA Modules:
  0.0 118.4 jit_solution(13826186587642056664)
XLA Ops:
  0.7 3.0 %attend.1 = (bf16[4,8,1024]{2,1,0:T(8,128)(2,1)S(1)}, bf16[3136,128]{1,0:T(8,128)(2,1)S(1)}, f32[8,128]{1,0:T(8,128)S(1)}) custom-call(bf16[8,1024]{1,0:T(8,128)(2,1)} %tokens.1, bf16[1024]{0:T(1024)(128)(2,1)} %refs_1_.1, bf16[1024,256]{1,0:T(8,128)(2,1)} %refs_2_.1, bf16[128]{0:T(256)(128)(2,1)} %refs_3_.1, bf16[1024,128]{1,0:T(8,128)(2,1)} %refs_4_.1, ...), custom_call_target="tpu_custom_call" | custom-call | tf_op jit(solution)/shard_map/attend/pallas_call | solution.py:436
  3.6 5.5 %collective-permute-start.1 = (bf16[3136,128]{1,0:T(8,128)(2,1)S(1)}, bf16[3136,128]{1,0:T(8,128)(2,1)S(1)}, u32[]{:S(2)}, u32[]{:S(2)}) collective-permute-start(bf16[3136,128]{1,0:T(8,128)(2,1)S(1)} %get-tuple-element.16.resident), channel_id=1, source_target_pairs={{0,1},{1,2},{2,3},{3,0},{4,7},{5,4},{6,5},{7,6},{8,9},{9,10},{10,1... | collective-permute-start | bytes 2408456 | tf_op jit(solution)/shard_map/ppermute | solution.py:43
  9.1 1.9 %collective-permute-start.2 = (bf16[3136,128]{1,0:T(8,128)(2,1)S(1)}, bf16[3136,128]{1,0:T(8,128)(2,1)}, u32[]{:S(2)}, u32[]{:S(2)}) collective-permute-start(bf16[3136,128]{1,0:T(8,128)(2,1)S(1)} %get-tuple-element.16.resident), channel_id=1, source_target_pairs={{0,3},{1,0},{2,1},{3,2},{4,5},{5,6},{6,7},{7,4},{8,11},{9,8},{10,9... | collective-permute-start | bytes 2408456 | tf_op jit(solution)/shard_map/ppermute | solution.py:43
  11.0 7.2 %collective-permute-done.1.refs_2_ = bf16[3136,128]{1,0:T(8,128)(2,1)S(1)} collective-permute-done((bf16[3136,128]{1,0:T(8,128)(2,1)S(1)}, bf16[3136,128]{1,0:T(8,128)(2,1)S(1)}, u32[]{:S(2)}, u32[]{:S(2)}) %collective-permute-start.1) | collective-permute-done | bytes 802848 | tf_op jit(solution)/shard_map/ppermute | solution.py:43
  18.2 0.0 copy-start.3
  18.2 5.0 %collective-permute-start.3 = (bf16[3136,128]{1,0:T(8,128)(2,1)S(1)}, bf16[3136,128]{1,0:T(8,128)(2,1)}, u32[]{:S(2)}, u32[]{:S(2)}) collective-permute-start(bf16[3136,128]{1,0:T(8,128)(2,1)S(1)} %collective-permute-done.1.refs_2_), channel_id=1, source_target_pairs={{0,1},{1,2},{2,3},{3,0},{4,7},{5,4},{6,5},{7,6},{8,9},{9,10},{10,1... | collective-permute-start | bytes 2408456 | tf_op jit(solution)/shard_map/ppermute | solution.py:43
  23.2 0.0 copy-start
  23.2 0.0 copy-start.1
  23.2 12.5 %all_to_all.20.partial = bf16[4,8,1024]{2,1,0:T(8,128)(2,1)S(1)} all-to-all(bf16[4,8,1024]{2,1,0:T(8,128)(2,1)S(1)} %get-tuple-element.13), channel_id=1, replica_groups=mesh['ep_0'=16,'ep_1'=4,'ep_2'=2,'tp'=4] {'tp'}, dimensions={0} | all-to-all | bytes 131072 | tf_op jit(solution)/shard_map/all_to_all | solution.py:449
  35.8 0.0 copy-done
  35.8 0.0 copy-done.1
  35.8 0.9 rows.1
  36.6 0.0 copy-start.8
  36.6 0.0 copy-start.6
  36.6 0.0 copy-start.7
  36.6 21.4 %all-to-all-start.1 = ((bf16[576,2,128]{2,1,0:T(2,128)(2,1)}), bf16[576,2,128]{2,1,0:T(2,128)(2,1)S(1)}, u32[]{:S(2)}, u32[]{:S(2)}) async-start(bf16[576,2,128]{2,1,0:T(2,128)(2,1)} %bitcast.8), calls=%async_computation.1 | async-start | bytes 589824 | tf_op jit(solution)/shard_map/all_to_all | solution.py:470
  58.0 7.2 %collective-permute-start.4 = (bf16[3136,128]{1,0:T(8,128)(2,1)S(1)}, bf16[3136,128]{1,0:T(8,128)(2,1)}, u32[]{:S(2)}, u32[]{:S(2)}) collective-permute-start(bf16[3136,128]{1,0:T(8,128)(2,1)S(1)} %get-tuple-element.16.resident), channel_id=1, source_target_pairs={{0,4},{4,0},{1,5},{5,1},{2,6},{6,2},{3,7},{7,3},{8,12},{12,8},{9,1... | collective-permute-start | bytes 2408456 | tf_op jit(solution)/shard_map/ppermute | solution.py:21
  65.2 0.0 collective-permute-done.2.refs_3_
  65.3 1.9 %collective-permute-start.6 = (bf16[3136,128]{1,0:T(8,128)(2,1)}, bf16[3136,128]{1,0:T(8,128)(2,1)S(1)}, u32[]{:S(2)}, u32[]{:S(2)}) collective-permute-start(bf16[3136,128]{1,0:T(8,128)(2,1)} %collective-permute-done.2.refs_3_), channel_id=1, source_target_pairs={{0,4},{4,0},{1,5},{5,1},{2,6},{6,2},{3,7},{7,3},{8,12},{12,8},{9,1... | collective-permute-start | bytes 2408456 | tf_op jit(solution)/shard_map/ppermute | solution.py:21
  67.2 2.4 %collective-permute-start.5 = (bf16[3136,128]{1,0:T(8,128)(2,1)S(1)}, bf16[3136,128]{1,0:T(8,128)(2,1)}, u32[]{:S(2)}, u32[]{:S(2)}) collective-permute-start(bf16[3136,128]{1,0:T(8,128)(2,1)S(1)} %collective-permute-done.1.refs_2_), channel_id=1, source_target_pairs={{0,4},{4,0},{1,5},{5,1},{2,6},{6,2},{3,7},{7,3},{8,12},{12,8},{9,1... | collective-permute-start | bytes 2408456 | tf_op jit(solution)/shard_map/ppermute | solution.py:21
  69.6 0.0 collective-permute-done.3.refs_4_
  69.6 1.9 %collective-permute-start.7 = (bf16[3136,128]{1,0:T(8,128)(2,1)}, bf16[3136,128]{1,0:T(8,128)(2,1)}, u32[]{:S(2)}, u32[]{:S(2)}) collective-permute-start(bf16[3136,128]{1,0:T(8,128)(2,1)} %collective-permute-done.3.refs_4_), channel_id=1, source_target_pairs={{0,4},{4,0},{1,5},{5,1},{2,6},{6,2},{3,7},{7,3},{8,12},{12,8},{9,1... | collective-permute-start | bytes 2408456 | tf_op jit(solution)/shard_map/ppermute | solution.py:21
  71.5 0.0 copy-done.8
  71.6 0.0 copy-done.6
  71.6 0.0 copy-done.7
  71.6 0.0 copy-start.2
  71.6 2.4 %collective-permute-start = (bf16[128,1024]{1,0:T(8,128)(2,1)S(1)}, bf16[128,1024]{1,0:T(8,128)(2,1)S(1)}, u32[]{:S(2)}, u32[]{:S(2)}) collective-permute-start(bf16[128,1024]{1,0:T(8,128)(2,1)S(1)} %fusion.4.refs_0_), channel_id=1, source_target_pairs={{0,4},{4,0},{1,5},{5,1},{2,6},{6,2},{3,7},{7,3},{8,12},{12,8},{9,1... | collective-permute-start | bytes 786440 | tf_op jit(solution)/shard_map/ppermute | solution.py:21
  74.0 1.1 collective-permute-done.refs_1_
  75.2 0.0 copy-start.5
  75.2 0.0 collective-permute-done.4.refs_5_
  75.2 0.9 all-to-all-done.1
  76.1 0.0 collective-permute-done.6.refs_7_
  76.1 0.0 copy-start.4
  76.1 0.0 collective-permute-done.5.refs_6_
  76.1 0.9 copy-done.4
  77.0 0.0 copy-done.3
  77.0 0.0 copy-done.2
  77.0 0.0 copy-done.5
  77.0 4.9 %share.1 = (f32[1024,128]{1,0:T(8,128)S(1)}, bf16[128,1024]{1,0:T(8,128)(2,1)S(1)}, f32[128,128]{1,0:T(8,128)S(1)}) custom-call(bf16[1152,128]{1,0:T(8,128)(2,1)S(1)} %bitcast.16, bf16[3136,128]{1,0:T(8,128)(2,1)S(1)} %get-tuple-element.16.resident, bf16[128,1024]{1,0:T(8,128)(2,1)} %copy-done.2, bf16[128,1024]{1,0:T(8,128)(2,1)} %copy-done.5, ...), custom_call_target="tpu_custom_call" | custom-call | tf_op jit(solution)/shard_map/share/pallas_call | solution.py:479
  82.0 0.0 collective-permute-done.7.source
  82.0 1.7 %last.1 = bf16[1024,128]{1,0:T(8,128)(2,1)S(1)} custom-call(f32[1024,128]{1,0:T(8,128)S(1)} %get-tuple-element.17.partial, bf16[128,1024]{1,0:T(8,128)(2,1)S(1)} %get-tuple-element.18.narrow, f32[128,128]{1,0:T(8,128)S(1)} %get-tuple-element.19.aside, bf16[3136,128]{1,0:T(8,128)(2,1)} %collective-permute-done.7.source), custom_call_target="tpu_custom_call" | custom-call | tf_op jit(solution)/shard_map/last/pallas_call | solution.py:504
  83.8 15.3 %all_to_all.21 = bf16[512,2,128]{2,1,0:T(2,128)(2,1)S(1)} all-to-all(bf16[512,2,128]{2,1,0:T(2,128)(2,1)S(1)} %bitcast.18), channel_id=1, replica_groups=mesh['ep_0'=16,'ep_1'=4,'ep_2'=2,'tp'=4] {'ep_1','tp'}, dimensions={0} | all-to-all | bytes 524288 | tf_op jit(solution)/shard_map/all_to_all | solution.py:517
  99.1 0.1 fold.1
  99.1 18.6 %all_to_all.22 = bf16[128,2,128]{2,1,0:T(2,128)(2,1)S(1)} all-to-all(bf16[128,2,128]{2,1,0:T(2,128)(2,1)S(1)} %bitcast.19), channel_id=1, replica_groups=mesh['ep_0'=16,'ep_1'=4,'ep_2'=2,'tp'=4] {'ep_0'}, dimensions={0} | all-to-all | bytes 131072 | tf_op jit(solution)/shard_map/all_to_all | solution.py:531
  117.7 0.6 finish.1
  (2 shorter events, 0.0 us)
Async XLA Ops:
  3.6 14.6 %collective-permute-start.1 = (bf16[3136,128]{1,0:T(8,128)(2,1)S(1)}, bf16[3136,128]{1,0:T(8,128)(2,1)S(1)}, u32[]{:S(2)}, u32[]{:S(2)}) collective-permute-start(bf16[3136,128]{1,0:T(8,128)(2,1)S(1)} %get-tuple-element.16.resident), channel_id=1, source_target_pairs={{0,1},{1,2},{2,3},{3,0},{4,7},{5,4},{6,5},{7,6},{8,9},{9,10},{10,1... | collective-permute-start | bytes 2408456 | tf_op jit(solution)/shard_map/ppermute | solution.py:43
  9.1 56.2 %collective-permute-start.2 = (bf16[3136,128]{1,0:T(8,128)(2,1)S(1)}, bf16[3136,128]{1,0:T(8,128)(2,1)}, u32[]{:S(2)}, u32[]{:S(2)}) collective-permute-start(bf16[3136,128]{1,0:T(8,128)(2,1)S(1)} %get-tuple-element.16.resident), channel_id=1, source_target_pairs={{0,3},{1,0},{2,1},{3,2},{4,5},{5,6},{6,7},{7,4},{8,11},{9,8},{10,9... | collective-permute-start | bytes 2408456 | tf_op jit(solution)/shard_map/ppermute | solution.py:43
  18.2 58.9 %copy-start.3 = (bf16[3136,128]{1,0:T(8,128)(2,1)}, bf16[3136,128]{1,0:T(8,128)(2,1)S(1)}, u32[]{:S(2)}) copy-start(bf16[3136,128]{1,0:T(8,128)(2,1)S(1)} %collective-permute-done.1.refs_2_) | copy-start | bytes 2408452
  18.2 51.4 %collective-permute-start.3 = (bf16[3136,128]{1,0:T(8,128)(2,1)S(1)}, bf16[3136,128]{1,0:T(8,128)(2,1)}, u32[]{:S(2)}, u32[]{:S(2)}) collective-permute-start(bf16[3136,128]{1,0:T(8,128)(2,1)S(1)} %collective-permute-done.1.refs_2_), channel_id=1, source_target_pairs={{0,1},{1,2},{2,3},{3,0},{4,7},{5,4},{6,5},{7,6},{8,9},{9,10},{10,1... | collective-permute-start | bytes 2408456 | tf_op jit(solution)/shard_map/ppermute | solution.py:43
  23.2 12.6 %copy-start = (bf16[8,1024]{1,0:T(8,128)(2,1)S(1)}, bf16[8,1024]{1,0:T(8,128)(2,1)}, u32[]{:S(2)}) copy-start(bf16[8,1024]{1,0:T(8,128)(2,1)} %tokens.1) | copy-start | bytes 49156
  23.2 12.5 %copy-start.1 = (bf16[1024]{0:T(1024)(128)(2,1)S(1)}, bf16[1024]{0:T(1024)(128)(2,1)}, u32[]{:S(2)}) copy-start(bf16[1024]{0:T(1024)(128)(2,1)} %ffn_gain.1) | copy-start | bytes 6148
  36.6 34.9 %copy-start.8 = (bf16[1024]{0:T(1024)(128)(2,1)S(1)}, bf16[1024]{0:T(1024)(128)(2,1)}, u32[]{:S(2)}) copy-start(bf16[1024]{0:T(1024)(128)(2,1)} %param.39) | copy-start | bytes 6148
  36.6 34.9 %copy-start.6 = (bf16[1024,32]{0,1:T(8,128)(2,1)S(1)}, bf16[1024,32]{0,1:T(8,128)(2,1)}, u32[]{:S(2)}) copy-start(bf16[1024,32]{0,1:T(8,128)(2,1)} %param.41) | copy-start | bytes 196612
  36.6 34.9 %copy-start.7 = (bf16[1024,32]{0,1:T(8,128)(2,1)S(1)}, bf16[1024,32]{0,1:T(8,128)(2,1)}, u32[]{:S(2)}) copy-start(bf16[1024,32]{0,1:T(8,128)(2,1)} %param.40) | copy-start | bytes 196612
  36.6 39.5 %all-to-all-start.1 = ((bf16[576,2,128]{2,1,0:T(2,128)(2,1)}), bf16[576,2,128]{2,1,0:T(2,128)(2,1)S(1)}, u32[]{:S(2)}, u32[]{:S(2)}) async-start(bf16[576,2,128]{2,1,0:T(2,128)(2,1)} %bitcast.8), calls=%async_computation.1 | async-start | bytes 589824 | tf_op jit(solution)/shard_map/all_to_all | solution.py:470
  58.0 17.1 %collective-permute-start.4 = (bf16[3136,128]{1,0:T(8,128)(2,1)S(1)}, bf16[3136,128]{1,0:T(8,128)(2,1)}, u32[]{:S(2)}, u32[]{:S(2)}) collective-permute-start(bf16[3136,128]{1,0:T(8,128)(2,1)S(1)} %get-tuple-element.16.resident), channel_id=1, source_target_pairs={{0,4},{4,0},{1,5},{5,1},{2,6},{6,2},{3,7},{7,3},{8,12},{12,8},{9,1... | collective-permute-start | bytes 2408456 | tf_op jit(solution)/shard_map/ppermute | solution.py:21
  65.3 10.9 %collective-permute-start.6 = (bf16[3136,128]{1,0:T(8,128)(2,1)}, bf16[3136,128]{1,0:T(8,128)(2,1)S(1)}, u32[]{:S(2)}, u32[]{:S(2)}) collective-permute-start(bf16[3136,128]{1,0:T(8,128)(2,1)} %collective-permute-done.2.refs_3_), channel_id=1, source_target_pairs={{0,4},{4,0},{1,5},{5,1},{2,6},{6,2},{3,7},{7,3},{8,12},{12,8},{9,1... | collective-permute-start | bytes 2408456 | tf_op jit(solution)/shard_map/ppermute | solution.py:21
  67.2 8.9 %collective-permute-start.5 = (bf16[3136,128]{1,0:T(8,128)(2,1)S(1)}, bf16[3136,128]{1,0:T(8,128)(2,1)}, u32[]{:S(2)}, u32[]{:S(2)}) collective-permute-start(bf16[3136,128]{1,0:T(8,128)(2,1)S(1)} %collective-permute-done.1.refs_2_), channel_id=1, source_target_pairs={{0,4},{4,0},{1,5},{5,1},{2,6},{6,2},{3,7},{7,3},{8,12},{12,8},{9,1... | collective-permute-start | bytes 2408456 | tf_op jit(solution)/shard_map/ppermute | solution.py:21
  69.6 12.4 %collective-permute-start.7 = (bf16[3136,128]{1,0:T(8,128)(2,1)}, bf16[3136,128]{1,0:T(8,128)(2,1)}, u32[]{:S(2)}, u32[]{:S(2)}) collective-permute-start(bf16[3136,128]{1,0:T(8,128)(2,1)} %collective-permute-done.3.refs_4_), channel_id=1, source_target_pairs={{0,4},{4,0},{1,5},{5,1},{2,6},{6,2},{3,7},{7,3},{8,12},{12,8},{9,1... | collective-permute-start | bytes 2408456 | tf_op jit(solution)/shard_map/ppermute | solution.py:21
  71.6 5.4 %copy-start.2 = (bf16[128,1024]{1,0:T(8,128)(2,1)}, bf16[128,1024]{1,0:T(8,128)(2,1)S(1)}, u32[]{:S(2)}) copy-start(bf16[128,1024]{1,0:T(8,128)(2,1)S(1)} %fusion.4.refs_0_) | copy-start | bytes 786436
  71.6 3.6 %collective-permute-start = (bf16[128,1024]{1,0:T(8,128)(2,1)S(1)}, bf16[128,1024]{1,0:T(8,128)(2,1)S(1)}, u32[]{:S(2)}, u32[]{:S(2)}) collective-permute-start(bf16[128,1024]{1,0:T(8,128)(2,1)S(1)} %fusion.4.refs_0_), channel_id=1, source_target_pairs={{0,4},{4,0},{1,5},{5,1},{2,6},{6,2},{3,7},{7,3},{8,12},{12,8},{9,1... | collective-permute-start | bytes 786440 | tf_op jit(solution)/shard_map/ppermute | solution.py:21
  75.2 1.9 %copy-start.5 = (bf16[128,1024]{1,0:T(8,128)(2,1)}, bf16[128,1024]{1,0:T(8,128)(2,1)S(1)}, u32[]{:S(2)}) copy-start(bf16[128,1024]{1,0:T(8,128)(2,1)S(1)} %collective-permute-done.refs_1_) | copy-start | bytes 786436
  76.1 0.9 copy-start.4

commit v8 on v6

--- a/solution.py
+++ b/solution.py
@@ -237,8 +237,8 @@
     for line in range(lines):
         chip, half = line // 2, line % 2
         for k in range(blocks + 1):
-            first = chip * stride + (half * blocks + k if k < blocks else 2 * blocks + half)
-            piece = wide[pl.ds(first, depth, stride=lines // 2 * stride), :]
+            first = half * blocks + k if k < blocks else 2 * blocks + half
+            piece = wide[pl.ds(chip * depth * stride + first, depth, stride=stride), :]
             if k < blocks:
                 at = (slice(line * depth, (line + 1) * depth), slice(k * LANES, (k + 1) * LANES))
                 narrow[at] = piece.astype(jnp.bfloat16)
@@ -441,17 +441,20 @@
     front = jnp.pad(front, ((0, LANES - front.shape[0]), (0, 0)))
 
     sub_rows = peers * (blocks + 1)
+    sent_rows = sub_rows // lax.axis_size(EP[1])
     residual, outgoing = pl.pallas_call(
         rows_kernel,
         in_specs=[VMEM] * 4,
         out_specs=[VMEM, VMEM],
         out_shape=[
             pltpu.VMEM((seqs, width // members), jnp.float32),
-            pltpu.VMEM((sub_rows, LANES), jnp.bfloat16),
+            pltpu.VMEM((sent_rows, LANES), jnp.bfloat16),
         ],
         name="rows",
     )(*map(in_vmem, (partial, tokens, ffn_gain, notes)))
-    own_rows = lax.all_to_all(outgoing.reshape(-1, 2, LANES), EP[:2], 0, 0, tiled=True)
+    column = lax.all_to_all(outgoing.reshape(-1, 2, LANES), EP[0], 0, 0, tiled=True)
+    copies_out = jnp.tile(column, (lax.axis_size(EP[1]), 1, 1))
+    own_rows = lax.all_to_all(copies_out, EP[1], 0, 0, tiled=True)
 
 
     pair_front = swap(front)

time: 120 us -> 127 us (1.058)
  the two profiles are of different devices: /device:TPU:1 before, /device:TPU:32 now
where the time goes in v8:
time: 127 us; the launch traced here: 126 us
  starting transfers between devices  40.6 us (32%)
  waiting for transfers between devices  36.4 us (29%)
  blocking collectives  36.3 us (29%)
  Pallas kernels  10.8 us (9%)
    ppermute x3, waiting for transfers between devices, shifted(): return lax.ppermute(shard, (PAIR, 'tp'), pairs)  19.7 us
    all_to_all x1, blocking collectives, per_device(): parts = lax.all_to_all(parts.reshape(-1, 2, LANES), EP[0], 0, 0, tiled=True)  15.6 us
    all_to_all x1, starting transfers between devices, per_device(): lax.all_to_all(outgoing.reshape(-1, 2, LANES), EP[0], 0, 0, tiled=True)  15.3 us
    all_to_all x1, blocking collectives, per_device(): lax.all_to_all(total.reshape(-1, 2, LANES), ('ep_1', 'tp'), 0, 0, tiled=T...  11.5 us
    ppermute x3, starting transfers between devices, shifted(): return lax.ppermute(shard, (PAIR, 'tp'), pairs)  10.9 us
    ppermute x5, starting transfers between devices, swap(): return lax.ppermute(shard, PAIR, [(0, 1), (1, 0)])  10.1 us
    all_to_all x1, waiting for transfers between devices, per_device(): lax.all_to_all(outgoing.reshape(-1, 2, LANES), EP[0], 0, 0, tiled=True)  9.8 us
    all_to_all x1, blocking collectives, per_device(): partial = lax.all_to_all(partial, 'tp', 0, 0, tiled=True)  9.18 us
  transfers between devices with their start and end apart: 10, of which 4 were waited for; matrix products, arithmetic and copies ran while one was open for 1% of the time, Pallas kernels for 4%

profile of v8, /device:TPU:32, one launch (start us, length us, event | category | flops | bytes accessed | tf_op | source)
XLA Modules:
  0.0 125.9 jit_solution(17951763843969678414)
XLA Ops:
  0.7 3.0 %attend.1 = (bf16[4,8,1024]{2,1,0:T(8,128)(2,1)S(1)}, bf16[3136,128]{1,0:T(8,128)(2,1)S(1)}, f32[8,128]{1,0:T(8,128)S(1)}) custom-call(bf16[8,1024]{1,0:T(8,128)(2,1)} %tokens.1, bf16[1024]{0:T(1024)(128)(2,1)} %refs_1_.1, bf16[1024,256]{1,0:T(8,128)(2,1)} %refs_2_.1, bf16[128]{0:T(256)(128)(2,1)} %refs_3_.1, bf16[1024,128]{1,0:T(8,128)(2,1)} %refs_4_.1, ...), custom_call_target="tpu_custom_call" | custom-call | tf_op jit(solution)/shard_map/attend/pallas_call | solution.py:420
  3.6 0.0 copy-start
  3.6 3.5 %collective-permute-start.2 = (bf16[3136,128]{1,0:T(8,128)(2,1)S(1)}, bf16[3136,128]{1,0:T(8,128)(2,1)}, u32[]{:S(2)}, u32[]{:S(2)}) collective-permute-start(bf16[3136,128]{1,0:T(8,128)(2,1)S(1)} %get-tuple-element.16.refs_0_), channel_id=1, source_target_pairs={{0,1},{1,2},{2,3},{3,0},{4,7},{5,4},{6,5},{7,6},{8,9},{9,10},{10,1... | collective-permute-start | bytes 2408456 | tf_op jit(solution)/shard_map/ppermute | solution.py:43
  7.1 3.6 %collective-permute-start.3 = (bf16[3136,128]{1,0:T(8,128)(2,1)S(1)}, bf16[3136,128]{1,0:T(8,128)(2,1)}, u32[]{:S(2)}, u32[]{:S(2)}) collective-permute-start(bf16[3136,128]{1,0:T(8,128)(2,1)S(1)} %get-tuple-element.16.refs_0_), channel_id=1, source_target_pairs={{0,3},{1,0},{2,1},{3,2},{4,5},{5,6},{6,7},{7,4},{8,11},{9,8},{10,9... | collective-permute-start | bytes 2408456 | tf_op jit(solution)/shard_map/ppermute | solution.py:43
  10.7 13.4 %collective-permute-done.2.refs_1_ = bf16[3136,128]{1,0:T(8,128)(2,1)} collective-permute-done((bf16[3136,128]{1,0:T(8,128)(2,1)S(1)}, bf16[3136,128]{1,0:T(8,128)(2,1)}, u32[]{:S(2)}, u32[]{:S(2)}) %collective-permute-start.2) | collective-permute-done | bytes 802848 | tf_op jit(solution)/shard_map/ppermute | solution.py:43
  24.1 3.8 %collective-permute-start.4 = (bf16[3136,128]{1,0:T(8,128)(2,1)}, bf16[3136,128]{1,0:T(8,128)(2,1)}, u32[]{:S(2)}, u32[]{:S(2)}) collective-permute-start(bf16[3136,128]{1,0:T(8,128)(2,1)} %collective-permute-done.2.refs_1_), channel_id=1, source_target_pairs={{0,1},{1,2},{2,3},{3,0},{4,7},{5,4},{6,5},{7,6},{8,9},{9,10},{10,1... | collective-permute-start | bytes 2408456 | tf_op jit(solution)/shard_map/ppermute | solution.py:43
  27.9 1.9 %collective-permute-start.1 = (bf16[3136,128]{1,0:T(8,128)(2,1)S(1)}, bf16[3136,128]{1,0:T(8,128)(2,1)}, u32[]{:S(2)}, u32[]{:S(2)}) collective-permute-start(bf16[3136,128]{1,0:T(8,128)(2,1)S(1)} %get-tuple-element.16.refs_0_), channel_id=1, source_target_pairs={{0,4},{4,0},{1,5},{5,1},{2,6},{6,2},{3,7},{7,3},{8,12},{12,8},{9,1... | collective-permute-start | bytes 2408456 | tf_op jit(solution)/shard_map/ppermute | solution.py:21
  29.9 2.4 %collective-permute-start.5 = (bf16[3136,128]{1,0:T(8,128)(2,1)}, bf16[3136,128]{1,0:T(8,128)(2,1)}, u32[]{:S(2)}, u32[]{:S(2)}) collective-permute-start(bf16[3136,128]{1,0:T(8,128)(2,1)} %collective-permute-done.2.refs_1_), channel_id=1, source_target_pairs={{0,4},{4,0},{1,5},{5,1},{2,6},{6,2},{3,7},{7,3},{8,12},{12,8},{9,1... | collective-permute-start | bytes 2408456 | tf_op jit(solution)/shard_map/ppermute | solution.py:21
  32.3 0.0 collective-permute-done.3.refs_2_
  32.3 1.9 %collective-permute-start.6 = (bf16[3136,128]{1,0:T(8,128)(2,1)}, bf16[3136,128]{1,0:T(8,128)(2,1)}, u32[]{:S(2)}, u32[]{:S(2)}) collective-permute-start(bf16[3136,128]{1,0:T(8,128)(2,1)} %collective-permute-done.3.refs_2_), channel_id=1, source_target_pairs={{0,4},{4,0},{1,5},{5,1},{2,6},{6,2},{3,7},{7,3},{8,12},{12,8},{9,1... | collective-permute-start | bytes 2408456 | tf_op jit(solution)/shard_map/ppermute | solution.py:21
  34.2 6.3 %collective-permute-done.4.refs_3_ = bf16[3136,128]{1,0:T(8,128)(2,1)} collective-permute-done((bf16[3136,128]{1,0:T(8,128)(2,1)}, bf16[3136,128]{1,0:T(8,128)(2,1)}, u32[]{:S(2)}, u32[]{:S(2)}) %collective-permute-start.4) | collective-permute-done | bytes 802848 | tf_op jit(solution)/shard_map/ppermute | solution.py:43
  40.5 1.9 %collective-permute-start.7 = (bf16[3136,128]{1,0:T(8,128)(2,1)}, bf16[3136,128]{1,0:T(8,128)(2,1)}, u32[]{:S(2)}, u32[]{:S(2)}) collective-permute-start(bf16[3136,128]{1,0:T(8,128)(2,1)} %collective-permute-done.4.refs_3_), channel_id=1, source_target_pairs={{0,4},{4,0},{1,5},{5,1},{2,6},{6,2},{3,7},{7,3},{8,12},{12,8},{9,1... | collective-permute-start | bytes 2408456 | tf_op jit(solution)/shard_map/ppermute | solution.py:21
  42.4 0.0 copy-start.1
  42.5 0.0 copy-start.2
  42.5 9.2 %all_to_all.25.partial = bf16[4,8,1024]{2,1,0:T(8,128)(2,1)S(1)} all-to-all(bf16[4,8,1024]{2,1,0:T(8,128)(2,1)S(1)} %get-tuple-element.13), channel_id=1, replica_groups=mesh['ep_0'=16,'ep_1'=4,'ep_2'=2,'tp'=4] {'tp'}, dimensions={0} | all-to-all | bytes 131072 | tf_op jit(solution)/shard_map/all_to_all | solution.py:433
  51.6 0.0 copy-done.1
  51.6 0.0 copy-done.2
  51.7 0.8 rows.1
  52.4 0.0 copy-start.5
  52.4 0.0 copy-start.3
  52.4 0.0 copy-start.4
  52.4 15.3 %all-to-all-start.1 = ((bf16[144,2,128]{2,1,0:T(2,128)(2,1)}), bf16[144,2,128]{2,1,0:T(2,128)(2,1)S(1)}, u32[]{:S(2)}, u32[]{:S(2)}) async-start(bf16[144,2,128]{2,1,0:T(2,128)(2,1)} %bitcast.8), calls=%async_computation.1 | async-start | bytes 147456 | tf_op jit(solution)/shard_map/all_to_all | solution.py:455
  67.8 0.0 copy-done.5
  67.8 0.0 copy-done.3
  67.8 0.0 copy-done.4
  67.8 1.9 %collective-permute-start = (bf16[128,1024]{1,0:T(8,128)(2,1)S(1)}, bf16[128,1024]{1,0:T(8,128)(2,1)S(1)}, u32[]{:S(2)}, u32[]{:S(2)}) collective-permute-start(bf16[128,1024]{1,0:T(8,128)(2,1)S(1)} %fusion.4.front), channel_id=1, source_target_pairs={{0,4},{4,0},{1,5},{5,1},{2,6},{6,2},{3,7},{7,3},{8,12},{12,8},{9,1... | collective-permute-start | bytes 786440 | tf_op jit(solution)/shard_map/ppermute | solution.py:21
  69.8 9.8 %all-to-all-done.1 = bf16[144,2,128]{2,1,0:T(2,128)(2,1)S(1)} async-done(((bf16[144,2,128]{2,1,0:T(2,128)(2,1)}), bf16[144,2,128]{2,1,0:T(2,128)(2,1)S(1)}, u32[]{:S(2)}, u32[]{:S(2)}) %all-to-all-start.1) | async-done | bytes 73760 | tf_op jit(solution)/shard_map/all_to_all | solution.py:455
  79.6 0.9 tile.4
  80.4 0.0 copy-done
  80.4 4.3 %all-to-all-start.2 = ((bf16[576,2,128]{2,1,0:T(2,128)(2,1)}), bf16[576,2,128]{2,1,0:T(2,128)(2,1)S(1)}, u32[]{:S(2)}, u32[]{:S(2)}) async-start(bf16[576,2,128]{2,1,0:T(2,128)(2,1)} %bitcast.9), calls=%async_computation.2 | async-start | bytes 589824 | tf_op jit(solution)/shard_map/all_to_all | solution.py:457
  84.7 0.0 collective-permute-done.pair_front
  84.7 6.9 %all-to-all-done.2 = bf16[576,2,128]{2,1,0:T(2,128)(2,1)S(1)} async-done(((bf16[576,2,128]{2,1,0:T(2,128)(2,1)}), bf16[576,2,128]{2,1,0:T(2,128)(2,1)S(1)}, u32[]{:S(2)}, u32[]{:S(2)}) %all-to-all-start.2) | async-done | bytes 294944 | tf_op jit(solution)/shard_map/all_to_all | solution.py:457
  91.6 0.0 collective-permute-done.1.resident
  91.6 0.0 collective-permute-done.5.refs_4_
  91.6 0.0 collective-permute-done.6.refs_5_
  91.6 4.7 %share.1 = (f32[1024,128]{1,0:T(8,128)S(1)}, bf16[128,1024]{1,0:T(8,128)(2,1)S(1)}, f32[128,128]{1,0:T(8,128)S(1)}) custom-call(bf16[1152,128]{1,0:T(8,128)(2,1)S(1)} %bitcast.17, bf16[128,1024]{1,0:T(8,128)(2,1)S(1)} %fusion.4.front, bf16[128,1024]{1,0:T(8,128)(2,1)S(1)} %collective-permute-done.pair_front, ...), custom_call_target="tpu_custom_call" | custom-call | tf_op jit(solution)/shard_map/share/pallas_call | solution.py:466
  96.3 0.0 collective-permute-done.7.pack
  96.3 1.7 %last.1 = bf16[1024,128]{1,0:T(8,128)(2,1)S(1)} custom-call(f32[1024,128]{1,0:T(8,128)S(1)} %get-tuple-element.17.partial, bf16[128,1024]{1,0:T(8,128)(2,1)S(1)} %get-tuple-element.18.narrow, f32[128,128]{1,0:T(8,128)S(1)} %get-tuple-element.19.aside, bf16[3136,128]{1,0:T(8,128)(2,1)} %collective-permute-done.7.pack), custom_call_target="tpu_custom_call" | custom-call | tf_op jit(solution)/shard_map/last/pallas_call | solution.py:486
  98.0 11.5 %all_to_all.26 = bf16[512,2,128]{2,1,0:T(2,128)(2,1)S(1)} all-to-all(bf16[512,2,128]{2,1,0:T(2,128)(2,1)S(1)} %bitcast.19), channel_id=1, replica_groups=mesh['ep_0'=16,'ep_1'=4,'ep_2'=2,'tp'=4] {'ep_1','tp'}, dimensions={0} | all-to-all | bytes 524288 | tf_op jit(solution)/shard_map/all_to_all | solution.py:494
  109.5 0.1 fold.1
  109.6 15.6 %all_to_all.27 = bf16[128,2,128]{2,1,0:T(2,128)(2,1)S(1)} all-to-all(bf16[128,2,128]{2,1,0:T(2,128)(2,1)S(1)} %bitcast.20), channel_id=1, replica_groups=mesh['ep_0'=16,'ep_1'=4,'ep_2'=2,'tp'=4] {'ep_0'}, dimensions={0} | all-to-all | bytes 131072 | tf_op jit(solution)/shard_map/all_to_all | solution.py:508
  125.3 0.6 finish.1
  (2 shorter events, 0.0 us)
Async XLA Ops:
  3.6 76.8 %copy-start = (bf16[3136,128]{1,0:T(8,128)(2,1)}, bf16[3136,128]{1,0:T(8,128)(2,1)S(1)}, u32[]{:S(2)}) copy-start(bf16[3136,128]{1,0:T(8,128)(2,1)S(1)} %get-tuple-element.16.refs_0_) | copy-start | bytes 2408452
  3.6 20.5 %collective-permute-start.2 = (bf16[3136,128]{1,0:T(8,128)(2,1)S(1)}, bf16[3136,128]{1,0:T(8,128)(2,1)}, u32[]{:S(2)}, u32[]{:S(2)}) collective-permute-start(bf16[3136,128]{1,0:T(8,128)(2,1)S(1)} %get-tuple-element.16.refs_0_), channel_id=1, source_target_pairs={{0,1},{1,2},{2,3},{3,0},{4,7},{5,4},{6,5},{7,6},{8,9},{9,10},{10,1... | collective-permute-start | bytes 2408456 | tf_op jit(solution)/shard_map/ppermute | solution.py:43
  7.1 25.1 %collective-permute-start.3 = (bf16[3136,128]{1,0:T(8,128)(2,1)S(1)}, bf16[3136,128]{1,0:T(8,128)(2,1)}, u32[]{:S(2)}, u32[]{:S(2)}) collective-permute-start(bf16[3136,128]{1,0:T(8,128)(2,1)S(1)} %get-tuple-element.16.refs_0_), channel_id=1, source_target_pairs={{0,3},{1,0},{2,1},{3,2},{4,5},{5,6},{6,7},{7,4},{8,11},{9,8},{10,9... | collective-permute-start | bytes 2408456 | tf_op jit(solution)/shard_map/ppermute | solution.py:43
  24.1 16.4 %collective-permute-start.4 = (bf16[3136,128]{1,0:T(8,128)(2,1)}, bf16[3136,128]{1,0:T(8,128)(2,1)}, u32[]{:S(2)}, u32[]{:S(2)}) collective-permute-start(bf16[3136,128]{1,0:T(8,128)(2,1)} %collective-permute-done.2.refs_1_), channel_id=1, source_target_pairs={{0,1},{1,2},{2,3},{3,0},{4,7},{5,4},{6,5},{7,6},{8,9},{9,10},{10,1... | collective-permute-start | bytes 2408456 | tf_op jit(solution)/shard_map/ppermute | solution.py:43
  27.9 63.7 %collective-permute-start.1 = (bf16[3136,128]{1,0:T(8,128)(2,1)S(1)}, bf16[3136,128]{1,0:T(8,128)(2,1)}, u32[]{:S(2)}, u32[]{:S(2)}) collective-permute-start(bf16[3136,128]{1,0:T(8,128)(2,1)S(1)} %get-tuple-element.16.refs_0_), channel_id=1, source_target_pairs={{0,4},{4,0},{1,5},{5,1},{2,6},{6,2},{3,7},{7,3},{8,12},{12,8},{9,1... | collective-permute-start | bytes 2408456 | tf_op jit(solution)/shard_map/ppermute | solution.py:21
  29.9 61.7 %collective-permute-start.5 = (bf16[3136,128]{1,0:T(8,128)(2,1)}, bf16[3136,128]{1,0:T(8,128)(2,1)}, u32[]{:S(2)}, u32[]{:S(2)}) collective-permute-start(bf16[3136,128]{1,0:T(8,128)(2,1)} %collective-permute-done.2.refs_1_), channel_id=1, source_target_pairs={{0,4},{4,0},{1,5},{5,1},{2,6},{6,2},{3,7},{7,3},{8,12},{12,8},{9,1... | collective-permute-start | bytes 2408456 | tf_op jit(solution)/shard_map/ppermute | solution.py:21
  32.3 59.3 %collective-permute-start.6 = (bf16[3136,128]{1,0:T(8,128)(2,1)}, bf16[3136,128]{1,0:T(8,128)(2,1)}, u32[]{:S(2)}, u32[]{:S(2)}) collective-permute-start(bf16[3136,128]{1,0:T(8,128)(2,1)} %collective-permute-done.3.refs_2_), channel_id=1, source_target_pairs={{0,4},{4,0},{1,5},{5,1},{2,6},{6,2},{3,7},{7,3},{8,12},{12,8},{9,1... | collective-permute-start | bytes 2408456 | tf_op jit(solution)/shard_map/ppermute | solution.py:21
  40.5 55.8 %collective-permute-start.7 = (bf16[3136,128]{1,0:T(8,128)(2,1)}, bf16[3136,128]{1,0:T(8,128)(2,1)}, u32[]{:S(2)}, u32[]{:S(2)}) collective-permute-start(bf16[3136,128]{1,0:T(8,128)(2,1)} %collective-permute-done.4.refs_3_), channel_id=1, source_target_pairs={{0,4},{4,0},{1,5},{5,1},{2,6},{6,2},{3,7},{7,3},{8,12},{12,8},{9,1... | collective-permute-start | bytes 2408456 | tf_op jit(solution)/shard_map/ppermute | solution.py:21
  42.4 9.2 %copy-start.1 = (bf16[8,1024]{1,0:T(8,128)(2,1)S(1)}, bf16[8,1024]{1,0:T(8,128)(2,1)}, u32[]{:S(2)}) copy-start(bf16[8,1024]{1,0:T(8,128)(2,1)} %tokens.1) | copy-start | bytes 49156
  42.5 9.2 %copy-start.2 = (bf16[1024]{0:T(1024)(128)(2,1)S(1)}, bf16[1024]{0:T(1024)(128)(2,1)}, u32[]{:S(2)}) copy-start(bf16[1024]{0:T(1024)(128)(2,1)} %ffn_gain.1) | copy-start | bytes 6148
  52.4 15.4 %copy-start.5 = (bf16[1024]{0:T(1024)(128)(2,1)S(1)}, bf16[1024]{0:T(1024)(128)(2,1)}, u32[]{:S(2)}) copy-start(bf16[1024]{0:T(1024)(128)(2,1)} %param.39) | copy-start | bytes 6148
  52.4 15.4 %copy-start.3 = (bf16[1024,32]{0,1:T(8,128)(2,1)S(1)}, bf16[1024,32]{0,1:T(8,128)(2,1)}, u32[]{:S(2)}) copy-start(bf16[1024,32]{0,1:T(8,128)(2,1)} %param.41) | copy-start | bytes 196612
  52.4 15.4 %copy-start.4 = (bf16[1024,32]{0,1:T(8,128)(2,1)S(1)}, bf16[1024,32]{0,1:T(8,128)(2,1)}, u32[]{:S(2)}) copy-start(bf16[1024,32]{0,1:T(8,128)(2,1)} %param.40) | copy-start | bytes 196612
  52.4 27.1 %all-to-all-start.1 = ((bf16[144,2,128]{2,1,0:T(2,128)(2,1)}), bf16[144,2,128]{2,1,0:T(2,128)(2,1)S(1)}, u32[]{:S(2)}, u32[]{:S(2)}) async-start(bf16[144,2,128]{2,1,0:T(2,128)(2,1)} %bitcast.8), calls=%async_computation.1 | async-start | bytes 147456 | tf_op jit(solution)/shard_map/all_to_all | solution.py:455
  67.8 16.9 %collective-permute-start = (bf16[128,1024]{1,0:T(8,128)(2,1)S(1)}, bf16[128,1024]{1,0:T(8,128)(2,1)S(1)}, u32[]{:S(2)}, u32[]{:S(2)}) collective-permute-start(bf16[128,1024]{1,0:T(8,128)(2,1)S(1)} %fusion.4.front), channel_id=1, source_target_pairs={{0,4},{4,0},{1,5},{5,1},{2,6},{6,2},{3,7},{7,3},{8,12},{12,8},{9,1... | collective-permute-start | bytes 786440 | tf_op jit(solution)/shard_map/ppermute | solution.py:21
  80.4 11.1 %all-to-all-start.2 = ((bf16[576,2,128]{2,1,0:T(2,128)(2,1)}), bf16[576,2,128]{2,1,0:T(2,128)(2,1)S(1)}, u32[]{:S(2)}, u32[]{:S(2)}) async-start(bf16[576,2,128]{2,1,0:T(2,128)(2,1)} %bitcast.9), calls=%async_computation.2 | async-start | bytes 589824 | tf_op jit(solution)/shard_map/all_to_all | solution.py:457

commit v9 on v6

--- a/solution.py
+++ b/solution.py
@@ -213,18 +213,18 @@
     return jnp.concatenate(columns, axis=1)
 
 
-def share_kernel(rows, front, pair_front, resident, *refs):
+def share_kernel(rows, front, pair_front, *refs):
     sources, refs = refs[:-7], refs[-7:]
     out, narrow, aside, wide, columns, staged, sems = refs
     copies = []
     for i, source in enumerate(sources):
         copies.append(pltpu.make_async_copy(source, staged.at[i], sems.at[i]))
-        copies[-1].start()
     members = lax.axis_size("tp")
     packs = [staged.at[i] for i in range(len(sources))]
-    packs.insert(members, resident)
     member = lax.axis_index("tp")
     core = lax.axis_index(PAIR)
+    for copy in copies:
+        copy.start()
     experts = (lax.axis_index(EP), lax.axis_index(EP) + 1 - 2 * core)
     width = front.shape[1]
     count = narrow.shape[0]
@@ -257,7 +257,7 @@
     down_start = 2 * width
     shared_start = down_start + blocks * LANES
     per_member = blocks // members
-    units = (resident.shape[0] - shared_start) // per_member
+    units = (packs[0].shape[0] - shared_start) // per_member
 
     fronts = [
         lax.dot_general(
@@ -274,11 +274,9 @@
     aside[:, LANES - units :] = shared[1].astype(jnp.float32)
 
     hidden = []
-    first_hidden = hidden_of(values, resident, width)
-    for copy, pack in zip(copies, packs[:members] + packs[members + 1 :]):
+    for copy, pack in zip(copies, packs):
         copy.wait()
         hidden.append(hidden_of(values, pack, width))
-    hidden.insert(members, first_hidden)
     ahead = jnp.where(core == 0, members - 1, 1)
     origins = (0, ahead, members - ahead, 2)
     for s, pair in enumerate((0, 2, 1, None)):
@@ -458,11 +456,11 @@
     pair_packs = []
     for pack in packs:
         pair_packs.append(swap(pack))
-    streamed = packs + pair_packs[1:-1]
+    streamed = packs + pair_packs[:-1]
     local_columns = pltpu.VMEM((members, peers, width // members), jnp.float32)
     partial_share, narrow, aside = pl.pallas_call(
         share_kernel,
-        in_specs=[VMEM] * 4 + [ANY] * len(streamed),
+        in_specs=[VMEM] * 3 + [ANY] * len(streamed),
         out_specs=[VMEM] * 3,
         out_shape=[
             pltpu.VMEM((peers * blocks, LANES), jnp.float32),
@@ -477,7 +475,7 @@
         ],
         name="share",
     )(
-        *map(in_vmem, (own_rows.reshape(sub_rows, LANES), front, pair_front, pair_packs[0])),
+        *map(in_vmem, (own_rows.reshape(sub_rows, LANES), front, pair_front)),
         *streamed,
     )
     total = pl.pallas_call(

time: 120 us -> 118 us (0.983)
  local copies, waits for them, and re-layouts: 2.06 us -> 0.03 us
    unnamed x16 -> x12, local copies, waits for them, and re-layouts: 2.06 us -> 0.03 us
  transfers between devices with their start and end apart: 9 -> 9, of which waited for: 2 -> 3; matrix products, arithmetic and copies ran while one was open for 0% -> 0% of each run, Pallas kernels for 4% -> 4%
where the time goes in v9:
time: 118 us; the launch traced here: 117 us
  starting transfers between devices  50 us (42%)
  blocking collectives  46.4 us (39%)
  Pallas kernels  10.2 us (9%)
  waiting for transfers between devices  9.12 us (8%)
    all_to_all x1, starting transfers between devices, per_device(): lax.all_to_all(outgoing.reshape(-1, 2, LANES), EP[:2], 0, 0, tiled=True)  21.6 us
    all_to_all x1, blocking collectives, per_device(): parts = lax.all_to_all(parts.reshape(-1, 2, LANES), EP[0], 0, 0, tiled=True)  18.8 us
    ppermute x5, starting transfers between devices, swap(): return lax.ppermute(shard, PAIR, [(0, 1), (1, 0)])  16 us
    all_to_all x1, blocking collectives, per_device(): lax.all_to_all(total.reshape(-1, 2, LANES), ('ep_1', 'tp'), 0, 0, tiled=T...  15.2 us
    ppermute x3, starting transfers between devices, shifted(): return lax.ppermute(shard, (PAIR, 'tp'), pairs)  12.5 us
    all_to_all x1, blocking collectives, per_device(): partial = lax.all_to_all(partial, 'tp', 0, 0, tiled=True)  12.4 us
    ppermute x3, waiting for transfers between devices, shifted(): return lax.ppermute(shard, (PAIR, 'tp'), pairs)  7.16 us
    pallas_call x1, Pallas kernels, per_device(): pl.pallas_call(share_kernel, in_specs=[VMEM] * 3 + [ANY] * len(streamed),...  3.97 us
  transfers between devices with their start and end apart: 9, of which 3 were waited for; matrix products, arithmetic and copies ran while one was open for 0% of the time, Pallas kernels for 4%

profile of v9, /device:TPU:1, one launch (start us, length us, event | category | flops | bytes accessed | tf_op | source)
XLA Modules:
  0.0 116.7 jit_solution(6111443433997035636)
XLA Ops:
  0.7 3.0 %attend.1 = (bf16[4,8,1024]{2,1,0:T(8,128)(2,1)S(1)}, bf16[3136,128]{1,0:T(8,128)(2,1)S(1)}, f32[8,128]{1,0:T(8,128)S(1)}) custom-call(bf16[8,1024]{1,0:T(8,128)(2,1)} %tokens.1, bf16[1024]{0:T(1024)(128)(2,1)} %refs_1_.1, bf16[1024,256]{1,0:T(8,128)(2,1)} %refs_2_.1, bf16[128]{0:T(256)(128)(2,1)} %refs_3_.1, bf16[1024,128]{1,0:T(8,128)(2,1)} %refs_4_.1, ...), custom_call_target="tpu_custom_call" | custom-call | tf_op jit(solution)/shard_map/attend/pallas_call | solution.py:418
  3.6 0.0 copy-start
  3.6 5.5 %collective-permute-start.1 = (bf16[3136,128]{1,0:T(8,128)(2,1)S(1)}, bf16[3136,128]{1,0:T(8,128)(2,1)}, u32[]{:S(2)}, u32[]{:S(2)}) collective-permute-start(bf16[3136,128]{1,0:T(8,128)(2,1)S(1)} %get-tuple-element.16.refs_0_), channel_id=1, source_target_pairs={{0,1},{1,2},{2,3},{3,0},{4,7},{5,4},{6,5},{7,6},{8,9},{9,10},{10,1... | collective-permute-start | bytes 2408456 | tf_op jit(solution)/shard_map/ppermute | solution.py:43
  9.1 1.9 %collective-permute-start.2 = (bf16[3136,128]{1,0:T(8,128)(2,1)S(1)}, bf16[3136,128]{1,0:T(8,128)(2,1)}, u32[]{:S(2)}, u32[]{:S(2)}) collective-permute-start(bf16[3136,128]{1,0:T(8,128)(2,1)S(1)} %get-tuple-element.16.refs_0_), channel_id=1, source_target_pairs={{0,3},{1,0},{2,1},{3,2},{4,5},{5,6},{6,7},{7,4},{8,11},{9,8},{10,9... | collective-permute-start | bytes 2408456 | tf_op jit(solution)/shard_map/ppermute | solution.py:43
  11.0 7.2 %collective-permute-done.1.refs_1_ = bf16[3136,128]{1,0:T(8,128)(2,1)} collective-permute-done((bf16[3136,128]{1,0:T(8,128)(2,1)S(1)}, bf16[3136,128]{1,0:T(8,128)(2,1)}, u32[]{:S(2)}, u32[]{:S(2)}) %collective-permute-start.1) | collective-permute-done | bytes 802848 | tf_op jit(solution)/shard_map/ppermute | solution.py:43
  18.2 5.1 %collective-permute-start.3 = (bf16[3136,128]{1,0:T(8,128)(2,1)}, bf16[3136,128]{1,0:T(8,128)(2,1)}, u32[]{:S(2)}, u32[]{:S(2)}) collective-permute-start(bf16[3136,128]{1,0:T(8,128)(2,1)} %collective-permute-done.1.refs_1_), channel_id=1, source_target_pairs={{0,1},{1,2},{2,3},{3,0},{4,7},{5,4},{6,5},{7,6},{8,9},{9,10},{10,1... | collective-permute-start | bytes 2408456 | tf_op jit(solution)/shard_map/ppermute | solution.py:43
  23.3 0.0 copy-start.1
  23.3 0.0 copy-start.2
  23.3 12.4 %all_to_all.20.partial = bf16[4,8,1024]{2,1,0:T(8,128)(2,1)S(1)} all-to-all(bf16[4,8,1024]{2,1,0:T(8,128)(2,1)S(1)} %get-tuple-element.13), channel_id=1, replica_groups=mesh['ep_0'=16,'ep_1'=4,'ep_2'=2,'tp'=4] {'tp'}, dimensions={0} | all-to-all | bytes 131072 | tf_op jit(solution)/shard_map/all_to_all | solution.py:431
  35.8 0.0 copy-done.1
  35.8 0.0 copy-done.2
  35.8 0.9 rows.1
  36.7 0.0 copy-start.5
  36.7 0.0 copy-start.3
  36.7 0.0 copy-start.4
  36.7 21.6 %all-to-all-start.1 = ((bf16[576,2,128]{2,1,0:T(2,128)(2,1)}), bf16[576,2,128]{2,1,0:T(2,128)(2,1)S(1)}, u32[]{:S(2)}, u32[]{:S(2)}) async-start(bf16[576,2,128]{2,1,0:T(2,128)(2,1)} %bitcast.8), calls=%async_computation.1 | async-start | bytes 589824 | tf_op jit(solution)/shard_map/all_to_all | solution.py:452
  58.2 7.3 %collective-permute-start.4 = (bf16[3136,128]{1,0:T(8,128)(2,1)S(1)}, bf16[3136,128]{1,0:T(8,128)(2,1)}, u32[]{:S(2)}, u32[]{:S(2)}) collective-permute-start(bf16[3136,128]{1,0:T(8,128)(2,1)S(1)} %get-tuple-element.16.refs_0_), channel_id=1, source_target_pairs={{0,4},{4,0},{1,5},{5,1},{2,6},{6,2},{3,7},{7,3},{8,12},{12,8},{9,1... | collective-permute-start | bytes 2408456 | tf_op jit(solution)/shard_map/ppermute | solution.py:21
  65.6 0.0 collective-permute-done.2.refs_2_
  65.6 1.9 %collective-permute-start.6 = (bf16[3136,128]{1,0:T(8,128)(2,1)}, bf16[3136,128]{1,0:T(8,128)(2,1)}, u32[]{:S(2)}, u32[]{:S(2)}) collective-permute-start(bf16[3136,128]{1,0:T(8,128)(2,1)} %collective-permute-done.2.refs_2_), channel_id=1, source_target_pairs={{0,4},{4,0},{1,5},{5,1},{2,6},{6,2},{3,7},{7,3},{8,12},{12,8},{9,1... | collective-permute-start | bytes 2408456 | tf_op jit(solution)/shard_map/ppermute | solution.py:21
  67.5 2.4 %collective-permute-start.5 = (bf16[3136,128]{1,0:T(8,128)(2,1)}, bf16[3136,128]{1,0:T(8,128)(2,1)}, u32[]{:S(2)}, u32[]{:S(2)}) collective-permute-start(bf16[3136,128]{1,0:T(8,128)(2,1)} %collective-permute-done.1.refs_1_), channel_id=1, source_target_pairs={{0,4},{4,0},{1,5},{5,1},{2,6},{6,2},{3,7},{7,3},{8,12},{12,8},{9,1... | collective-permute-start | bytes 2408456 | tf_op jit(solution)/shard_map/ppermute | solution.py:21
  69.9 0.0 collective-permute-done.3.refs_3_
  69.9 1.9 %collective-permute-start.7 = (bf16[3136,128]{1,0:T(8,128)(2,1)}, bf16[3136,128]{1,0:T(8,128)(2,1)}, u32[]{:S(2)}, u32[]{:S(2)}) collective-permute-start(bf16[3136,128]{1,0:T(8,128)(2,1)} %collective-permute-done.3.refs_3_), channel_id=1, source_target_pairs={{0,4},{4,0},{1,5},{5,1},{2,6},{6,2},{3,7},{7,3},{8,12},{12,8},{9,1... | collective-permute-start | bytes 2408456 | tf_op jit(solution)/shard_map/ppermute | solution.py:21
  71.9 0.0 copy-done.5
  71.9 0.0 copy-done.3
  71.9 0.0 copy-done.4
  71.9 2.4 %collective-permute-start = (bf16[128,1024]{1,0:T(8,128)(2,1)S(1)}, bf16[128,1024]{1,0:T(8,128)(2,1)S(1)}, u32[]{:S(2)}, u32[]{:S(2)}) collective-permute-start(bf16[128,1024]{1,0:T(8,128)(2,1)S(1)} %fusion.4.front), channel_id=1, source_target_pairs={{0,4},{4,0},{1,5},{5,1},{2,6},{6,2},{3,7},{7,3},{8,12},{12,8},{9,1... | collective-permute-start | bytes 786440 | tf_op jit(solution)/shard_map/ppermute | solution.py:21
  74.3 1.1 collective-permute-done.pair_front
  75.5 0.0 collective-permute-done.4.refs_4_
  75.5 0.8 all-to-all-done.1
  76.3 0.0 collective-permute-done.6.refs_6_
  76.3 0.0 collective-permute-done.5.refs_5_
  76.3 0.0 copy-done
  76.3 4.0 %share.1 = (f32[1024,128]{1,0:T(8,128)S(1)}, bf16[128,1024]{1,0:T(8,128)(2,1)S(1)}, f32[128,128]{1,0:T(8,128)S(1)}) custom-call(bf16[1152,128]{1,0:T(8,128)(2,1)S(1)} %bitcast.16, bf16[128,1024]{1,0:T(8,128)(2,1)S(1)} %fusion.4.front, bf16[128,1024]{1,0:T(8,128)(2,1)S(1)} %collective-permute-done.pair_front, bf16[3136,128]{1,0:T(8,128)(2,1)} %copy-done, ...), custom_call_target="tpu_custom_call" | custom-call | tf_op jit(solution)/shard_map/share/pallas_call | solution.py:461
  80.3 0.0 collective-permute-done.7.pack
  80.3 1.7 %last.1 = bf16[1024,128]{1,0:T(8,128)(2,1)S(1)} custom-call(f32[1024,128]{1,0:T(8,128)S(1)} %get-tuple-element.17.partial, bf16[128,1024]{1,0:T(8,128)(2,1)S(1)} %get-tuple-element.18.narrow, f32[128,128]{1,0:T(8,128)S(1)} %get-tuple-element.19.aside, bf16[3136,128]{1,0:T(8,128)(2,1)} %collective-permute-done.7.pack), custom_call_target="tpu_custom_call" | custom-call | tf_op jit(solution)/shard_map/last/pallas_call | solution.py:481
  82.0 15.2 %all_to_all.21 = bf16[512,2,128]{2,1,0:T(2,128)(2,1)S(1)} all-to-all(bf16[512,2,128]{2,1,0:T(2,128)(2,1)S(1)} %bitcast.18), channel_id=1, replica_groups=mesh['ep_0'=16,'ep_1'=4,'ep_2'=2,'tp'=4] {'ep_1','tp'}, dimensions={0} | all-to-all | bytes 524288 | tf_op jit(solution)/shard_map/all_to_all | solution.py:489
  97.2 0.1 fold.1
  97.2 18.8 %all_to_all.22 = bf16[128,2,128]{2,1,0:T(2,128)(2,1)S(1)} all-to-all(bf16[128,2,128]{2,1,0:T(2,128)(2,1)S(1)} %bitcast.19), channel_id=1, replica_groups=mesh['ep_0'=16,'ep_1'=4,'ep_2'=2,'tp'=4] {'ep_0'}, dimensions={0} | all-to-all | bytes 131072 | tf_op jit(solution)/shard_map/all_to_all | solution.py:503
  116.1 0.6 finish.1
  (2 shorter events, 0.0 us)
Async XLA Ops:
  3.6 72.7 %copy-start = (bf16[3136,128]{1,0:T(8,128)(2,1)}, bf16[3136,128]{1,0:T(8,128)(2,1)S(1)}, u32[]{:S(2)}) copy-start(bf16[3136,128]{1,0:T(8,128)(2,1)S(1)} %get-tuple-element.16.refs_0_) | copy-start | bytes 2408452
  3.6 14.6 %collective-permute-start.1 = (bf16[3136,128]{1,0:T(8,128)(2,1)S(1)}, bf16[3136,128]{1,0:T(8,128)(2,1)}, u32[]{:S(2)}, u32[]{:S(2)}) collective-permute-start(bf16[3136,128]{1,0:T(8,128)(2,1)S(1)} %get-tuple-element.16.refs_0_), channel_id=1, source_target_pairs={{0,1},{1,2},{2,3},{3,0},{4,7},{5,4},{6,5},{7,6},{8,9},{9,10},{10,1... | collective-permute-start | bytes 2408456 | tf_op jit(solution)/shard_map/ppermute | solution.py:43
  9.1 56.5 %collective-permute-start.2 = (bf16[3136,128]{1,0:T(8,128)(2,1)S(1)}, bf16[3136,128]{1,0:T(8,128)(2,1)}, u32[]{:S(2)}, u32[]{:S(2)}) collective-permute-start(bf16[3136,128]{1,0:T(8,128)(2,1)S(1)} %get-tuple-element.16.refs_0_), channel_id=1, source_target_pairs={{0,3},{1,0},{2,1},{3,2},{4,5},{5,6},{6,7},{7,4},{8,11},{9,8},{10,9... | collective-permute-start | bytes 2408456 | tf_op jit(solution)/shard_map/ppermute | solution.py:43
  18.2 51.7 %collective-permute-start.3 = (bf16[3136,128]{1,0:T(8,128)(2,1)}, bf16[3136,128]{1,0:T(8,128)(2,1)}, u32[]{:S(2)}, u32[]{:S(2)}) collective-permute-start(bf16[3136,128]{1,0:T(8,128)(2,1)} %collective-permute-done.1.refs_1_), channel_id=1, source_target_pairs={{0,1},{1,2},{2,3},{3,0},{4,7},{5,4},{6,5},{7,6},{8,9},{9,10},{10,1... | collective-permute-start | bytes 2408456 | tf_op jit(solution)/shard_map/ppermute | solution.py:43
  23.3 12.5 %copy-start.1 = (bf16[8,1024]{1,0:T(8,128)(2,1)S(1)}, bf16[8,1024]{1,0:T(8,128)(2,1)}, u32[]{:S(2)}) copy-start(bf16[8,1024]{1,0:T(8,128)(2,1)} %tokens.1) | copy-start | bytes 49156
  23.3 12.4 %copy-start.2 = (bf16[1024]{0:T(1024)(128)(2,1)S(1)}, bf16[1024]{0:T(1024)(128)(2,1)}, u32[]{:S(2)}) copy-start(bf16[1024]{0:T(1024)(128)(2,1)} %ffn_gain.1) | copy-start | bytes 6148
  36.7 35.2 %copy-start.5 = (bf16[1024]{0:T(1024)(128)(2,1)S(1)}, bf16[1024]{0:T(1024)(128)(2,1)}, u32[]{:S(2)}) copy-start(bf16[1024]{0:T(1024)(128)(2,1)} %param.39) | copy-start | bytes 6148
  36.7 35.2 %copy-start.3 = (bf16[1024,32]{0,1:T(8,128)(2,1)S(1)}, bf16[1024,32]{0,1:T(8,128)(2,1)}, u32[]{:S(2)}) copy-start(bf16[1024,32]{0,1:T(8,128)(2,1)} %param.41) | copy-start | bytes 196612
  36.7 35.2 %copy-start.4 = (bf16[1024,32]{0,1:T(8,128)(2,1)S(1)}, bf16[1024,32]{0,1:T(8,128)(2,1)}, u32[]{:S(2)}) copy-start(bf16[1024,32]{0,1:T(8,128)(2,1)} %param.40) | copy-start | bytes 196612
  36.7 39.6 %all-to-all-start.1 = ((bf16[576,2,128]{2,1,0:T(2,128)(2,1)}), bf16[576,2,128]{2,1,0:T(2,128)(2,1)S(1)}, u32[]{:S(2)}, u32[]{:S(2)}) async-start(bf16[576,2,128]{2,1,0:T(2,128)(2,1)} %bitcast.8), calls=%async_computation.1 | async-start | bytes 589824 | tf_op jit(solution)/shard_map/all_to_all | solution.py:452
  58.2 17.2 %collective-permute-start.4 = (bf16[3136,128]{1,0:T(8,128)(2,1)S(1)}, bf16[3136,128]{1,0:T(8,128)(2,1)}, u32[]{:S(2)}, u32[]{:S(2)}) collective-permute-start(bf16[3136,128]{1,0:T(8,128)(2,1)S(1)} %get-tuple-element.16.refs_0_), channel_id=1, source_target_pairs={{0,4},{4,0},{1,5},{5,1},{2,6},{6,2},{3,7},{7,3},{8,12},{12,8},{9,1... | collective-permute-start | bytes 2408456 | tf_op jit(solution)/shard_map/ppermute | solution.py:21
  65.6 10.7 %collective-permute-start.6 = (bf16[3136,128]{1,0:T(8,128)(2,1)}, bf16[3136,128]{1,0:T(8,128)(2,1)}, u32[]{:S(2)}, u32[]{:S(2)}) collective-permute-start(bf16[3136,128]{1,0:T(8,128)(2,1)} %collective-permute-done.2.refs_2_), channel_id=1, source_target_pairs={{0,4},{4,0},{1,5},{5,1},{2,6},{6,2},{3,7},{7,3},{8,12},{12,8},{9,1... | collective-permute-start | bytes 2408456 | tf_op jit(solution)/shard_map/ppermute | solution.py:21
  67.5 8.8 %collective-permute-start.5 = (bf16[3136,128]{1,0:T(8,128)(2,1)}, bf16[3136,128]{1,0:T(8,128)(2,1)}, u32[]{:S(2)}, u32[]{:S(2)}) collective-permute-start(bf16[3136,128]{1,0:T(8,128)(2,1)} %collective-permute-done.1.refs_1_), channel_id=1, source_target_pairs={{0,4},{4,0},{1,5},{5,1},{2,6},{6,2},{3,7},{7,3},{8,12},{12,8},{9,1... | collective-permute-start | bytes 2408456 | tf_op jit(solution)/shard_map/ppermute | solution.py:21
  69.9 10.4 %collective-permute-start.7 = (bf16[3136,128]{1,0:T(8,128)(2,1)}, bf16[3136,128]{1,0:T(8,128)(2,1)}, u32[]{:S(2)}, u32[]{:S(2)}) collective-permute-start(bf16[3136,128]{1,0:T(8,128)(2,1)} %collective-permute-done.3.refs_3_), channel_id=1, source_target_pairs={{0,4},{4,0},{1,5},{5,1},{2,6},{6,2},{3,7},{7,3},{8,12},{12,8},{9,1... | collective-permute-start | bytes 2408456 | tf_op jit(solution)/shard_map/ppermute | solution.py:21
  71.9 3.6 %collective-permute-start = (bf16[128,1024]{1,0:T(8,128)(2,1)S(1)}, bf16[128,1024]{1,0:T(8,128)(2,1)S(1)}, u32[]{:S(2)}, u32[]{:S(2)}) collective-permute-start(bf16[128,1024]{1,0:T(8,128)(2,1)S(1)} %fusion.4.front), channel_id=1, source_target_pairs={{0,4},{4,0},{1,5},{5,1},{2,6},{6,2},{3,7},{7,3},{8,12},{12,8},{9,1... | collective-permute-start | bytes 786440 | tf_op jit(solution)/shard_map/ppermute | solution.py:21
